TPU v7x, 512 devices: a whole 4x8x8 slice. The times are simulated.
512 devices in a mesh: sp: 64 (over z, y), fs: 4 (over x), tp: 2 (over core).
Axes of the slice: x: 4, y: 8, z: 8, core: 2. Of those that a mesh axis runs over, the one named last changes fastest.
Arguments:
- q_latent: bfloat16 [16384, 512], P('sp'), may hold values from -6 to 6
- kv_latent: bfloat16 [16384, 256], P('sp'), may hold values from -6 to 6
- key_rope: bfloat16 [16384, 64], P('sp'), may hold values from -6 to 6
- pool_input: bfloat16 [16384, 1024], P('sp', 'fs'), may hold values from -6 to 6
- q_lat_gain: float32 [512], replicated, may hold values from 0.1 to 1.9
- kv_lat_gain: float32 [256], replicated, may hold values from 0.1 to 1.9
- q_head_gain: float32 [192], replicated, may hold values from 1 to 4.2
- k_head_gain: float32 [192], replicated, may hold values from 1 to 4.2
- pool_gain: float32 [1024], P(('fs', 'tp')), may hold values from 0.1 to 1.9
- q_up: bfloat16 [512, 3072], P(None, ('fs', 'tp')), may hold values from -1 to 1
- key_up: bfloat16 [256, 2048], P(None, ('fs', 'tp')), may hold values from -1 to 1
- value_up: bfloat16 [256, 2048], P(None, ('fs', 'tp')), may hold values from -0.375 to 0.375
- pool_mix: bfloat16 [4, 256, 256], P('fs', None, 'tp'), may hold values from -0.375 to 0.375
- out_pool: bfloat16 [1024, 4096], P(('fs', 'tp')), may hold values from -0.109375 to 0.109375
- out_attn: bfloat16 [2048, 4096], P(('fs', 'tp')), may hold values from -0.109375 to 0.109375
Outputs:
- mixed: bfloat16 [16384, 4096], P(('sp', 'fs', 'tp'))
- log_weight: float32 [16, 16384], P(('fs', 'tp'), 'sp')
All inputs are finite; a program needn't handle non-finite values.
Results may differ from a plain program's by a relative error of at most 0.015.
Values may be sent and summed in bfloat16 or wider, within the bound.
No kernel may reach another device: no remote copies, remote signals or barrier semaphores. Data moves between devices by JAX's collectives and lax.ppermute only.
A program may use at most 128 MiB of HBM per device.

v0:
```python
from functools import partial
import math

import jax
import jax.numpy as jnp
from jax import lax
from jax.sharding import PartitionSpec as P

NOPE = 128
ROPE = 64
VD = 128


EPS = 1e-06
THETA = 10000.0
HUGE = 1e30


def joined_along(tiles, dim):
    tiles = jnp.moveaxis(tiles, 0, dim)
    dims = tiles.shape
    return tiles.reshape(*dims[:dim], dims[dim] * dims[dim + 1], *dims[dim + 2 :])


def sent_to_all(shard, axis):
    length = lax.axis_size(axis)
    return lax.all_to_all(
        jnp.broadcast_to(shard[None], (length, *shard.shape)), axis, 0, 0, tiled=True
    )


def gathered_copies(shard, axis, dim):
    return joined_along(sent_to_all(shard, axis), dim)


def sent_together(arrays, axis, dim, along):
    both = jnp.concatenate(arrays, axis=along)
    whole, at, done = (gathered_copies(both, axis, dim), 0, [])
    for a in arrays:
        done.append(lax.slice_in_dim(whole, at, at + a.shape[along], axis=along))
        at += a.shape[along]
    return tuple(done)


def sent_together_2(arrays, axis, dim, along):
    ends, at = ([], 0)
    for a in arrays[:-1]:
        at += a.shape[along]
        ends.append(at)
    both = jnp.concatenate(arrays, axis=along)
    return tuple(jnp.split(lax.all_gather(both, axis, axis=dim, tiled=True), ends, axis=along))


def shifted(value, axis, steps):
    count = lax.axis_size(axis)
    initial, last = (max(0, -steps), min(count, count - steps))
    return lax.ppermute(value, axis, [(source, source + steps) for source in range(initial, last)])


def row_norm(values, row_gain):
    mean_sq = jnp.mean(values * values, axis=-1, keepdims=True)
    return values * lax.rsqrt(mean_sq + EPS) * row_gain


def rotate(values, position):
    half_width = values.shape[-1] // 2
    frequency = 1.0 / THETA ** (
        jnp.arange(0, 2 * half_width, 2, dtype=jnp.float32) / (2 * half_width)
    )
    angles = position.astype(jnp.float32)[:, None] * frequency[None, :]
    cosine_table = jnp.cos(angles)[:, None, :]
    sine_table = jnp.sin(angles)[:, None, :]
    first_half = values[..., :half_width]
    second_half = values[..., half_width:]
    return jnp.concatenate(
        [
            first_half * cosine_table - second_half * sine_table,
            first_half * sine_table + second_half * cosine_table,
        ],
        axis=-1,
    )


def make_queries(latent, lat_gain, q_up, norm_gain, position):
    row_count = latent.shape[0]
    normed = row_norm(latent.astype(jnp.float32), lat_gain).astype(jnp.bfloat16)
    query = jnp.dot(normed, q_up, preferred_element_type=jnp.float32).reshape(
        row_count, -1, NOPE + ROPE
    )
    query = row_norm(query, norm_gain)
    query = jnp.concatenate([query[..., :NOPE], rotate(query[..., NOPE:], position)], axis=-1)
    return (query * (NOPE + ROPE) ** (-0.5)).astype(jnp.bfloat16)


def make_keys(latent, rope_part, key_up, value_up, norm_gain, position):
    row_count = latent.shape[0]
    unrotated = jnp.dot(latent, key_up, preferred_element_type=jnp.float32).reshape(
        row_count, -1, NOPE
    )
    head_count = unrotated.shape[1]
    shared = jnp.broadcast_to(
        rope_part.astype(jnp.float32)[:, None, :], (row_count, head_count, ROPE)
    )
    key_heads = row_norm(jnp.concatenate([unrotated, shared], axis=-1), norm_gain)
    key_heads = jnp.concatenate(
        [key_heads[..., :NOPE], rotate(key_heads[..., NOPE:], position)], axis=-1
    )
    value_heads = jnp.dot(latent, value_up, preferred_element_type=jnp.float32).reshape(
        row_count, head_count, VD
    )
    return (key_heads.astype(jnp.bfloat16), value_heads.astype(jnp.bfloat16))


def attend_keys(query_block, query_pos, key_heads, value_heads, key_pos, state_now):
    running_max, running_sum, numerator = state_now
    scores = jnp.einsum("qhd,khd->qhk", query_block, key_heads, preferred_element_type=jnp.float32)
    allowed = key_pos[None, None, :] <= query_pos[:, None, None]
    scores = jnp.where(allowed, scores, -HUGE)
    new_max = jnp.maximum(running_max, jnp.max(scores, axis=-1))
    weights = jnp.where(allowed, jnp.exp(scores - new_max[..., None]), 0.0)
    factor = jnp.exp(running_max - new_max)
    new_sum = running_sum * factor + jnp.sum(weights, axis=-1)
    update = jnp.einsum(
        "qhk,khd->qhd",
        weights.astype(jnp.bfloat16),
        value_heads,
        preferred_element_type=jnp.float32,
    )
    return (new_max, new_sum, numerator * factor[..., None] + update)


def finish(state_now):
    running_max, running_sum, numerator = state_now
    return (numerator / running_sum[..., None], running_max + jnp.log(running_sum))


def local(
    q_latent,
    kv_latent,
    key_rope,
    pool_input,
    q_lat_gain,
    kv_lat_gain,
    q_head_gain,
    k_head_gain,
    pool_gain,
    q_up,
    key_up,
    value_up,
    pool_mix,
    out_pool,
    out_attn,
):
    row_count = q_latent.shape[0]
    half_rows = row_count // 2
    sp_index = lax.axis_index("sp")
    first_pos = sp_index * row_count
    own_pos = first_pos + jnp.arange(row_count, dtype=jnp.int32)
    queries = make_queries(q_latent, q_lat_gain, q_up, q_head_gain, own_pos)
    head_count = queries.shape[1]
    kv_normed = row_norm(kv_latent.astype(jnp.float32), kv_lat_gain).astype(jnp.bfloat16)
    lower_pos = own_pos[:half_rows]
    upper_queries = queries[half_rows:]
    upper_pos = own_pos[half_rows:]
    query_sets = (queries[:half_rows], upper_queries)
    position_sets = (lower_pos, upper_pos)
    last_pos = jnp.maximum(lower_pos[-1], upper_pos[-1])
    single = (
        jnp.full((half_rows, head_count), -HUGE, jnp.float32),
        jnp.zeros((half_rows, head_count), jnp.float32),
        jnp.zeros((half_rows, head_count, VD), jnp.float32),
    )
    initial = (single, single)
    group_size = lax.axis_size("fs") * lax.axis_size("tp")
    share_rows = row_count // group_size
    member = lax.axis_index("fs") * lax.axis_size("tp") + lax.axis_index("tp")
    own_latent = lax.dynamic_slice_in_dim(kv_normed, member * share_rows, share_rows, 0)
    own_rope = lax.dynamic_slice_in_dim(key_rope, member * share_rows, share_rows, 0)
    spread_latent, spread_rope = sent_together((own_latent, own_rope), "sp", 0, 1)
    span_rows = spread_latent.shape[0]
    incoming = sent_together_2((spread_latent, spread_rope), ("fs", "tp"), 0, 1)
    global_row = jnp.arange(incoming[0].shape[0], dtype=jnp.int32)
    owner_block = global_row // span_rows
    within = global_row % span_rows
    positions = within // share_rows * row_count + owner_block * share_rows + within % share_rows
    latent = incoming[0]
    rope_part = incoming[1]
    piece_rows = latent.shape[0]
    block_rows = math.gcd(piece_rows, 512)

    def advance(block_number, running_state):
        offset = block_number * block_rows
        lat_block = lax.dynamic_slice_in_dim(latent, offset, block_rows, 0)
        rope_block = lax.dynamic_slice_in_dim(rope_part, offset, block_rows, 0)
        key_pos = lax.dynamic_slice_in_dim(positions, offset, block_rows, 0)
        first_key = jnp.min(key_pos)

        def compute(states):
            key_heads, value_heads = make_keys(
                lat_block, rope_block, key_up, value_up, k_head_gain, key_pos
            )
            results = []
            for query_block, query_pos, state_now in zip(query_sets, position_sets, states):
                step_fn = partial(
                    attend_keys, query_block, query_pos, key_heads, value_heads, key_pos
                )
                results.append(
                    lax.cond(
                        first_key <= query_pos[-1],
                        step_fn,
                        lambda state_kept: state_kept,
                        state_now,
                    )
                )
            return tuple(results)

        return lax.cond(
            first_key <= last_pos, compute, lambda state_kept: state_kept, running_state
        )

    states = lax.fori_loop(0, piece_rows // block_rows, advance, initial)
    lower_attn, lower_log = finish(states[0])
    upper_attn, upper_log = finish(states[1])
    attended = jnp.concatenate([lower_attn, upper_attn], axis=0).reshape(row_count, head_count * VD)
    attended = attended.astype(jnp.bfloat16)
    log_weight = jnp.transpose(jnp.concatenate([lower_log, upper_log], axis=0))
    earlier = shifted(pool_input[row_count - 15 :], "sp", 1)
    extended = jnp.concatenate([earlier, pool_input], axis=0).astype(jnp.float32)
    window = jnp.left_shift(jnp.int32(2), lax.axis_index("fs"))
    window_sum = jnp.zeros((row_count, pool_input.shape[1]), jnp.float32)
    for lag_rows in range(16):
        window_sum = window_sum + jnp.where(
            lag_rows < window, extended[15 - lag_rows : 15 - lag_rows + row_count], 0.0
        )
    counts = jnp.minimum(own_pos + 1, window).astype(jnp.float32)[:, None]
    pool_diff = (window_sum / counts - extended[15:]).astype(jnp.bfloat16)
    pooled = (
        jnp.dot(pool_diff, pool_mix[0], preferred_element_type=jnp.float32) * pool_gain
    ).astype(jnp.bfloat16)
    mixed = lax.psum_scatter(
        (
            jnp.dot(pooled, out_pool, preferred_element_type=jnp.float32)
            + jnp.dot(attended, out_attn, preferred_element_type=jnp.float32)
        ).astype(jnp.bfloat16),
        ("fs", "tp"),
        scatter_dimension=0,
        tiled=True,
    )
    return (mixed, log_weight)


def solution(mesh):
    in_specs = (
        P("sp", None),
        P("sp", None),
        P("sp", None),
        P("sp", "fs"),
        P(),
        P(),
        P(),
        P(),
        P(("fs", "tp")),
        P(None, ("fs", "tp")),
        P(None, ("fs", "tp")),
        P(None, ("fs", "tp")),
        P("fs", None, "tp"),
        P(("fs", "tp"), None),
        P(("fs", "tp"), None),
    )
    out_specs = (P(("sp", "fs", "tp"), None), P(("fs", "tp"), "sp"))
    return jax.shard_map(local, mesh=mesh, in_specs=in_specs, out_specs=out_specs, check_vma=False)
```

profile of v0, /device:TPU:8, one launch (start us, length us, event | category | flops | bytes accessed | tf_op | source)
XLA Modules:
  0.0 687.8 jit_solution(16192583361975005944)
XLA Ops:
  11.3 57.5 %all_to_all.5 = bf16[64,32,320]{2,1,0:T(8,128)(2,1)} all-to-all(bf16[64,32,320]{2,1,0:T(8,128)(2,1)S(1)} %broadcast_in_dim.106), channel_id=1, replica_groups=mesh['sp'=64,'fs'=4,'tp'=2] {'sp'}, dimensions={0} | all-to-all | bytes 2621440 | tf_op jit(solution)/shard_map/all_to_all | solution.py:27
  68.9 2.2 collective-permute-start
  74.6 4.5 fusion.25
  79.2 58.3 %all-gather.2.cloned.1.call-done = bf16[16384,320]{1,0:T(8,128)(2,1)} async-done(((bf16[2048,320]{1,0:T(8,128)(2,1)}), bf16[16384,320]{1,0:T(8,128)(2,1)}) %all-gather.2.cloned.1.call-update) | async-done | bytes 10485776 | tf_op jit(solution)/shard_map/all_gather | solution.py:51
  137.5 3.7 split.9
  141.2 4.8 copy.31
  146.0 7.1 %split.8 = bf16[16384,256]{1,0:T(8,128)(2,1)} slice(bf16[16384,320]{1,0:T(8,128)(2,1)} %all-gather.2.cloned.1.call-done), slice={[0:16384], [0:256]} | slice | bytes 16777216 | tf_op jit(solution)/shard_map/split | solution.py:51
  153.7 155.1 %while.23 = (s32[]{:T(128)}, f32[128,2]{0,1:T(2,128)S(1)}, f32[128,2]{0,1:T(2,128)S(1)}, f32[128,2,128]{2,0,1:T(8,128)S(1)}, f32[128,2]{0,1:T(2,128)S(1)}, /*ind...) while((s32[]{:T(128)}, f32[128,2]{0,1:T(2,128)S(1)}, ...), condition=%wide.region_16.17_spmd, body=%wide.region_3.16_spmd.sunk | while | flops 307153984 | bytes 12259133 | solution.py:221
  155.0 13.7 %conditional.4 = ((f32[128,2]{0,1:T(2,128)S(1)}, f32[128,2]{0,1:T(2,128)S(1)}, f32[128,2,128]{2,0,1:T(8,128)S(1)}, f32[128,2]{0,1:T(2,128)S(1)}, f32[128,2]{0,1:T(2,128)}, /*index=5*/f32[128,2,128]{2,0,1:T(8,128)S(1)})) conditional(s32[]{:T(128)} %convert_element_type.132, (f32[128,2]{0,1:T(2,128)S(1)}, f32[128,2]{0,1:T(2,128)S(1)}, ...), branch_computations={%region_5.5_spmd, %region_6.15_spmd} | conditional | flops 307153472 | bytes 12254580 | solution.py:217
  161.7 2.9 conditional.1
  162.9 1.3 multiply_add_fusion.1
  167.1 1.7 conditional
  174.4 13.7 %conditional.4 = ((f32[128,2]{0,1:T(2,128)S(1)}, f32[128,2]{0,1:T(2,128)S(1)}, f32[128,2,128]{2,0,1:T(8,128)S(1)}, f32[128,2]{0,1:T(2,128)S(1)}, f32[128,2]{0,1:T(2,128)}, /*index=5*/f32[128,2,128]{2,0,1:T(8,128)S(1)})) conditional(s32[]{:T(128)} %convert_element_type.132, (f32[128,2]{0,1:T(2,128)S(1)}, f32[128,2]{0,1:T(2,128)S(1)}, ...), branch_computations={%region_5.5_spmd, %region_6.15_spmd} | conditional | flops 307153472 | bytes 12254580 | solution.py:217
  177.9 1.2 convolution_convert_fusion
  181.1 2.9 conditional.1
  182.3 1.3 multiply_add_fusion.1
  186.4 1.7 conditional
  193.8 13.7 %conditional.4 = ((f32[128,2]{0,1:T(2,128)S(1)}, f32[128,2]{0,1:T(2,128)S(1)}, f32[128,2,128]{2,0,1:T(8,128)S(1)}, f32[128,2]{0,1:T(2,128)S(1)}, f32[128,2]{0,1:T(2,128)}, /*index=5*/f32[128,2,128]{2,0,1:T(8,128)S(1)})) conditional(s32[]{:T(128)} %convert_element_type.132, (f32[128,2]{0,1:T(2,128)S(1)}, f32[128,2]{0,1:T(2,128)S(1)}, ...), branch_computations={%region_5.5_spmd, %region_6.15_spmd} | conditional | flops 307153472 | bytes 12254580 | solution.py:217
  197.3 1.2 convolution_convert_fusion
  200.4 2.9 conditional.1
  201.7 1.3 multiply_add_fusion.1
  205.8 1.7 conditional
  213.2 13.7 %conditional.4 = ((f32[128,2]{0,1:T(2,128)S(1)}, f32[128,2]{0,1:T(2,128)S(1)}, f32[128,2,128]{2,0,1:T(8,128)S(1)}, f32[128,2]{0,1:T(2,128)S(1)}, f32[128,2]{0,1:T(2,128)}, /*index=5*/f32[128,2,128]{2,0,1:T(8,128)S(1)})) conditional(s32[]{:T(128)} %convert_element_type.132, (f32[128,2]{0,1:T(2,128)S(1)}, f32[128,2]{0,1:T(2,128)S(1)}, ...), branch_computations={%region_5.5_spmd, %region_6.15_spmd} | conditional | flops 307153472 | bytes 12254580 | solution.py:217
  216.7 1.2 convolution_convert_fusion
  219.8 2.9 conditional.1
  221.1 1.3 multiply_add_fusion.1
  225.2 1.7 conditional
  232.6 13.7 %conditional.4 = ((f32[128,2]{0,1:T(2,128)S(1)}, f32[128,2]{0,1:T(2,128)S(1)}, f32[128,2,128]{2,0,1:T(8,128)S(1)}, f32[128,2]{0,1:T(2,128)S(1)}, f32[128,2]{0,1:T(2,128)}, /*index=5*/f32[128,2,128]{2,0,1:T(8,128)S(1)})) conditional(s32[]{:T(128)} %convert_element_type.132, (f32[128,2]{0,1:T(2,128)S(1)}, f32[128,2]{0,1:T(2,128)S(1)}, ...), branch_computations={%region_5.5_spmd, %region_6.15_spmd} | conditional | flops 307153472 | bytes 12254580 | solution.py:217
  236.1 1.2 convolution_convert_fusion
  239.2 2.9 conditional.1
  240.5 1.3 multiply_add_fusion.1
  244.6 1.7 conditional
  252.0 13.7 %conditional.4 = ((f32[128,2]{0,1:T(2,128)S(1)}, f32[128,2]{0,1:T(2,128)S(1)}, f32[128,2,128]{2,0,1:T(8,128)S(1)}, f32[128,2]{0,1:T(2,128)S(1)}, f32[128,2]{0,1:T(2,128)}, /*index=5*/f32[128,2,128]{2,0,1:T(8,128)S(1)})) conditional(s32[]{:T(128)} %convert_element_type.132, (f32[128,2]{0,1:T(2,128)S(1)}, f32[128,2]{0,1:T(2,128)S(1)}, ...), branch_computations={%region_5.5_spmd, %region_6.15_spmd} | conditional | flops 307153472 | bytes 12254580 | solution.py:217
  255.5 1.2 convolution_convert_fusion
  258.6 2.9 conditional.1
  259.8 1.3 multiply_add_fusion.1
  264.0 1.7 conditional
  271.3 13.7 %conditional.4 = ((f32[128,2]{0,1:T(2,128)S(1)}, f32[128,2]{0,1:T(2,128)S(1)}, f32[128,2,128]{2,0,1:T(8,128)S(1)}, f32[128,2]{0,1:T(2,128)S(1)}, f32[128,2]{0,1:T(2,128)}, /*index=5*/f32[128,2,128]{2,0,1:T(8,128)S(1)})) conditional(s32[]{:T(128)} %convert_element_type.132, (f32[128,2]{0,1:T(2,128)S(1)}, f32[128,2]{0,1:T(2,128)S(1)}, ...), branch_computations={%region_5.5_spmd, %region_6.15_spmd} | conditional | flops 307153472 | bytes 12254580 | solution.py:217
  278.0 2.9 conditional.1
  279.2 1.3 multiply_add_fusion.1
  283.4 1.7 conditional
  290.7 13.7 %conditional.4 = ((f32[128,2]{0,1:T(2,128)S(1)}, f32[128,2]{0,1:T(2,128)S(1)}, f32[128,2,128]{2,0,1:T(8,128)S(1)}, f32[128,2]{0,1:T(2,128)S(1)}, f32[128,2]{0,1:T(2,128)}, /*index=5*/f32[128,2,128]{2,0,1:T(8,128)S(1)})) conditional(s32[]{:T(128)} %convert_element_type.132, (f32[128,2]{0,1:T(2,128)S(1)}, f32[128,2]{0,1:T(2,128)S(1)}, ...), branch_computations={%region_5.5_spmd, %region_6.15_spmd} | conditional | flops 307153472 | bytes 12254580 | solution.py:217
  294.2 1.2 convolution_convert_fusion
  297.4 2.9 conditional.1
  298.6 1.3 multiply_add_fusion.1
  302.8 1.7 conditional
  309.7 4.3 fusion.23
  315.3 365.7 %reduce-scatter.2.cloned.1.call-done = bf16[32,4096]{1,0:T(8,128)(2,1)} async-done(((bf16[256,4096]{1,0:T(8,128)(2,1)}), bf16[32,4096]{1,0:T(8,128)(2,1)}) %reduce-scatter.2.cloned.1.call-update) | async-done | bytes 262160 | tf_op jit(solution)/shard_map/reduce_scatter | solution.py:240
  (357 shorter events, 103.3 us)
Async XLA Ops:
  7.2 302.5 %copy-start = (bf16[256,4096]{1,0:T(8,128)(2,1)S(1)}, bf16[256,4096]{1,0:T(8,128)(2,1)}, u32[]{:S(2)}) copy-start(bf16[256,4096]{1,0:T(8,128)(2,1)} %param.37) | copy-start | bytes 6291460
  7.2 61.7 %copy-start.5 = (bf16[256,256]{1,0:T(8,128)(2,1)S(1)}, bf16[256,256]{1,0:T(8,128)(2,1)}, u32[]{:S(2)}) copy-start(bf16[256,256]{1,0:T(8,128)(2,1)} %param.26) | copy-start | bytes 393220
  7.2 63.9 %copy-start.3 = (bf16[256,512]{1,0:T(8,128)(2,1)S(1)}, bf16[256,512]{1,0:T(8,128)(2,1)}, u32[]{:S(2)}) copy-start(bf16[256,512]{1,0:T(8,128)(2,1)} %param.23) | copy-start | bytes 786436
  7.2 64.0 %copy-start.7 = (f32[512]{0:T(512)S(1)}, f32[512]{0:T(512)}, u32[]{:S(2)}) copy-start(f32[512]{0:T(512)} %param.27) | copy-start | bytes 6148
  7.2 64.0 %copy-start.4 = (bf16[512,384]{1,0:T(8,128)(2,1)S(1)}, bf16[512,384]{1,0:T(8,128)(2,1)}, u32[]{:S(2)}) copy-start(bf16[512,384]{1,0:T(8,128)(2,1)} %param.32) | copy-start | bytes 1179652
  7.2 130.3 %all-gather.2.cloned.1.call-start = ((), (), s32[]{:S(2)}) async-start(), calls=%async_computation.2 | async-start | bytes 14155776 | tf_op jit(solution)/shard_map/all_gather | solution.py:51
  9.4 62.3 %copy-start.8 = (f32[192]{0:T(256)S(1)}, f32[192]{0:T(256)}, u32[]{:S(2)}) copy-start(f32[192]{0:T(256)} %param.29) | copy-start | bytes 2308
  11.3 63.3 %copy-start.9 = (bf16[1,256,128]{2,1,0:T(8,128)(2,1)S(1)}, bf16[1,256,128]{2,1,0:T(8,128)(2,1)}, u32[]{:S(2)}) copy-start(bf16[1,256,128]{2,1,0:T(8,128)(2,1)} %param.35) | copy-start | bytes 196612
  11.3 63.3 %copy-start.10 = (f32[128]{0:T(128)S(1)}, f32[128]{0:T(128)}, u32[]{:S(2)}) copy-start(f32[128]{0:T(128)} %param.31) | copy-start | bytes 1540
  68.8 612.1 %reduce-scatter.2.cloned.1.call-start = ((), (), s32[]{:S(2)}) async-start(), calls=%async_computation.3 | async-start | bytes 2359296 | tf_op jit(solution)/shard_map/reduce_scatter | solution.py:240
  68.9 5.7 collective-permute-start
  145.9 7.7 %copy-start.1 = (bf16[256,256]{1,0:T(8,128)(2,1)S(1)}, bf16[256,256]{1,0:T(8,128)(2,1)}, u32[]{:S(2)}) copy-start(bf16[256,256]{1,0:T(8,128)(2,1)} %param.33) | copy-start | bytes 393220
  145.9 7.7 %copy-start.2 = (bf16[256,256]{1,0:T(8,128)(2,1)S(1)}, bf16[256,256]{1,0:T(8,128)(2,1)}, u32[]{:S(2)}) copy-start(bf16[256,256]{1,0:T(8,128)(2,1)} %param.34) | copy-start | bytes 393220
  155.1 4.7 copy-start.6
  174.4 4.7 copy-start.6
  193.8 4.7 copy-start.6
  213.2 4.7 copy-start.6
  232.6 4.7 copy-start.6
  252.0 4.7 copy-start.6
  271.4 4.7 copy-start.6
  290.8 4.7 copy-start.6
Sparse Core Ops, SparseCore 0:
  68.9 68.5 all-gather.1
  314.1 366.7 reduce-scatter.1
where the time goes:
time: 695 us; the launch traced here: 688 us
  waiting for transfers between devices  424 us (61%)
  other arithmetic  69.9 us (10%)
  blocking collectives  57.5 us (8%)
  loops' own time  43.9 us (6%)
  matrix products  40.7 us (6%)
  local copies, waits for them, and re-layouts  33.8 us (5%)
  between operations  15.7 us (2%)
    reduce_scatter x1, waiting for transfers between devices, local(): lax.psum_scatter((jnp.dot(pooled, out_pool, preferred_element_type=jnp.fl...  366 us
    all_gather x1, waiting for transfers between devices, sent_together_2(): lax.all_gather(both, axis, axis=dim, tiled=True)  58.3 us
    all_to_all x1, blocking collectives, sent_to_all(): lax.all_to_all(jnp.broadcast_to(shard[None], (length, *shard.shape)), axi...  57.5 us
    reduce_min x32, other arithmetic, advance(): first_key = jnp.min(key_pos)  23.4 us
    another operation x32, loops' own time, advance(): lax.cond(first_key <= last_pos, compute, lambda state_kept: state_kept, r...  21.8 us
    another operation x1, loops' own time, local(): states = lax.fori_loop(0, piece_rows // block_rows, advance, initial)  21.6 us
    slice x16, local copies, waits for them, and re-layouts, compute(): query_pos[-1]  14.7 us
  transfers between devices with their start and end apart: 3, of which 2 were waited for; matrix products, arithmetic and copies ran while one was open for 1% of the time, Pallas kernels for 0%

commit v1 on v0

v1 whole, which is shorter than its diff:
```python
from functools import partial
import math

import jax
import jax.numpy as jnp
from jax import lax
from jax.experimental import pallas as pl
from jax.experimental.pallas import tpu as pltpu
from jax.sharding import PartitionSpec as P

NOPE = 128
ROPE = 64
VD = 128
EPS = 1e-06
THETA = 10000.0
HUGE = 1e30
LOG2E = math.log2(math.e)
LN2 = math.log(2.0)
HALF = 128
NB = 8


def row_norm(values, row_gain):
    mean_sq = jnp.mean(values * values, axis=-1, keepdims=True)
    return values * lax.rsqrt(mean_sq + EPS) * row_gain


def angle_tables(position):
    frequency = 1.0 / THETA ** (jnp.arange(0, ROPE, 2, dtype=jnp.float32) / ROPE)
    angles = position.astype(jnp.float32)[:, None] * frequency[None, :]
    return jnp.cos(angles), jnp.sin(angles)


def rotate(values, position):
    half_width = values.shape[-1] // 2
    cosine_table, sine_table = angle_tables(position)
    cosine_table = cosine_table[:, None, :]
    sine_table = sine_table[:, None, :]
    first_half = values[..., :half_width]
    second_half = values[..., half_width:]
    return jnp.concatenate(
        [
            first_half * cosine_table - second_half * sine_table,
            first_half * sine_table + second_half * cosine_table,
        ],
        axis=-1,
    )


def make_queries(latent, lat_gain, q_up, norm_gain, key_gain, position):
    row_count = latent.shape[0]
    normed = row_norm(latent.astype(jnp.float32), lat_gain).astype(jnp.bfloat16)
    query = jnp.dot(normed, q_up, preferred_element_type=jnp.float32).reshape(
        row_count, -1, NOPE + ROPE
    )
    query = row_norm(query, norm_gain)
    scale = LOG2E * (NOPE + ROPE) ** (-0.5)
    query = jnp.concatenate(
        [
            query[..., :NOPE] * (key_gain[:NOPE] * scale),
            rotate(query[..., NOPE:], position) * scale,
            jnp.zeros((*query.shape[:2], 256 - NOPE - ROPE), jnp.float32),
        ],
        axis=-1,
    )
    return jnp.transpose(query.astype(jnp.bfloat16), (1, 0, 2))


def attend_kernel(
    first,
    final,
    where_ref,
    keys_ref,
    q_ref,
    key_up_ref,
    value_up_ref,
    gain_ref,
    block_cos_ref,
    block_sin_ref,
    in_cos_ref,
    in_sin_ref,
    *refs,
):
    if first:
        state_in, refs = None, refs
    else:
        state_in, refs = refs[:3], refs[3:]
    if final:
        out_ref, log_ref, max_ref, sum_ref, acc_ref, key_ref = refs
    else:
        max_ref, sum_ref, acc_ref, key_ref = refs
    heads, rows, _ = q_ref.shape
    step = pl.program_id(0)
    own_block, half_offset = where_ref[0], where_ref[1]
    diagonal = own_block // NB
    width = NB * HALF

    @pl.when(step == 0)
    def _():
        if first:
            max_ref[...] = jnp.full(max_ref.shape, -HUGE, jnp.float32)
            sum_ref[...] = jnp.zeros_like(sum_ref)
            acc_ref[...] = jnp.zeros_like(acc_ref)
        else:
            max_ref[...] = state_in[0][...]
            sum_ref[...] = state_in[1][...]
            acc_ref[...] = state_in[2][...]
        key_ref[:, NOPE + ROPE :, :] = jnp.zeros(
            (heads, 256 - NOPE - ROPE, width), key_ref.dtype
        )

    def build_keys():
        for n in range(NB):
            at = pl.ds(n * HALF, HALF)
            raw = jnp.dot(
                key_up_ref[...], keys_ref[n, :256, :], preferred_element_type=jnp.float32
            )
            rope = keys_ref[n, 256:, :].astype(jnp.float32)
            rope_sq = jnp.sum(rope * rope, axis=0, keepdims=True)
            rope = rope * gain_ref[...]
            block_cos, block_sin = block_cos_ref[n], block_sin_ref[n]
            in_cos, in_sin = in_cos_ref[...], in_sin_ref[...]
            cosine = block_cos * in_cos - block_sin * in_sin
            sine = block_sin * in_cos + block_cos * in_sin
            a, b = rope[: ROPE // 2], rope[ROPE // 2 :]
            turned = jnp.concatenate([a * cosine - b * sine, a * sine + b * cosine], axis=0)
            for h in range(heads):
                part = raw[h * NOPE : (h + 1) * NOPE]
                square = jnp.sum(part * part, axis=0, keepdims=True) + rope_sq
                inverse = lax.rsqrt(square * (1.0 / (NOPE + ROPE)) + EPS)
                key_ref[h, :NOPE, at] = (part * inverse).astype(key_ref.dtype)
                key_ref[h, NOPE : NOPE + ROPE, at] = (turned * inverse).astype(key_ref.dtype)

    def attend(masked):
        build_keys()
        latent = jnp.concatenate([keys_ref[n, :256, :] for n in range(NB)], axis=1)
        for h in range(heads):
            scores = jnp.dot(q_ref[h], key_ref[h], preferred_element_type=jnp.float32)
            if masked:
                column = lax.broadcasted_iota(jnp.int32, (rows, width), 1)
                row = lax.broadcasted_iota(jnp.int32, (rows, width), 0)
                key_pos = (
                    (step * NB + column // HALF) * rows + half_offset + column % HALF
                )
                scores = jnp.where(key_pos <= own_block * rows + row, scores, -HUGE)
            before = max_ref[h]
            after = jnp.maximum(before, jnp.max(scores, axis=1, keepdims=True))
            factor = jnp.exp2(before - after)
            weights = jnp.exp2(scores - after[:, :1])
            partial_sum = weights[:, :128]
            for n in range(1, width // 128):
                partial_sum = partial_sum + weights[:, n * 128 : (n + 1) * 128]
            max_ref[h] = after
            sum_ref[h] = sum_ref[h] * factor + partial_sum
            update = lax.dot_general(
                weights.astype(jnp.bfloat16),
                latent,
                (((1,), (1,)), ((), ())),
                preferred_element_type=jnp.float32,
            )
            acc_ref[h] = acc_ref[h] * factor[:, :1] + update

    pl.when(step < diagonal)(lambda: attend(False))
    pl.when(step == diagonal)(lambda: attend(True))

    if final:

        @pl.when(step == pl.num_programs(0) - 1)
        def _():
            for h in range(heads):
                total = jnp.sum(sum_ref[h], axis=1, keepdims=True)
                mean = acc_ref[h] / total
                high = mean.astype(jnp.bfloat16)
                low = (mean - high.astype(jnp.float32)).astype(jnp.bfloat16)
                value = value_up_ref[:, h * VD : (h + 1) * VD]
                out_ref[:, h * VD : (h + 1) * VD] = (
                    jnp.dot(high, value, preferred_element_type=jnp.float32)
                    + jnp.dot(low, value, preferred_element_type=jnp.float32)
                ).astype(out_ref.dtype)
                log_ref[h] = (max_ref[h] + jnp.log2(total)) * LN2


def attend_part(
    keys, own_block, half_offset, queries, key_up, value_up, gain, block_tables, in_tables, state, final
):
    block_count = keys.shape[0]
    heads, rows, _ = queries.shape
    first = state is None
    place = jnp.stack([own_block, half_offset]).astype(jnp.int32)

    def whole(*shape):
        return pl.BlockSpec(shape, lambda i, w: (0,) * len(shape))

    def tile(*shape):
        return pl.BlockSpec(
            shape, lambda i, w: (jnp.minimum(i, w[0] // NB),) + (0,) * (len(shape) - 1)
        )

    state_shapes = [(heads, rows, 128), (heads, rows, 128), (heads, rows, 256)]
    in_specs = [
        tile(NB, 320, HALF),
        whole(heads, rows, 256),
        whole(*key_up.shape),
        whole(*value_up.shape),
        whole(ROPE, 1),
        tile(NB, ROPE // 2, 1),
        tile(NB, ROPE // 2, 1),
        whole(ROPE // 2, HALF),
        whole(ROPE // 2, HALF),
    ]
    operands = [keys, queries, key_up, value_up, gain, *block_tables, *in_tables]
    if not first:
        in_specs += [whole(*s) for s in state_shapes]
        operands += list(state)
    key_scratch = pltpu.VMEM((heads, 256, NB * HALF), jnp.bfloat16)
    if final:
        out_shape = [
            jax.ShapeDtypeStruct((rows, heads * VD), jnp.bfloat16),
            jax.ShapeDtypeStruct((heads, rows, 128), jnp.float32),
        ]
        out_specs = [whole(rows, heads * VD), whole(heads, rows, 128)]
        scratch = [pltpu.VMEM(s, jnp.float32) for s in state_shapes] + [key_scratch]
    else:
        out_shape = [jax.ShapeDtypeStruct(s, jnp.float32) for s in state_shapes]
        out_specs = [whole(*s) for s in state_shapes]
        scratch = [key_scratch]
    flops = 2 * block_count * HALF * heads * rows * 512
    return pl.pallas_call(
        partial(attend_kernel, first, final),
        out_shape=out_shape,
        grid_spec=pltpu.PrefetchScalarGridSpec(
            num_scalar_prefetch=1,
            grid=(block_count // NB,),
            in_specs=in_specs,
            out_specs=out_specs,
            scratch_shapes=scratch,
        ),
        compiler_params=pltpu.CompilerParams(
            dimension_semantics=("arbitrary",), vmem_limit_bytes=60 * 2**20
        ),
        cost_estimate=pl.CostEstimate(
            flops=flops,
            bytes_accessed=keys.size * 2,
            transcendentals=block_count * HALF * heads * rows,
        ),
        name="attend_last" if final else "attend_first",
    )(place, *operands)


def local(
    q_latent,
    kv_latent,
    key_rope,
    pool_input,
    q_lat_gain,
    kv_lat_gain,
    q_head_gain,
    k_head_gain,
    pool_gain,
    q_up,
    key_up,
    value_up,
    pool_mix,
    out_pool,
    out_attn,
):
    row_count = q_latent.shape[0]
    sp_index = lax.axis_index("sp")
    sp_size = lax.axis_size("sp")
    core = lax.axis_index("tp")
    own_pos = sp_index * row_count + jnp.arange(row_count, dtype=jnp.int32)

    share = lax.dynamic_slice_in_dim(kv_latent, core * HALF, HALF, 0)
    share_rope = lax.dynamic_slice_in_dim(key_rope, core * HALF, HALF, 0)
    share = row_norm(share.astype(jnp.float32), kv_lat_gain).astype(jnp.bfloat16)
    share = jnp.concatenate([share.T, share_rope.T], axis=0)
    mine = lax.all_gather(share, "sp", axis=0)
    other = lax.ppermute(mine, "tp", [(0, 1), (1, 0)])

    queries = make_queries(q_latent, q_lat_gain, q_up, q_head_gain, k_head_gain, own_pos)
    head_count = queries.shape[0]
    gain = k_head_gain[NOPE:, None]
    block_tables = [
        t[:, :, None] for t in angle_tables(jnp.arange(sp_size, dtype=jnp.int32) * row_count)
    ]
    offset = core * HALF
    near = [
        t.T for t in angle_tables(offset + jnp.arange(HALF, dtype=jnp.int32))
    ]
    far = [
        t.T for t in angle_tables(HALF - offset + jnp.arange(HALF, dtype=jnp.int32))
    ]
    common = (queries, key_up.T, value_up, gain, block_tables)
    state = attend_part(mine, sp_index, offset, *common, near, None, False)
    attended, log_wide = attend_part(other, sp_index, HALF - offset, *common, far, state, True)
    log_weight = log_wide[:, :, 0]

    earlier = lax.ppermute(
        pool_input[row_count - 15 :], "sp", [(i, i + 1) for i in range(sp_size - 1)]
    )
    extended = jnp.concatenate([earlier, pool_input], axis=0).astype(jnp.float32)
    window = jnp.left_shift(jnp.int32(2), lax.axis_index("fs"))
    window_sum = jnp.zeros((row_count, pool_input.shape[1]), jnp.float32)
    for lag_rows in range(16):
        window_sum = window_sum + jnp.where(
            lag_rows < window, extended[15 - lag_rows : 15 - lag_rows + row_count], 0.0
        )
    counts = jnp.minimum(own_pos + 1, window).astype(jnp.float32)[:, None]
    pool_diff = (window_sum / counts - extended[15:]).astype(jnp.bfloat16)
    pooled = (
        jnp.dot(pool_diff, pool_mix[0], preferred_element_type=jnp.float32) * pool_gain
    ).astype(jnp.bfloat16)
    mixed = lax.psum_scatter(
        (
            jnp.dot(pooled, out_pool, preferred_element_type=jnp.float32)
            + jnp.dot(attended, out_attn, preferred_element_type=jnp.float32)
        ).astype(jnp.bfloat16),
        ("fs", "tp"),
        scatter_dimension=0,
        tiled=True,
    )
    return (mixed, log_weight)


def solution(mesh):
    in_specs = (
        P("sp", None),
        P("sp", None),
        P("sp", None),
        P("sp", "fs"),
        P(),
        P(),
        P(),
        P(),
        P(("fs", "tp")),
        P(None, ("fs", "tp")),
        P(None, ("fs", "tp")),
        P(None, ("fs", "tp")),
        P("fs", None, "tp"),
        P(("fs", "tp"), None),
        P(("fs", "tp"), None),
    )
    out_specs = (P(("sp", "fs", "tp"), None), P(("fs", "tp"), "sp"))
    return jax.shard_map(local, mesh=mesh, in_specs=in_specs, out_specs=out_specs, check_vma=False)
```

time: 695 us -> 209 us (0.30)
  waiting for transfers between devices: 424 us -> 150 us
  other arithmetic: 69.9 us -> 11.9 us
  blocking collectives: 57.5 us -> 0 us
  loops' own time: 43.9 us -> 0 us
  matrix products: 40.7 us -> 10.5 us
  local copies, waits for them, and re-layouts: 33.8 us -> 5.03 us
  Pallas kernels: 0 us -> 11.4 us
    reduce_scatter x1, waiting for transfers between devices: 366 us -> 56.2 us  [local(): lax.psum_scatter((jnp.dot(pooled, out_pool, preferred_element_type=jnp.fl...]
    all_to_all x1 -> x0, blocking collectives: 57.5 us -> none  [sent_to_all(): lax.all_to_all(jnp.broadcast_to(shard[None], (length, *shard.shape)), axi...]
    another operation x49 -> x0, loops' own time: 43.9 us -> none  [the longest x32 21.8 us: advance(): lax.cond(first_key <= last_pos, compute, lambda state_kept: state_kept, r...]
    all_gather x1, waiting for transfers between devices: 58.3 us -> 93.4 us  [local(): mine = lax.all_gather(share, 'sp', axis=0)]
    dot_general x48 -> x0, matrix products: 31.6 us -> none  [the longest x8 9.77 us: make_keys(): jnp.dot(latent, value_up, preferred_element_type=jnp.float32)]
    reduce_min x32 -> x0, other arithmetic: 23.4 us -> none  [advance(): first_key = jnp.min(key_pos)]
    slice x29 -> x2, local copies, waits for them, and re-layouts: 16.1 us -> 1.43 us  [the longest x1 0.73 us: local(): log_weight = log_wide[:, :, 0]]
    le x16 -> x0, other arithmetic: 11.6 us -> none  [attend_keys(): allowed = key_pos[None, None, :] <= query_pos[:, None, None]]
  transfers between devices with their start and end apart: 3 -> 4, of which waited for: 2 -> 2; matrix products, arithmetic and copies ran while one was open for 1% -> 9% of each run, Pallas kernels for 0% -> 3%
where the time goes in v1:
time: 209 us; the launch traced here: 208 us
  waiting for transfers between devices  150 us (72%)
  between operations  14.3 us (7%)
  other arithmetic  11.9 us (6%)
  Pallas kernels  11.4 us (5%)
  matrix products  10.5 us (5%)
  starting transfers between devices  5.48 us (3%)
  local copies, waits for them, and re-layouts  5.03 us (2%)
    all_gather x1, waiting for transfers between devices, local(): mine = lax.all_gather(share, 'sp', axis=0)  93.4 us
    reduce_scatter x1, waiting for transfers between devices, local(): lax.psum_scatter((jnp.dot(pooled, out_pool, preferred_element_type=jnp.fl...  56.2 us
    pallas_call x2, Pallas kernels, attend_part(): pl.pallas_call(partial(attend_kernel, first, final), out_shape=out_shape,...  11.4 us
    sin x2, other arithmetic, angle_tables(): return (jnp.cos(angles), jnp.sin(angles))  5.61 us
    dot_general x1, matrix products, local(): jnp.dot(pooled, out_pool, preferred_element_type=jnp.float32)  4.62 us
    dot_general x1, matrix products, local(): jnp.dot(attended, out_attn, preferred_element_type=jnp.float32)  4.37 us
  transfers between devices with their start and end apart: 4, of which 2 were waited for; matrix products, arithmetic and copies ran while one was open for 9% of the time, Pallas kernels for 3%

profile of v1, /device:TPU:8, one launch (start us, length us, event | category | flops | bytes accessed | tf_op | source)
XLA Modules:
  0.0 208.4 jit_solution(1418108690457370609)
XLA Ops:
  7.2 0.0 copy-start
  7.2 0.0 copy-start.5
  7.2 0.0 all-gather.3.cloned.1.call-start
  7.2 1.0 constant_dynamic-slice_fusion
  8.2 0.1 copy.43
  8.3 0.1 fusion.30
  8.4 0.7 dynamic-slice_bitcast_fusion
  9.1 0.8 fusion.71
  9.9 0.6 pad_maximum_fusion
  10.6 0.0 all-gather.3.cloned.1.call-update
  10.6 0.0 reduce-scatter.2.cloned.1.call-start
  10.6 93.4 %all-gather.3.cloned.1.call-done = bf16[20480,128]{1,0:T(8,128)(2,1)} async-done(((bf16[320,128]{1,0:T(8,128)(2,1)}), bf16[20480,128]{1,0:T(8,128)(2,1)}) %all-gather.3.cloned.1.call-update) | async-done | bytes 5242896 | tf_op jit(solution)/shard_map/all_gather | solution.py:277
  104.1 1.9 collective-permute-start.1
  106.0 0.7 slice.73
  106.7 3.5 %collective-permute-start = (bf16[15,256]{1,0:T(8,128)(2,1)S(1)}, bf16[15,256]{1,0:T(8,128)(2,1)S(1)}, u32[]{:S(2)}, u32[]{:S(2)}) collective-permute-start(bf16[15,256]{1,0:T(8,128)(2,1)S(1)} %slice.73), channel_id=1, source_target_pairs={{0,8},{8,16},{16,24},{24,32},{32,40},{40,48},{48,56},{56,64},{64,7... | collective-permute-start | bytes 23048 | tf_op jit(solution)/shard_map/ppermute | solution.py:298
  110.2 1.1 fusion.3
  111.3 0.0 copy-start.3
  111.3 1.5 fusion.6
  112.8 0.0 copy-start.2
  112.8 0.0 copy-start.4
  112.8 0.0 copy-start.6
  112.9 0.2 copy.37
  113.1 0.1 pad.4.clone
  113.2 0.6 pad_add_fusion.1.where_ref
  113.8 0.5 multiply_cosine_fusion.1
  114.3 0.8 multiply_multiply_fusion
  115.2 0.2 multiply_subtract_fusion
  115.3 0.1 fusion.26
  115.5 0.0 copy-done.5
  115.5 0.8 multiply_sine_fusion.2
  116.3 0.8 maximum_bitcast_fusion.q_ref
  117.1 4.8 %multiply_sine_fusion = (f32[64,32,1]{2,1,0:T(8,128)}, f32[64,32,1]{2,1,0:T(8,128)}) fusion(f32[64]{0:T(128)S(1)} %multiply_convert_fusion, f32[32]{0:T(128)S(1)} %negate_power_fusion), kind=kLoop, calls=%fused_computation.2 | loop fusion | flops 2048 | bytes 16768 | tf_op jit(solution)/shard_map/sin | solution.py:31
  121.9 0.6 pad_add_fusion.where_ref
  122.6 0.0 copy-done.3
  122.6 0.8 copy.38
  123.3 0.7 copy.41.gain_ref
  124.0 0.0 collective-permute-done
  124.1 0.0 copy-done.4
  124.1 0.0 copy-done.6
  124.1 4.6 %fusion.2 = f32[256,4096]{1,0:T(8,128)} fusion(bf16[128,4096]{1,0:T(8,128)(2,1)} %param.28, f32[271,256]{1,0:T(8,128)S(1)} %maximum_convert_fusion, f32[256]{0:T(256)S(1)} %minimum_convert_fusion, pred[]{:T(512)S(6)} %gt.63, pred[]{:T(512)S(6)} %gt.62, pred[]{:T(512)S(6)} %gt.61, pred[]{:T(512)S(6)} %gt.60, pred[]{:T(512)S(6)} %gt.59, pred[]{:T(512)S(6)} %gt.58, ...), kind=kOutput, calls=%fused_computation.6 | convolution fusion | flops 287506432 | bytes 9504272 | tf_op jit(solution)/shard_map/dot_general | solution.py:315
  128.7 5.4 %attend_first.1 = (f32[2,256,128]{2,1,0:T(8,128)}, f32[2,256,128]{2,1,0:T(8,128)}, f32[2,256,256]{2,1,0:T(8,128)}) custom-call(s32[2]{0:T(128)} %pad_add_fusion.1.where_ref, bf16[64,320,128]{2,1,0:T(8,128)(2,1)} %bitcast.27, bf16[2,256,256]{2,1,0:T(8,128)(2,1)} %maximum_bitcast_fusion.q_ref, bf16[256,256]{1,0:T(8,128)(2,1)} %bitcast.24, ...), custom_call_target="tpu_custom_call" | custom-call | flops 4294967296 | bytes 5242880 | tf_op jit(solution)/shard_map/attend_first/pallas_call | solution.py:228
  134.1 0.0 collective-permute-done.1.keys_ref
  134.1 6.0 %attend_last.1 = (bf16[256,256]{1,0:T(8,128)(2,1)}, f32[2,256,128]{2,1,0:T(8,128)}) custom-call(s32[2]{0:T(128)} %pad_add_fusion.where_ref, bf16[64,320,128]{2,1,0:T(8,128)(2,1)} %collective-permute-done.1.keys_ref, bf16[2,256,256]{2,1,0:T(8,128)(2,1)} %maximum_bitcast_fusion.q_ref, bf16[256,256]{1,0:T(8,128)(2,1)} %bitcast.25, ...), custom_call_target="tpu_custom_call" | custom-call | flops 4294967296 | bytes 5242880 | tf_op jit(solution)/shard_map/attend_last/pallas_call | solution.py:228
  140.1 0.0 copy-done
  140.2 4.4 %fusion = bf16[256,4096]{1,0:T(8,128)(2,1)} fusion(f32[256,4096]{1,0:T(8,128)} %fusion.2, bf16[256,256]{1,0:T(8,128)(2,1)} %get-tuple-element.10, bf16[256,4096]{1,0:T(8,128)(2,1)S(1)} %copy-done), kind=kOutput, calls=%fused_computation.1 | convolution fusion | flops 538968064 | bytes 8519680 | tf_op jit(solution)/shard_map/dot_general | solution.py:316
  144.5 0.0 reduce-scatter.2.cloned.1.call-update
  144.6 0.7 slice_reduce_fusion
  145.3 56.2 %reduce-scatter.2.cloned.1.call-done = bf16[32,4096]{1,0:T(8,128)(2,1)} async-done(((bf16[256,4096]{1,0:T(8,128)(2,1)}), bf16[32,4096]{1,0:T(8,128)(2,1)}) %reduce-scatter.2.cloned.1.call-update) | async-done | bytes 262160 | tf_op jit(solution)/shard_map/reduce_scatter | solution.py:313
  (17 shorter events, 0.2 us)
Async XLA Ops:
  7.2 133.0 %copy-start = (bf16[256,4096]{1,0:T(8,128)(2,1)S(1)}, bf16[256,4096]{1,0:T(8,128)(2,1)}, u32[]{:S(2)}) copy-start(bf16[256,4096]{1,0:T(8,128)(2,1)} %param.29) | copy-start | bytes 6291460
  7.2 108.3 %copy-start.5 = (f32[192]{0:T(256)S(1)}, f32[192]{0:T(256)}, u32[]{:S(2)}) copy-start(f32[192]{0:T(256)} %param.22) | copy-start | bytes 2308
  7.2 96.9 %all-gather.3.cloned.1.call-start = ((), (), s32[]{:S(2)}) async-start(), calls=%async_computation.2 | async-start | bytes 5324800 | tf_op jit(solution)/shard_map/all_gather | solution.py:277
  10.6 190.9 %reduce-scatter.2.cloned.1.call-start = ((), (), s32[]{:S(2)}) async-start(), calls=%async_computation.1 | async-start | bytes 2359296 | tf_op jit(solution)/shard_map/reduce_scatter | solution.py:313
  104.1 30.1 %collective-permute-start.1 = (bf16[64,320,128]{2,1,0:T(8,128)(2,1)}, bf16[64,320,128]{2,1,0:T(8,128)(2,1)}, u32[]{:S(2)}, u32[]{:S(2)}) collective-permute-start(bf16[64,320,128]{2,1,0:T(8,128)(2,1)} %bitcast.26), channel_id=1, source_target_pairs={{0,1},{1,0},{2,3},{3,2},{4,5},{5,4},{6,7},{7,6},{8,9},{9,8},{10,11... | collective-permute-start | bytes 15728648 | tf_op jit(solution)/shard_map/ppermute | solution.py:278
  106.7 17.3 %collective-permute-start = (bf16[15,256]{1,0:T(8,128)(2,1)S(1)}, bf16[15,256]{1,0:T(8,128)(2,1)S(1)}, u32[]{:S(2)}, u32[]{:S(2)}) collective-permute-start(bf16[15,256]{1,0:T(8,128)(2,1)S(1)} %slice.73), channel_id=1, source_target_pairs={{0,8},{8,16},{16,24},{24,32},{32,40},{40,48},{48,56},{56,64},{64,7... | collective-permute-start | bytes 23048 | tf_op jit(solution)/shard_map/ppermute | solution.py:298
  111.3 11.3 %copy-start.3 = (bf16[256,256]{1,0:T(8,128)(2,1)S(1)}, bf16[256,256]{1,0:T(8,128)(2,1)}, u32[]{:S(2)}) copy-start(bf16[256,256]{1,0:T(8,128)(2,1)} %param.25) | copy-start | bytes 393220
  112.8 11.2 %copy-start.2 = (bf16[256,256]{1,0:T(8,128)(2,1)S(1)}, bf16[256,256]{1,0:T(8,128)(2,1)}, u32[]{:S(2)}) copy-start(bf16[256,256]{1,0:T(8,128)(2,1)} %param.18) | copy-start | bytes 393220
  112.8 11.2 %copy-start.4 = (bf16[1,256,128]{2,1,0:T(8,128)(2,1)S(1)}, bf16[1,256,128]{2,1,0:T(8,128)(2,1)}, u32[]{:S(2)}) copy-start(bf16[1,256,128]{2,1,0:T(8,128)(2,1)} %param.27) | copy-start | bytes 196612
  112.8 11.2 %copy-start.6 = (f32[128]{0:T(128)S(1)}, f32[128]{0:T(128)}, u32[]{:S(2)}) copy-start(f32[128]{0:T(128)} %param.23) | copy-start | bytes 1540
  140.1 4.4 %copy-start.1 = (f32[2,256,128]{2,1,0:T(8,128)S(1)}, f32[2,256,128]{2,1,0:T(8,128)}, u32[]{:S(2)}) copy-start(f32[2,256,128]{2,1,0:T(8,128)} %get-tuple-element.11) | copy-start | bytes 786436
Sparse Core Ops, SparseCore 0:
  11.6 92.4 all-gather.2
  144.7 56.7 reduce-scatter.1

commit v2 on v1

v2 whole, which is shorter than its diff:
```python
import math

import jax
import jax.numpy as jnp
import numpy as np
from jax import lax
from jax.experimental import pallas as pl
from jax.experimental.pallas import tpu as pltpu
from jax.sharding import PartitionSpec as P

NOPE = 128
ROPE = 64
VD = 128
EPS = 1e-06
THETA = 10000.0
HUGE = 1e30
LOG2E = math.log2(math.e)
LN2 = math.log(2.0)
HALF = 128
Y = 8
PLANES = 8
MEMBERS = 4
EXTRA = 16


def turn_tables(block_rows, blocks):
    frequency = 1.0 / THETA ** (np.arange(0, ROPE, 2, dtype=np.float64) / ROPE)
    at_block = (np.arange(blocks) * block_rows)[:, None] * frequency
    within = np.arange(block_rows)[:, None] * frequency
    return [t.astype(np.float32) for a in (at_block, within) for t in (np.cos(a), np.sin(a))]


def row_norm(values, row_gain):
    mean_sq = jnp.mean(values * values, axis=-1, keepdims=True)
    return values * lax.rsqrt(mean_sq + EPS) * row_gain


def make_queries(latent, lat_gain, q_up, norm_gain, key_gain, cosine, sine):
    row_count = latent.shape[0]
    normed = row_norm(latent.astype(jnp.float32), lat_gain).astype(jnp.bfloat16)
    query = jnp.dot(normed, q_up, preferred_element_type=jnp.float32).reshape(
        row_count, -1, NOPE + ROPE
    )
    query = row_norm(query, norm_gain)
    scale = LOG2E * (NOPE + ROPE) ** (-0.5)
    cosine, sine = cosine[:, None, :] * scale, sine[:, None, :] * scale
    a, b = query[..., NOPE : NOPE + ROPE // 2], query[..., NOPE + ROPE // 2 :]
    turned = jnp.concatenate([a * cosine - b * sine, a * sine + b * cosine], axis=-1)
    return jnp.concatenate(
        [
            (query[..., :NOPE] * (key_gain[:NOPE] * scale)).reshape(row_count, -1),
            turned.reshape(row_count, -1),
        ],
        axis=-1,
    ).astype(jnp.bfloat16)


def attend_kernel(
    place_ref,
    mine_ref,
    other_ref,
    q_ref,
    key_up_ref,
    value_up_ref,
    gain_ref,
    block_cos_ref,
    block_sin_ref,
    near_ref,
    far_ref,
    out_ref,
    max_ref,
    sum_ref,
    acc_ref,
    key_ref,
    lat_ref,
):
    heads = key_up_ref.shape[0] // NOPE
    count, rows, _ = q_ref.shape
    step = pl.program_id(0)
    plane, parity, own_y, offset = place_ref[step], place_ref[2], place_ref[3], place_ref[4]
    width = Y * rows

    @pl.when(step == 0)
    def _():
        max_ref[...] = jnp.full(max_ref.shape, -HUGE, jnp.float32)
        sum_ref[...] = jnp.zeros_like(sum_ref)
        acc_ref[...] = jnp.zeros_like(acc_ref)
        key_ref[:, NOPE:, :] = jnp.zeros((heads, 256 - NOPE, width), key_ref.dtype)

    def build_keys():
        @pl.loop(0, Y)
        def _(n):
            for u, (keys_ref, in_ref) in enumerate(((mine_ref, near_ref), (other_ref, far_ref))):
                in_cos, in_sin = in_ref[0], in_ref[1]
                at = pl.ds(pl.multiple_of((u * Y + n) * HALF, HALF), HALF)
                parts = [keys_ref[x, n] for x in range(4)]
                latent = jnp.concatenate([*parts[:3], parts[3][:16]], axis=0)
                lat_ref[:, at] = latent
                raw = jnp.dot(key_up_ref[...], latent, preferred_element_type=jnp.float32)
                rope = parts[3][16:].astype(jnp.float32)
                rope_sq = jnp.sum(rope * rope, axis=0, keepdims=True)
                rope = rope * gain_ref[...]
                block_cos, block_sin = block_cos_ref[n], block_sin_ref[n]
                cosine = block_cos * in_cos - block_sin * in_sin
                sine = block_sin * in_cos + block_cos * in_sin
                a, b = rope[: ROPE // 2], rope[ROPE // 2 :]
                turned = jnp.concatenate([a * cosine - b * sine, a * sine + b * cosine], axis=0)
                for h in range(heads):
                    part = raw[h * NOPE : (h + 1) * NOPE]
                    square = jnp.sum(part * part, axis=0, keepdims=True) + rope_sq
                    inverse = lax.rsqrt(square * (1.0 / (NOPE + ROPE)) + EPS)
                    key_ref[h, :NOPE, at] = (part * inverse).astype(key_ref.dtype)
                    key_ref[h, NOPE + h * ROPE : NOPE + (h + 1) * ROPE, at] = (
                        turned * inverse
                    ).astype(key_ref.dtype)

    def attend(i, h, masked):
        query = jnp.concatenate(
            [q_ref[i, :, pl.ds(pl.multiple_of(h * NOPE, NOPE), NOPE)], q_ref[i, :, heads * NOPE :]], axis=1
        )
        scores = jnp.dot(query, key_ref[h], preferred_element_type=jnp.float32)
        if masked:
            column = lax.broadcasted_iota(jnp.int32, (rows, width), 1)
            row = lax.broadcasted_iota(jnp.int32, (rows, width), 0)
            half_at = jnp.where(column < Y * HALF, offset, HALF - offset)
            key_at = (column % (Y * HALF)) // HALF * rows + half_at + column % HALF
            scores = jnp.where(key_at <= own_y * rows + row, scores, -HUGE)
        at = i * heads + h
        before = max_ref[at]
        after = jnp.maximum(before, jnp.max(scores, axis=1, keepdims=True))
        factor = jnp.exp2(before - after)
        weights = jnp.exp2(scores - after[:, :1])
        partial_sum = weights[:, :128]
        for n in range(1, width // 128):
            partial_sum = partial_sum + weights[:, n * 128 : (n + 1) * 128]
        max_ref[at] = after
        sum_ref[at] = sum_ref[at] * factor + partial_sum
        update = lax.dot_general(
            weights.astype(jnp.bfloat16),
            lat_ref[...],
            (((1,), (1,)), ((), ())),
            preferred_element_type=jnp.float32,
        )
        acc_ref[at] = acc_ref[at] * factor[:, :1] + update

    @pl.when(plane <= parity + 2 * (count - 1))
    def _():
        build_keys()

        @pl.loop(0, count * heads)
        def _(at):
            i, h = at // heads, at % heads
            query_plane = parity + 2 * i
            pl.when(plane < query_plane)(lambda: attend(i, h, False))
            pl.when(plane == query_plane)(lambda: attend(i, h, True))

    @pl.when(step == pl.num_programs(0) - 1)
    def _():
        @pl.loop(0, count)
        def _(i):
            out_ref[i, rows:, :] = jnp.zeros((EXTRA, heads * VD), out_ref.dtype)
            for h in range(heads):
                at = i * heads + h
                total = jnp.sum(sum_ref[at], axis=1, keepdims=True)
                seen = total > 0.0
                total = jnp.where(seen, total, 1.0)
                mean = acc_ref[at] / total
                high = mean.astype(jnp.bfloat16)
                low = (mean - high.astype(jnp.float32)).astype(jnp.bfloat16)
                value = value_up_ref[:, h * VD : (h + 1) * VD]
                out_ref[i, :rows, h * VD : (h + 1) * VD] = (
                    jnp.dot(high, value, preferred_element_type=jnp.float32)
                    + jnp.dot(low, value, preferred_element_type=jnp.float32)
                ).astype(out_ref.dtype)
                level = jnp.where(seen, max_ref[at] + jnp.log2(total), -HUGE).T[:1]
                for term in range(3):
                    rounded = level.astype(jnp.bfloat16)
                    out_ref[i, pl.ds(rows + h * 3 + term, 1), :] = rounded
                    level = level - rounded.astype(jnp.float32)


def attend(place, mine, other, queries, key_up, value_up, gain, block_tables, near, far):
    count, rows, _ = queries.shape
    heads = key_up.shape[0] // NOPE

    def whole(*shape):
        return pl.BlockSpec(shape, lambda i, w: (0,) * len(shape))

    keys = pl.BlockSpec((4, Y, 80, HALF), lambda i, w: (0, i, 0, 0))
    table = pl.BlockSpec((Y, ROPE // 2, 1), lambda i, w: (w[i], 0, 0))
    return pl.pallas_call(
        attend_kernel,
        out_shape=jax.ShapeDtypeStruct((count, rows + EXTRA, heads * VD), jnp.bfloat16),
        grid_spec=pltpu.PrefetchScalarGridSpec(
            num_scalar_prefetch=1,
            grid=(2,),
            in_specs=[
                keys,
                keys,
                whole(*queries.shape),
                whole(*key_up.shape),
                whole(*value_up.shape),
                whole(ROPE, 1),
                table,
                table,
                whole(*near.shape),
                whole(*far.shape),
            ],
            out_specs=whole(count, rows + EXTRA, heads * VD),
            scratch_shapes=[
                pltpu.VMEM((count * heads, rows, 128), jnp.float32),
                pltpu.VMEM((count * heads, rows, 128), jnp.float32),
                pltpu.VMEM((count * heads, rows, 256), jnp.float32),
                pltpu.VMEM((heads, 256, Y * rows), jnp.bfloat16),
                pltpu.VMEM((256, Y * rows), jnp.bfloat16),
            ],
        ),
        compiler_params=pltpu.CompilerParams(
            dimension_semantics=("arbitrary",), vmem_limit_bytes=60 * 2**20
        ),
        cost_estimate=pl.CostEstimate(
            flops=5 * 2 * rows * Y * rows * heads * 512,
            bytes_accessed=mine.size * 4,
            transcendentals=5 * rows * Y * rows * heads,
        ),
        name="attend",
    )(place, mine, other, queries, key_up, value_up, gain, *block_tables, near, far)


def to_all(value, axis, groups=None):
    count = len(groups[0]) if groups else lax.axis_size(axis)
    return lax.all_to_all(
        jnp.broadcast_to(value[None], (count, *value.shape)), axis, 0, 0, axis_index_groups=groups
    )


def local(
    q_latent,
    kv_latent,
    key_rope,
    pool_input,
    q_lat_gain,
    kv_lat_gain,
    q_head_gain,
    k_head_gain,
    pool_gain,
    q_up,
    key_up,
    value_up,
    pool_mix,
    out_pool,
    out_attn,
):
    row_count = q_latent.shape[0]
    sp_index = lax.axis_index("sp")
    sp_size = lax.axis_size("sp")
    core = lax.axis_index("tp")
    line = lax.axis_index("fs")
    z, y = sp_index // Y, sp_index % Y
    own_pos = sp_index * row_count + jnp.arange(row_count, dtype=jnp.int32)
    key_groups = [
        [p * Y + n for p in (j, PLANES - 1 - j) for n in range(Y)] for j in range(PLANES // 2)
    ]
    query_groups = [
        [(c + 2 * i) * Y + n for i in range(MEMBERS)] for c in range(2) for n in range(Y)
    ]
    block_cos, block_sin, in_cos, in_sin = turn_tables(row_count, sp_size)

    share = lax.dynamic_slice_in_dim(kv_latent, core * HALF, HALF, 0)
    share_rope = lax.dynamic_slice_in_dim(key_rope, core * HALF, HALF, 0)
    share = row_norm(share.astype(jnp.float32), kv_lat_gain).astype(jnp.bfloat16)
    share = jnp.concatenate([share.T, share_rope.T], axis=0)
    share = lax.dynamic_slice_in_dim(share, line * 80, 80, 0)
    mine = to_all(to_all(share, "sp", key_groups), "fs")
    other = lax.ppermute(mine, "tp", [(0, 1), (1, 0)])

    own_cos = lax.dynamic_slice_in_dim(jnp.asarray(block_cos), sp_index, 1, 0)
    own_sin = lax.dynamic_slice_in_dim(jnp.asarray(block_sin), sp_index, 1, 0)
    queries = make_queries(
        q_latent,
        q_lat_gain,
        q_up,
        q_head_gain,
        k_head_gain,
        own_cos * in_cos - own_sin * in_sin,
        own_sin * in_cos + own_cos * in_sin,
    )
    queries = to_all(queries, "sp", query_groups)
    within = jnp.asarray(np.stack([in_cos.T, in_sin.T]))
    near = lax.dynamic_slice_in_dim(within, core * HALF, HALF, 2)
    far = lax.dynamic_slice_in_dim(within, HALF - core * HALF, HALF, 2)
    low_plane = jnp.minimum(z, PLANES - 1 - z)
    place = jnp.stack([low_plane, PLANES - 1 - low_plane, z % 2, y, core * HALF]).astype(jnp.int32)
    partial_out = attend(
        place,
        mine,
        other,
        queries,
        key_up.T,
        value_up,
        k_head_gain[NOPE:, None],
        [jnp.asarray(t[:, :, None]) for t in (block_cos, block_sin)],
        near,
        far,
    )
    parts = lax.all_to_all(partial_out, "sp", 0, 0, axis_index_groups=query_groups)
    head_count = parts.shape[2] // VD
    terms = parts[:, row_count : row_count + 3 * head_count].astype(jnp.float32)
    level = jnp.sum(terms.reshape(MEMBERS, head_count, 3, row_count), axis=2)
    top = jnp.max(level, axis=0)
    shares = jnp.exp2(level - top)
    total = jnp.sum(shares, axis=0)
    log_weight = (top + jnp.log2(total)) * LN2
    shares = jnp.transpose(shares / total, (0, 2, 1))[..., None]
    attended = jnp.sum(
        parts[:, :row_count].reshape(MEMBERS, row_count, head_count, VD).astype(jnp.float32)
        * shares,
        axis=0,
    )
    attended = attended.reshape(row_count, head_count * VD).astype(jnp.bfloat16)

    earlier = lax.ppermute(
        pool_input[row_count - 15 :], "sp", [(i, i + 1) for i in range(sp_size - 1)]
    )
    extended = jnp.concatenate([earlier, pool_input], axis=0).astype(jnp.float32)
    window = jnp.left_shift(jnp.int32(2), line)
    window_sum = jnp.zeros((row_count, pool_input.shape[1]), jnp.float32)
    for lag_rows in range(16):
        window_sum = window_sum + jnp.where(
            lag_rows < window, extended[15 - lag_rows : 15 - lag_rows + row_count], 0.0
        )
    counts = jnp.minimum(own_pos + 1, window).astype(jnp.float32)[:, None]
    pool_diff = (window_sum / counts - extended[15:]).astype(jnp.bfloat16)
    pooled = (
        jnp.dot(pool_diff, pool_mix[0], preferred_element_type=jnp.float32) * pool_gain
    ).astype(jnp.bfloat16)

    lines = lax.axis_size("fs")
    channels = jnp.concatenate([pooled, attended], axis=1).reshape(lines, 2, -1, 128 + head_count * VD)

    def projected(rows):
        rows = rows.reshape(-1, rows.shape[-1])
        return jnp.dot(rows[:, :128], out_pool, preferred_element_type=jnp.float32) + jnp.dot(
            rows[:, 128:], out_attn, preferred_element_type=jnp.float32
        )

    sent = projected(lax.dynamic_index_in_dim(channels, 1 - core, 1, False)).astype(jnp.bfloat16)
    received = lax.ppermute(sent, "tp", [(0, 1), (1, 0)])
    kept = projected(lax.dynamic_index_in_dim(channels, core, 1, False))
    chip = (kept + received.astype(jnp.float32)).astype(jnp.bfloat16)
    chip = lax.all_to_all(chip.reshape(lines, -1, chip.shape[1]), "fs", 0, 0)
    mixed = jnp.sum(chip.astype(jnp.float32), axis=0).astype(jnp.bfloat16)
    return (mixed, log_weight)


def solution(mesh):
    in_specs = (
        P("sp", None),
        P("sp", None),
        P("sp", None),
        P("sp", "fs"),
        P(),
        P(),
        P(),
        P(),
        P(("fs", "tp")),
        P(None, ("fs", "tp")),
        P(None, ("fs", "tp")),
        P(None, ("fs", "tp")),
        P("fs", None, "tp"),
        P(("fs", "tp"), None),
        P(("fs", "tp"), None),
    )
    out_specs = (P(("sp", "fs", "tp"), None), P(("fs", "tp"), "sp"))
    return jax.shard_map(local, mesh=mesh, in_specs=in_specs, out_specs=out_specs, check_vma=False)
```

time: 209 us -> 164 us (0.78)
  the two profiles are of different devices: /device:TPU:8 before, /device:TPU:72 now
where the time goes in v2:
time: 164 us; the launch traced here: 163 us
  waiting for transfers between devices  73.2 us (45%)
  starting transfers between devices  35.9 us (22%)
  Pallas kernels  24.9 us (15%)
  local copies, waits for them, and re-layouts  16 us (10%)
  other arithmetic  6.85 us (4%)
  matrix products  5.18 us (3%)
    all_to_all x3, waiting for transfers between devices, to_all(): lax.all_to_all(jnp.broadcast_to(value[None], (count, *value.shape)), axis...  46.9 us
    pallas_call x1, Pallas kernels, attend(): pl.pallas_call(attend_kernel, out_shape=jax.ShapeDtypeStruct((count, rows...  24.9 us
    all_to_all x3, starting transfers between devices, to_all(): lax.all_to_all(jnp.broadcast_to(value[None], (count, *value.shape)), axis...  23.2 us
    all_to_all x1, waiting for transfers between devices, local(): chip = lax.all_to_all(chip.reshape(lines, -1, chip.shape[1]), 'fs', 0, 0)  13.4 us
    all_to_all x1, waiting for transfers between devices, local(): lax.all_to_all(partial_out, 'sp', 0, 0, axis_index_groups=query_groups)  7.12 us
    mul x2, local copies, waits for them, and re-layouts, local(): parts[:, :row_count].reshape(MEMBERS, row_count, head_count, VD)  5.14 us
    ppermute x1, waiting for transfers between devices, local(): lax.ppermute(pool_input[row_count - 15:], 'sp', [(i, i + 1) for i in rang...  3.56 us
    unnamed x30, local copies, waits for them, and re-layouts  3.56 us
  transfers between devices with their start and end apart: 8, of which 7 were waited for; matrix products, arithmetic and copies ran while one was open for 7% of the time, Pallas kernels for 0%

profile of v2, /device:TPU:72, one launch (start us, length us, event | category | flops | bytes accessed | tf_op | source)
XLA Modules:
  0.0 163.1 jit_solution(12658522174555583304)
XLA Ops:
  0.7 1.1 fusion.28
  1.8 0.7 dynamic-slice_bitcast_fusion
  2.5 0.1 copy.44
  2.6 0.9 fusion.32
  3.6 0.1 fusion.38
  3.8 0.8 broadcast_in_dim.28
  4.6 15.1 %all-to-all-start = ((bf16[16,80,128]{2,1,0:T(8,128)(2,1)}), bf16[16,80,128]{2,1,0:T(8,128)(2,1)S(1)}, u32[]{:S(2)}, u32[]{:S(2)}) async-start(bf16[16,80,128]{2,1,0:T(8,128)(2,1)} %broadcast_in_dim.28), calls=%async_computation | async-start | bytes 655360 | tf_op jit(solution)/shard_map/all_to_all | solution.py:232
  19.7 1.1 fusion.2
  20.8 1.5 fusion.5
  22.4 11.5 %all-to-all-done = bf16[16,80,128]{2,1,0:T(8,128)(2,1)S(1)} async-done(((bf16[16,80,128]{2,1,0:T(8,128)(2,1)}), bf16[16,80,128]{2,1,0:T(8,128)(2,1)S(1)}, u32[]{:S(2)}, u32[]{:S(2)}) %all-to-all-start) | async-done | bytes 327712 | tf_op jit(solution)/shard_map/all_to_all | solution.py:232
  33.9 1.2 broadcast_in_dim.56
  35.1 4.3 %all-to-all-start.1 = ((bf16[4,16,80,128]{3,2,1,0:T(8,128)(2,1)}), bf16[4,16,80,128]{3,2,1,0:T(8,128)(2,1)}, u32[]{:S(2)}, u32[]{:S(2)}) async-start(bf16[4,16,80,128]{3,2,1,0:T(8,128)(2,1)} %broadcast_in_dim.56), calls=%async_computation.1 | async-start | bytes 2621440 | tf_op jit(solution)/shard_map/all_to_all | solution.py:232
  39.4 0.7 fusion.46
  40.5 15.2 %all-to-all-done.1.mine_ref = bf16[4,16,80,128]{3,2,1,0:T(8,128)(2,1)} async-done(((bf16[4,16,80,128]{3,2,1,0:T(8,128)(2,1)}), bf16[4,16,80,128]{3,2,1,0:T(8,128)(2,1)}, u32[]{:S(2)}, u32[]{:S(2)}) %all-to-all-start.1) | async-done | bytes 1310752 | tf_op jit(solution)/shard_map/all_to_all | solution.py:232
  55.7 1.9 %collective-permute-start.1 = (bf16[4,16,80,128]{3,2,1,0:T(8,128)(2,1)}, bf16[4,16,80,128]{3,2,1,0:T(8,128)(2,1)}, u32[]{:S(2)}, u32[]{:S(2)}) collective-permute-start(bf16[4,16,80,128]{3,2,1,0:T(8,128)(2,1)} %all-to-all-done.1.mine_ref), channel_id=1, source_target_pairs={{0,1},{1,0},{2,3},{3,2},{4,5},{5,4},{6,7},{7,6},{8,9},{9,8},{10,11... | collective-permute-start | bytes 3932168 | tf_op jit(solution)/shard_map/ppermute | solution.py:275
  57.8 0.1 copy.48
  57.9 1.0 broadcast_in_dim.57
  58.9 3.7 %all-to-all-start.2 = ((bf16[4,256,384]{2,1,0:T(8,128)(2,1)}), bf16[4,256,384]{2,1,0:T(8,128)(2,1)S(1)}, u32[]{:S(2)}, u32[]{:S(2)}) async-start(bf16[4,256,384]{2,1,0:T(8,128)(2,1)} %broadcast_in_dim.57), calls=%async_computation.2 | async-start | bytes 1572864 | tf_op jit(solution)/shard_map/all_to_all | solution.py:232
  62.6 0.7 copy.50.gain_ref
  63.3 0.8 copy.49
  64.1 0.6 stack.23.place_ref
  64.7 0.6 constant_dynamic-slice_fusion.2
  65.3 20.2 %all-to-all-done.2.q_ref = bf16[4,256,384]{2,1,0:T(8,128)(2,1)S(1)} async-done(((bf16[4,256,384]{2,1,0:T(8,128)(2,1)}), bf16[4,256,384]{2,1,0:T(8,128)(2,1)S(1)}, u32[]{:S(2)}, u32[]{:S(2)}) %all-to-all-start.2) | async-done | bytes 786464 | tf_op jit(solution)/shard_map/all_to_all | solution.py:232
  85.5 0.9 copy-done.3
  86.4 24.9 %attend.1 = bf16[4,272,256]{2,1,0:T(8,128)(2,1)} custom-call(s32[5]{0:T(128)} %stack.23.place_ref, bf16[4,16,80,128]{3,2,1,0:T(8,128)(2,1)} %all-to-all-done.1.mine_ref, bf16[4,16,80,128]{3,2,1,0:T(8,128)(2,1)} %collective-permute-done.1.other_ref, bf16[4,256,384]{2,1,0:T(8,128)(2,1)} %copy-done.3, bf16[256,256]{1,0:T(8,128)(2,1)} %bitcast.53, ...), custom_call_target="tpu_custom_call" | custom-call | flops 5368709120 | bytes 2621440 | tf_op jit(solution)/shard_map/attend/pallas_call | solution.py:191
  111.3 3.5 %all-to-all-start.3 = ((bf16[4,272,256]{2,1,0:T(8,128)(2,1)}), bf16[4,272,256]{2,1,0:T(8,128)(2,1)S(1)}, u32[]{:S(2)}, u32[]{:S(2)}) async-start(bf16[4,272,256]{2,1,0:T(8,128)(2,1)} %attend.1), calls=%async_computation.3 | async-start | bytes 1114112 | tf_op jit(solution)/shard_map/all_to_all | solution.py:306
  114.8 1.9 %collective-permute-start = (bf16[15,256]{1,0:T(8,128)(2,1)S(1)}, bf16[15,256]{1,0:T(8,128)(2,1)S(1)}, u32[]{:S(2)}, u32[]{:S(2)}) collective-permute-start(bf16[15,256]{1,0:T(8,128)(2,1)S(1)} %slice.85), channel_id=1, source_target_pairs={{0,8},{8,16},{16,24},{24,32},{32,40},{40,48},{48,56},{56,64},{64,7... | collective-permute-start | bytes 23048 | tf_op jit(solution)/shard_map/ppermute | solution.py:322
  116.8 3.6 %collective-permute-done = bf16[15,256]{1,0:T(8,128)(2,1)S(1)} collective-permute-done((bf16[15,256]{1,0:T(8,128)(2,1)S(1)}, bf16[15,256]{1,0:T(8,128)(2,1)S(1)}, u32[]{:S(2)}, u32[]{:S(2)}) %collective-permute-start) | collective-permute-done | bytes 7712 | tf_op jit(solution)/shard_map/ppermute | solution.py:322
  120.4 0.7 fusion.1
  121.1 0.1 copy.58
  121.2 7.1 %all-to-all-done.3 = bf16[4,272,256]{2,1,0:T(8,128)(2,1)S(1)} async-done(((bf16[4,272,256]{2,1,0:T(8,128)(2,1)}), bf16[4,272,256]{2,1,0:T(8,128)(2,1)S(1)}, u32[]{:S(2)}, u32[]{:S(2)}) %all-to-all-start.3) | async-done | bytes 557088 | tf_op jit(solution)/shard_map/all_to_all | solution.py:306
  128.4 0.1 copy.61
  128.7 0.1 copy.62
  128.9 0.2 copy.57
  129.2 2.0 %mul.217 = f32[4,256,2,128]{3,2,1,0:T(2,128)} broadcast(f32[4,256,2]{2,1,0:T(8,128)S(1)} %copy.57), dimensions={0,1,2} | broadcast | bytes 1056768 | tf_op jit(solution)/shard_map/mul | solution.py:316
  131.2 3.1 %mul.218 = f32[4,256,256]{2,1,0:T(8,128)} reshape(f32[4,256,2,128]{3,2,1,0:T(2,128)} %mul.217) | data formatting | bytes 2097152 | tf_op jit(solution)/shard_map/mul | solution.py:316
  134.3 1.5 multiply_reduce_fusion
  135.9 0.4 fusion.39
  136.3 0.5 fusion
  136.8 1.9 %collective-permute-start.2 = (bf16[128,4096]{1,0:T(8,128)(2,1)S(1)}, bf16[128,4096]{1,0:T(8,128)(2,1)S(1)}, u32[]{:S(2)}, u32[]{:S(2)}) collective-permute-start(bf16[128,4096]{1,0:T(8,128)(2,1)S(1)} %fusion), channel_id=1, source_target_pairs={{0,1},{1,0},{2,3},{3,2},{4,5},{5,4},{6,7},{7,6},{8,9},{9,8},{10,11... | collective-permute-start | bytes 3145736 | tf_op jit(solution)/shard_map/ppermute | solution.py:348
  138.8 0.4 fusion.41
  139.2 2.2 %collective-permute-done.2 = bf16[128,4096]{1,0:T(8,128)(2,1)S(1)} collective-permute-done((bf16[128,4096]{1,0:T(8,128)(2,1)S(1)}, bf16[128,4096]{1,0:T(8,128)(2,1)S(1)}, u32[]{:S(2)}, u32[]{:S(2)}) %collective-permute-start.2) | collective-permute-done | bytes 1048608 | tf_op jit(solution)/shard_map/ppermute | solution.py:348
  141.4 1.6 add_convert_fusion
  143.0 3.5 %all-to-all-start.4 = ((bf16[4,32,4096]{2,1,0:T(8,128)(2,1)}), bf16[4,32,4096]{2,1,0:T(8,128)(2,1)S(1)}, u32[]{:S(2)}, u32[]{:S(2)}) async-start(bf16[4,32,4096]{2,1,0:T(8,128)(2,1)} %bitcast.22), calls=%async_computation.4 | async-start | bytes 2097152 | tf_op jit(solution)/shard_map/all_to_all | solution.py:351
  146.5 0.7 add_multiply_fusion
  147.2 1.6 copy.59
  148.8 13.4 %all-to-all-done.4 = bf16[4,32,4096]{2,1,0:T(8,128)(2,1)S(1)} async-done(((bf16[4,32,4096]{2,1,0:T(8,128)(2,1)}), bf16[4,32,4096]{2,1,0:T(8,128)(2,1)S(1)}, u32[]{:S(2)}, u32[]{:S(2)}) %all-to-all-start.4) | async-done | bytes 1048608 | tf_op jit(solution)/shard_map/all_to_all | solution.py:351
  162.2 0.9 reduce_sum.75
  (53 shorter events, 1.0 us)
Async XLA Ops:
  0.6 135.7 %copy-start = (bf16[256,4096]{1,0:T(8,128)(2,1)S(1)}, bf16[256,4096]{1,0:T(8,128)(2,1)}, u32[]{:S(2)}) copy-start(bf16[256,4096]{1,0:T(8,128)(2,1)} %param.36) | copy-start | bytes 6291460
  0.6 21.7 %copy-start.11 = (f32[192]{0:T(256)S(1)}, f32[192]{0:T(256)}, u32[]{:S(2)}) copy-start(f32[192]{0:T(256)} %param.29) | copy-start | bytes 2308
  4.6 29.3 %all-to-all-start = ((bf16[16,80,128]{2,1,0:T(8,128)(2,1)}), bf16[16,80,128]{2,1,0:T(8,128)(2,1)S(1)}, u32[]{:S(2)}, u32[]{:S(2)}) async-start(bf16[16,80,128]{2,1,0:T(8,128)(2,1)} %broadcast_in_dim.28), calls=%async_computation | async-start | bytes 655360 | tf_op jit(solution)/shard_map/all_to_all | solution.py:232
  22.4 17.8 %copy-start.7 = (f32[256,32]{0,1:T(8,128)S(1)}, f32[256,32]{0,1:T(8,128)}, u32[]{:S(2)}) copy-start(f32[256,32]{0,1:T(8,128)} %constant.136.clone) | copy-start | bytes 98308
  22.4 17.8 %copy-start.8 = (f32[256,32]{0,1:T(8,128)S(1)}, f32[256,32]{0,1:T(8,128)}, u32[]{:S(2)}) copy-start(f32[256,32]{0,1:T(8,128)} %constant.135.clone) | copy-start | bytes 98308
  22.4 17.8 %copy-start.9 = (f32[192]{0:T(256)S(1)}, f32[192]{0:T(256)}, u32[]{:S(2)}) copy-start(f32[192]{0:T(256)} %param.28) | copy-start | bytes 2308
  35.1 20.6 %all-to-all-start.1 = ((bf16[4,16,80,128]{3,2,1,0:T(8,128)(2,1)}), bf16[4,16,80,128]{3,2,1,0:T(8,128)(2,1)}, u32[]{:S(2)}, u32[]{:S(2)}) async-start(bf16[4,16,80,128]{3,2,1,0:T(8,128)(2,1)} %broadcast_in_dim.56), calls=%async_computation.1 | async-start | bytes 2621440 | tf_op jit(solution)/shard_map/all_to_all | solution.py:232
  40.3 23.0 %copy-start.5 = (bf16[256,256]{1,0:T(8,128)(2,1)S(1)}, bf16[256,256]{1,0:T(8,128)(2,1)}, u32[]{:S(2)}) copy-start(bf16[256,256]{1,0:T(8,128)(2,1)} %param.32) | copy-start | bytes 393220
  40.4 24.3 %copy-start.6 = (f32[2,32,256]{2,1,0:T(8,128)S(1)}, f32[2,32,256]{2,1,0:T(8,128)}, u32[]{:S(2)}) copy-start(f32[2,32,256]{2,1,0:T(8,128)} %constant.137.clone) | copy-start | bytes 196612
  55.7 29.8 %collective-permute-start.1 = (bf16[4,16,80,128]{3,2,1,0:T(8,128)(2,1)}, bf16[4,16,80,128]{3,2,1,0:T(8,128)(2,1)}, u32[]{:S(2)}, u32[]{:S(2)}) collective-permute-start(bf16[4,16,80,128]{3,2,1,0:T(8,128)(2,1)} %all-to-all-done.1.mine_ref), channel_id=1, source_target_pairs={{0,1},{1,0},{2,3},{3,2},{4,5},{5,4},{6,7},{7,6},{8,9},{9,8},{10,11... | collective-permute-start | bytes 3932168 | tf_op jit(solution)/shard_map/ppermute | solution.py:275
  58.9 26.6 %all-to-all-start.2 = ((bf16[4,256,384]{2,1,0:T(8,128)(2,1)}), bf16[4,256,384]{2,1,0:T(8,128)(2,1)S(1)}, u32[]{:S(2)}, u32[]{:S(2)}) async-start(bf16[4,256,384]{2,1,0:T(8,128)(2,1)} %broadcast_in_dim.57), calls=%async_computation.2 | async-start | bytes 1572864 | tf_op jit(solution)/shard_map/all_to_all | solution.py:232
  85.5 0.9 copy-start.3
  86.4 28.4 %copy-start.4 = (bf16[256,256]{1,0:T(8,128)(2,1)S(1)}, bf16[256,256]{1,0:T(8,128)(2,1)}, u32[]{:S(2)}) copy-start(bf16[256,256]{1,0:T(8,128)(2,1)} %param.25) | copy-start | bytes 393220
  86.4 34.0 %copy-start.10 = (bf16[1,256,128]{2,1,0:T(8,128)(2,1)S(1)}, bf16[1,256,128]{2,1,0:T(8,128)(2,1)}, u32[]{:S(2)}) copy-start(bf16[1,256,128]{2,1,0:T(8,128)(2,1)} %param.34) | copy-start | bytes 196612
  86.4 34.0 %copy-start.12 = (f32[128]{0:T(128)S(1)}, f32[128]{0:T(128)}, u32[]{:S(2)}) copy-start(f32[128]{0:T(128)} %param.30) | copy-start | bytes 1540
  111.3 17.1 %all-to-all-start.3 = ((bf16[4,272,256]{2,1,0:T(8,128)(2,1)}), bf16[4,272,256]{2,1,0:T(8,128)(2,1)S(1)}, u32[]{:S(2)}, u32[]{:S(2)}) async-start(bf16[4,272,256]{2,1,0:T(8,128)(2,1)} %attend.1), calls=%async_computation.3 | async-start | bytes 1114112 | tf_op jit(solution)/shard_map/all_to_all | solution.py:306
  114.8 5.5 %collective-permute-start = (bf16[15,256]{1,0:T(8,128)(2,1)S(1)}, bf16[15,256]{1,0:T(8,128)(2,1)S(1)}, u32[]{:S(2)}, u32[]{:S(2)}) collective-permute-start(bf16[15,256]{1,0:T(8,128)(2,1)S(1)} %slice.85), channel_id=1, source_target_pairs={{0,8},{8,16},{16,24},{24,32},{32,40},{40,48},{48,56},{56,64},{64,7... | collective-permute-start | bytes 23048 | tf_op jit(solution)/shard_map/ppermute | solution.py:322
  128.4 0.8 copy-start.2
  131.2 4.7 %copy-start.1 = (bf16[128,4096]{1,0:T(8,128)(2,1)S(1)}, bf16[128,4096]{1,0:T(8,128)(2,1)}, u32[]{:S(2)}) copy-start(bf16[128,4096]{1,0:T(8,128)(2,1)} %param.35) | copy-start | bytes 3145732
  136.8 4.6 %collective-permute-start.2 = (bf16[128,4096]{1,0:T(8,128)(2,1)S(1)}, bf16[128,4096]{1,0:T(8,128)(2,1)S(1)}, u32[]{:S(2)}, u32[]{:S(2)}) collective-permute-start(bf16[128,4096]{1,0:T(8,128)(2,1)S(1)} %fusion), channel_id=1, source_target_pairs={{0,1},{1,0},{2,3},{3,2},{4,5},{5,4},{6,7},{7,6},{8,9},{9,8},{10,11... | collective-permute-start | bytes 3145736 | tf_op jit(solution)/shard_map/ppermute | solution.py:348
  143.0 19.2 %all-to-all-start.4 = ((bf16[4,32,4096]{2,1,0:T(8,128)(2,1)}), bf16[4,32,4096]{2,1,0:T(8,128)(2,1)S(1)}, u32[]{:S(2)}, u32[]{:S(2)}) async-start(bf16[4,32,4096]{2,1,0:T(8,128)(2,1)} %bitcast.22), calls=%async_computation.4 | async-start | bytes 2097152 | tf_op jit(solution)/shard_map/all_to_all | solution.py:351

commit v3 on v2

--- a/solution.py
+++ b/solution.py
@@ -7,6 +7,7 @@
 from jax.experimental import pallas as pl
 from jax.experimental.pallas import tpu as pltpu
 from jax.sharding import PartitionSpec as P
+
 
 NOPE = 128
 ROPE = 64
@@ -59,33 +60,43 @@
     place_ref,
     mine_ref,
     other_ref,
-    q_ref,
-    key_up_ref,
-    value_up_ref,
-    gain_ref,
-    block_cos_ref,
-    block_sin_ref,
-    near_ref,
-    far_ref,
-    out_ref,
-    max_ref,
-    sum_ref,
-    acc_ref,
-    key_ref,
-    lat_ref,
+    *refs,
 ):
+    query_refs, refs = refs[:MEMBERS], refs[MEMBERS:]
+    (
+        key_up_ref,
+        value_up_ref,
+        gain_ref,
+        block_cos_ref,
+        block_sin_ref,
+        near_ref,
+        far_ref,
+        out_ref,
+        q_ref,
+        lat_ref,
+        weight_ref,
+        *refs,
+    ) = refs
     heads = key_up_ref.shape[0] // NOPE
-    count, rows, _ = q_ref.shape
+    max_refs, sum_refs, acc_refs, key_refs, score_refs = (
+        refs[n * heads : (n + 1) * heads] for n in range(5)
+    )
+    count = MEMBERS
+    rows = query_refs[0].shape[0]
     step = pl.program_id(0)
-    plane, parity, own_y, offset = place_ref[step], place_ref[2], place_ref[3], place_ref[4]
+    plane, parity, own_y = place_ref[step], place_ref[2], place_ref[3]
+    offset, member = place_ref[4], place_ref[5]
     width = Y * rows
 
     @pl.when(step == 0)
     def _():
-        max_ref[...] = jnp.full(max_ref.shape, -HUGE, jnp.float32)
-        sum_ref[...] = jnp.zeros_like(sum_ref)
-        acc_ref[...] = jnp.zeros_like(acc_ref)
-        key_ref[:, NOPE:, :] = jnp.zeros((heads, 256 - NOPE, width), key_ref.dtype)
+        for d in range(count):
+            q_ref[lax.rem(member + (count - d), count)] = query_refs[d][...]
+        for h in range(heads):
+            max_refs[h][...] = jnp.full(max_refs[h].shape, -HUGE, jnp.float32)
+            sum_refs[h][...] = jnp.zeros_like(sum_refs[h])
+            acc_refs[h][...] = jnp.zeros_like(acc_refs[h])
+            key_refs[h][NOPE:, :] = jnp.zeros((256 - NOPE, width), jnp.bfloat16)
 
     def build_keys():
         @pl.loop(0, Y)
@@ -109,50 +120,74 @@
                     part = raw[h * NOPE : (h + 1) * NOPE]
                     square = jnp.sum(part * part, axis=0, keepdims=True) + rope_sq
                     inverse = lax.rsqrt(square * (1.0 / (NOPE + ROPE)) + EPS)
-                    key_ref[h, :NOPE, at] = (part * inverse).astype(key_ref.dtype)
-                    key_ref[h, NOPE + h * ROPE : NOPE + (h + 1) * ROPE, at] = (
+                    key_refs[h][:NOPE, at] = (part * inverse).astype(jnp.bfloat16)
+                    key_refs[h][NOPE + h * ROPE : NOPE + (h + 1) * ROPE, at] = (
                         turned * inverse
-                    ).astype(key_ref.dtype)
-
-    def attend(i, h, masked):
+                    ).astype(jnp.bfloat16)
+
+    def score(i, h):
         query = jnp.concatenate(
-            [q_ref[i, :, pl.ds(pl.multiple_of(h * NOPE, NOPE), NOPE)], q_ref[i, :, heads * NOPE :]], axis=1
+            [q_ref[i, :, h * NOPE : (h + 1) * NOPE], q_ref[i, :, heads * NOPE :]], axis=1
         )
-        scores = jnp.dot(query, key_ref[h], preferred_element_type=jnp.float32)
-        if masked:
-            column = lax.broadcasted_iota(jnp.int32, (rows, width), 1)
-            row = lax.broadcasted_iota(jnp.int32, (rows, width), 0)
-            half_at = jnp.where(column < Y * HALF, offset, HALF - offset)
-            key_at = (column % (Y * HALF)) // HALF * rows + half_at + column % HALF
-            scores = jnp.where(key_at <= own_y * rows + row, scores, -HUGE)
-        at = i * heads + h
-        before = max_ref[at]
-        after = jnp.maximum(before, jnp.max(scores, axis=1, keepdims=True))
+        score_refs[h][...] = jnp.dot(query, key_refs[h][...], preferred_element_type=jnp.float32)
+
+    def mask(h):
+        column = lax.broadcasted_iota(jnp.int32, (rows, width), 1)
+        row = lax.broadcasted_iota(jnp.int32, (rows, width), 0)
+        half_at = jnp.where(column < Y * HALF, offset, HALF - offset)
+        key_at = (column % (Y * HALF)) // HALF * rows + half_at + column % HALF
+        seen = key_at <= own_y * rows + row
+        score_refs[h][...] = jnp.where(seen, score_refs[h][...], -HUGE)
+
+    def weigh(i, h):
+        slices = [pl.ds(n * 128, 128) for n in range(width // 128)]
+        top = score_refs[h][:, slices[0]]
+        for at in slices[1:]:
+            top = jnp.maximum(top, score_refs[h][:, at])
+        before = max_refs[h][i]
+        after = jnp.maximum(before, jnp.max(top, axis=1, keepdims=True))
         factor = jnp.exp2(before - after)
-        weights = jnp.exp2(scores - after[:, :1])
-        partial_sum = weights[:, :128]
-        for n in range(1, width // 128):
-            partial_sum = partial_sum + weights[:, n * 128 : (n + 1) * 128]
-        max_ref[at] = after
-        sum_ref[at] = sum_ref[at] * factor + partial_sum
+        total = sum_refs[h][i] * factor
+        for at in slices:
+            weights = jnp.exp2(score_refs[h][:, at] - after)
+            weight_ref[:, at] = weights.astype(jnp.bfloat16)
+            total = total + weights
+        max_refs[h][i] = after
+        sum_refs[h][i] = total
         update = lax.dot_general(
-            weights.astype(jnp.bfloat16),
+            weight_ref[...],
             lat_ref[...],
             (((1,), (1,)), ((), ())),
             preferred_element_type=jnp.float32,
         )
-        acc_ref[at] = acc_ref[at] * factor[:, :1] + update
-
-    @pl.when(plane <= parity + 2 * (count - 1))
+        acc_refs[h][i] = acc_refs[h][i] * jnp.concatenate([factor, factor], axis=1) + update
+
+    first = lax.div(plane - parity + 1, 2)
+
+    @pl.when(first < count)
     def _():
         build_keys()
-
-        @pl.loop(0, count * heads)
-        def _(at):
-            i, h = at // heads, at % heads
-            query_plane = parity + 2 * i
-            pl.when(plane < query_plane)(lambda: attend(i, h, False))
-            pl.when(plane == query_plane)(lambda: attend(i, h, True))
+        score(first, 0)
+        own = plane == parity + 2 * first
+
+        @pl.when(own)
+        def _():
+            for h in range(1, heads):
+                score(first, h)
+            for h in range(heads):
+                mask(h)
+            for h in range(heads):
+                weigh(first, h)
+            score(jnp.minimum(first + 1, count - 1), 0)
+
+        @pl.loop(jnp.where(own, first + 1, first), count)
+        def _(i):
+            for h in range(heads):
+                if h + 1 < heads:
+                    score(i, h + 1)
+                else:
+                    score(jnp.minimum(i + 1, count - 1), 0)
+                weigh(i, h)
 
     @pl.when(step == pl.num_programs(0) - 1)
     def _():
@@ -160,11 +195,10 @@
         def _(i):
             out_ref[i, rows:, :] = jnp.zeros((EXTRA, heads * VD), out_ref.dtype)
             for h in range(heads):
-                at = i * heads + h
-                total = jnp.sum(sum_ref[at], axis=1, keepdims=True)
+                total = jnp.sum(sum_refs[h][i], axis=1, keepdims=True)
                 seen = total > 0.0
                 total = jnp.where(seen, total, 1.0)
-                mean = acc_ref[at] / total
+                mean = acc_refs[h][i] / total
                 high = mean.astype(jnp.bfloat16)
                 low = (mean - high.astype(jnp.float32)).astype(jnp.bfloat16)
                 value = value_up_ref[:, h * VD : (h + 1) * VD]
@@ -172,7 +206,7 @@
                     jnp.dot(high, value, preferred_element_type=jnp.float32)
                     + jnp.dot(low, value, preferred_element_type=jnp.float32)
                 ).astype(out_ref.dtype)
-                level = jnp.where(seen, max_ref[at] + jnp.log2(total), -HUGE).T[:1]
+                level = jnp.where(seen, max_refs[h][i] + jnp.log2(total), -HUGE).T[:1]
                 for term in range(3):
                     rounded = level.astype(jnp.bfloat16)
                     out_ref[i, pl.ds(rows + h * 3 + term, 1), :] = rounded
@@ -180,7 +214,7 @@
 
 
 def attend(place, mine, other, queries, key_up, value_up, gain, block_tables, near, far):
-    count, rows, _ = queries.shape
+    rows, channels = queries[0].shape
     heads = key_up.shape[0] // NOPE
 
     def whole(*shape):
@@ -188,16 +222,23 @@
 
     keys = pl.BlockSpec((4, Y, 80, HALF), lambda i, w: (0, i, 0, 0))
     table = pl.BlockSpec((Y, ROPE // 2, 1), lambda i, w: (w[i], 0, 0))
+    wide = [
+        pltpu.VMEM((MEMBERS, rows, 128), jnp.float32),
+        pltpu.VMEM((MEMBERS, rows, 128), jnp.float32),
+        pltpu.VMEM((MEMBERS, rows, 256), jnp.float32),
+        pltpu.VMEM((256, Y * rows), jnp.bfloat16),
+        pltpu.VMEM((rows, Y * rows), jnp.float32),
+    ]
     return pl.pallas_call(
         attend_kernel,
-        out_shape=jax.ShapeDtypeStruct((count, rows + EXTRA, heads * VD), jnp.bfloat16),
+        out_shape=jax.ShapeDtypeStruct((MEMBERS, rows + EXTRA, heads * VD), jnp.bfloat16),
         grid_spec=pltpu.PrefetchScalarGridSpec(
             num_scalar_prefetch=1,
             grid=(2,),
             in_specs=[
                 keys,
                 keys,
-                whole(*queries.shape),
+                *[whole(rows, channels)] * MEMBERS,
                 whole(*key_up.shape),
                 whole(*value_up.shape),
                 whole(ROPE, 1),
@@ -206,13 +247,12 @@
                 whole(*near.shape),
                 whole(*far.shape),
             ],
-            out_specs=whole(count, rows + EXTRA, heads * VD),
+            out_specs=whole(MEMBERS, rows + EXTRA, heads * VD),
             scratch_shapes=[
-                pltpu.VMEM((count * heads, rows, 128), jnp.float32),
-                pltpu.VMEM((count * heads, rows, 128), jnp.float32),
-                pltpu.VMEM((count * heads, rows, 256), jnp.float32),
-                pltpu.VMEM((heads, 256, Y * rows), jnp.bfloat16),
+                pltpu.VMEM((MEMBERS, rows, channels), jnp.bfloat16),
                 pltpu.VMEM((256, Y * rows), jnp.bfloat16),
+                pltpu.VMEM((rows, Y * rows), jnp.bfloat16),
+                *[s for s in wide for _ in range(heads)],
             ],
         ),
         compiler_params=pltpu.CompilerParams(
@@ -224,7 +264,7 @@
             transcendentals=5 * rows * Y * rows * heads,
         ),
         name="attend",
-    )(place, mine, other, queries, key_up, value_up, gain, *block_tables, near, far)
+    )(place, mine, other, *queries, key_up, value_up, gain, *block_tables, near, far)
 
 
 def to_all(value, axis, groups=None):
@@ -256,7 +296,7 @@
     sp_size = lax.axis_size("sp")
     core = lax.axis_index("tp")
     line = lax.axis_index("fs")
-    z, y = sp_index // Y, sp_index % Y
+    z, y = lax.div(sp_index, Y), lax.rem(sp_index, Y)
     own_pos = sp_index * row_count + jnp.arange(row_count, dtype=jnp.int32)
     key_groups = [
         [p * Y + n for p in (j, PLANES - 1 - j) for n in range(Y)] for j in range(PLANES // 2)
@@ -271,7 +311,8 @@
     share = row_norm(share.astype(jnp.float32), kv_lat_gain).astype(jnp.bfloat16)
     share = jnp.concatenate([share.T, share_rope.T], axis=0)
     share = lax.dynamic_slice_in_dim(share, line * 80, 80, 0)
-    mine = to_all(to_all(share, "sp", key_groups), "fs")
+    mine = to_all(share, "sp", key_groups)
+    mine = to_all(mine, "fs")
     other = lax.ppermute(mine, "tp", [(0, 1), (1, 0)])
 
     own_cos = lax.dynamic_slice_in_dim(jnp.asarray(block_cos), sp_index, 1, 0)
@@ -285,12 +326,21 @@
         own_cos * in_cos - own_sin * in_sin,
         own_sin * in_cos + own_cos * in_sin,
     )
-    queries = to_all(queries, "sp", query_groups)
+    queries = [queries] + [
+        lax.ppermute(
+            queries,
+            "sp",
+            [(g[i], g[(i + d) % MEMBERS]) for g in query_groups for i in range(MEMBERS)],
+        )
+        for d in range(1, MEMBERS)
+    ]
     within = jnp.asarray(np.stack([in_cos.T, in_sin.T]))
     near = lax.dynamic_slice_in_dim(within, core * HALF, HALF, 2)
     far = lax.dynamic_slice_in_dim(within, HALF - core * HALF, HALF, 2)
     low_plane = jnp.minimum(z, PLANES - 1 - z)
-    place = jnp.stack([low_plane, PLANES - 1 - low_plane, z % 2, y, core * HALF]).astype(jnp.int32)
+    place = jnp.stack(
+        [low_plane, PLANES - 1 - low_plane, lax.rem(z, 2), y, core * HALF, lax.div(z, 2)]
+    ).astype(jnp.int32)
     partial_out = attend(
         place,
         mine,
@@ -372,4 +422,5 @@
         P(("fs", "tp"), None),
     )
     out_specs = (P(("sp", "fs", "tp"), None), P(("fs", "tp"), "sp"))
+
     return jax.shard_map(local, mesh=mesh, in_specs=in_specs, out_specs=out_specs, check_vma=False)

time: 164 us -> 162 us (0.988)
  the two profiles are of different devices: /device:TPU:72 before, /device:TPU:8 now
where the time goes in v3:
time: 162 us; the launch traced here: 161 us
  waiting for transfers between devices  68.4 us (42%)
  starting transfers between devices  49.6 us (31%)
  Pallas kernels  16.2 us (10%)
  local copies, waits for them, and re-layouts  14.9 us (9%)
  other arithmetic  6.85 us (4%)
  matrix products  4.1 us (3%)
    all_to_all x2, waiting for transfers between devices, to_all(): lax.all_to_all(jnp.broadcast_to(value[None], (count, *value.shape)), axis...  26.9 us
    all_to_all x2, starting transfers between devices, to_all(): lax.all_to_all(jnp.broadcast_to(value[None], (count, *value.shape)), axis...  20.5 us
    pallas_call x1, Pallas kernels, attend(): pl.pallas_call(attend_kernel, out_shape=jax.ShapeDtypeStruct((MEMBERS, ro...  16.2 us
    ppermute x3, waiting for transfers between devices, local(): lax.ppermute(queries, 'sp', [(g[i], g[(i + d) % MEMBERS]) for g in query_...  14.4 us
    all_to_all x1, waiting for transfers between devices, local(): chip = lax.all_to_all(chip.reshape(lines, -1, chip.shape[1]), 'fs', 0, 0)  13.4 us
    ppermute x3, starting transfers between devices, local(): lax.ppermute(queries, 'sp', [(g[i], g[(i + d) % MEMBERS]) for g in query_...  12.5 us
    all_to_all x1, waiting for transfers between devices, local(): lax.all_to_all(partial_out, 'sp', 0, 0, axis_index_groups=query_groups)  8.03 us
    all_to_all x1, starting transfers between devices, local(): lax.all_to_all(partial_out, 'sp', 0, 0, axis_index_groups=query_groups)  7.35 us
  transfers between devices with their start and end apart: 10, of which 9 were waited for; matrix products, arithmetic and copies ran while one was open for 6% of the time, Pallas kernels for 0%

profile of v3, /device:TPU:8, one launch (start us, length us, event | category | flops | bytes accessed | tf_op | source)
XLA Modules:
  0.0 161.3 jit_solution(10509751048171689149)
XLA Ops:
  0.7 1.1 fusion.28
  1.8 0.7 dynamic-slice_bitcast_fusion
  2.6 0.9 fusion.32
  3.8 0.8 broadcast_in_dim.49
  4.6 16.0 %all-to-all-start = ((bf16[16,80,128]{2,1,0:T(8,128)(2,1)}), bf16[16,80,128]{2,1,0:T(8,128)(2,1)S(1)}, u32[]{:S(2)}, u32[]{:S(2)}) async-start(bf16[16,80,128]{2,1,0:T(8,128)(2,1)} %broadcast_in_dim.49), calls=%async_computation | async-start | bytes 655360 | tf_op jit(solution)/shard_map/all_to_all | solution.py:272
  20.6 1.1 fusion.2
  21.7 11.3 %all-to-all-done = bf16[16,80,128]{2,1,0:T(8,128)(2,1)S(1)} async-done(((bf16[16,80,128]{2,1,0:T(8,128)(2,1)}), bf16[16,80,128]{2,1,0:T(8,128)(2,1)S(1)}, u32[]{:S(2)}, u32[]{:S(2)}) %all-to-all-start) | async-done | bytes 327712 | tf_op jit(solution)/shard_map/all_to_all | solution.py:272
  33.0 1.2 broadcast_in_dim.50
  34.2 4.4 %all-to-all-start.1 = ((bf16[4,16,80,128]{3,2,1,0:T(8,128)(2,1)}), bf16[4,16,80,128]{3,2,1,0:T(8,128)(2,1)}, u32[]{:S(2)}, u32[]{:S(2)}) async-start(bf16[4,16,80,128]{3,2,1,0:T(8,128)(2,1)} %broadcast_in_dim.50), calls=%async_computation.1 | async-start | bytes 2621440 | tf_op jit(solution)/shard_map/all_to_all | solution.py:272
  38.7 0.4 fusion.5
  39.3 15.6 %all-to-all-done.1.mine_ref = bf16[4,16,80,128]{3,2,1,0:T(8,128)(2,1)} async-done(((bf16[4,16,80,128]{3,2,1,0:T(8,128)(2,1)}), bf16[4,16,80,128]{3,2,1,0:T(8,128)(2,1)}, u32[]{:S(2)}, u32[]{:S(2)}) %all-to-all-start.1) | async-done | bytes 1310752 | tf_op jit(solution)/shard_map/all_to_all | solution.py:272
  55.0 1.9 %collective-permute-start.1 = (bf16[4,16,80,128]{3,2,1,0:T(8,128)(2,1)}, bf16[4,16,80,128]{3,2,1,0:T(8,128)(2,1)}, u32[]{:S(2)}, u32[]{:S(2)}) collective-permute-start(bf16[4,16,80,128]{3,2,1,0:T(8,128)(2,1)} %all-to-all-done.1.mine_ref), channel_id=1, source_target_pairs={{0,1},{1,0},{2,3},{3,2},{4,5},{5,4},{6,7},{7,6},{8,9},{9,8},{10,11... | collective-permute-start | bytes 3932168 | tf_op jit(solution)/shard_map/ppermute | solution.py:316
  57.1 0.7 fusion.46
  58.1 6.2 %collective-permute-start.4 = (bf16[256,384]{1,0:T(8,128)(2,1)S(1)}, bf16[256,384]{1,0:T(8,128)(2,1)S(1)}, u32[]{:S(2)}, u32[]{:S(2)}) collective-permute-start(bf16[256,384]{1,0:T(8,128)(2,1)S(1)} %pad_maximum_fusion.refs_0_), channel_id=1, source_target_pairs={{0,384},{128,0},{256,128},{384,256},{8,392},{136,8},{264,136},{392... | collective-permute-start | bytes 589832 | tf_op jit(solution)/shard_map/ppermute | solution.py:330
  64.3 4.4 %collective-permute-start.3 = (bf16[256,384]{1,0:T(8,128)(2,1)S(1)}, bf16[256,384]{1,0:T(8,128)(2,1)S(1)}, u32[]{:S(2)}, u32[]{:S(2)}) collective-permute-start(bf16[256,384]{1,0:T(8,128)(2,1)S(1)} %pad_maximum_fusion.refs_0_), channel_id=1, source_target_pairs={{0,256},{128,384},{256,0},{384,128},{8,264},{136,392},{264,8},{392... | collective-permute-start | bytes 589832 | tf_op jit(solution)/shard_map/ppermute | solution.py:330
  68.7 1.9 %collective-permute-start.2 = (bf16[256,384]{1,0:T(8,128)(2,1)S(1)}, bf16[256,384]{1,0:T(8,128)(2,1)S(1)}, u32[]{:S(2)}, u32[]{:S(2)}) collective-permute-start(bf16[256,384]{1,0:T(8,128)(2,1)S(1)} %pad_maximum_fusion.refs_0_), channel_id=1, source_target_pairs={{0,128},{128,256},{256,384},{384,0},{8,136},{136,264},{264,392},{3... | collective-permute-start | bytes 589832 | tf_op jit(solution)/shard_map/ppermute | solution.py:330
  70.7 0.7 copy.50.refs_6_
  71.4 0.8 copy.49
  72.2 0.6 stack.27.place_ref
  72.8 0.6 constant_dynamic-slice_fusion.2
  73.4 7.5 %collective-permute-done.4.refs_3_ = bf16[256,384]{1,0:T(8,128)(2,1)S(1)} collective-permute-done((bf16[256,384]{1,0:T(8,128)(2,1)S(1)}, bf16[256,384]{1,0:T(8,128)(2,1)S(1)}, u32[]{:S(2)}, u32[]{:S(2)}) %collective-permute-start.4) | collective-permute-done | bytes 196640 | tf_op jit(solution)/shard_map/ppermute | solution.py:330
  80.9 4.5 %collective-permute-done.3.refs_2_ = bf16[256,384]{1,0:T(8,128)(2,1)S(1)} collective-permute-done((bf16[256,384]{1,0:T(8,128)(2,1)S(1)}, bf16[256,384]{1,0:T(8,128)(2,1)S(1)}, u32[]{:S(2)}, u32[]{:S(2)}) %collective-permute-start.3) | collective-permute-done | bytes 196640 | tf_op jit(solution)/shard_map/ppermute | solution.py:330
  85.4 2.4 %collective-permute-done.2.refs_1_ = bf16[256,384]{1,0:T(8,128)(2,1)S(1)} collective-permute-done((bf16[256,384]{1,0:T(8,128)(2,1)S(1)}, bf16[256,384]{1,0:T(8,128)(2,1)S(1)}, u32[]{:S(2)}, u32[]{:S(2)}) %collective-permute-start.2) | collective-permute-done | bytes 196640 | tf_op jit(solution)/shard_map/ppermute | solution.py:330
  87.8 0.7 copy-done.15
  88.5 16.2 %attend.1 = bf16[4,272,256]{2,1,0:T(8,128)(2,1)} custom-call(s32[6]{0:T(128)} %stack.27.place_ref, bf16[4,16,80,128]{3,2,1,0:T(8,128)(2,1)} %all-to-all-done.1.mine_ref, bf16[4,16,80,128]{3,2,1,0:T(8,128)(2,1)} %collective-permute-done.1.other_ref, bf16[256,384]{1,0:T(8,128)(2,1)} %copy-done.5, bf16[256,384]{1,0:T(8,128)(2,1)} %copy-done.15, ...), custom_call_target="tpu_custom_call" | custom-call | flops 5368709120 | bytes 2621440 | tf_op jit(solution)/shard_map/attend/pallas_call | solution.py:232
  104.7 7.4 %all-to-all-start.2 = ((bf16[4,272,256]{2,1,0:T(8,128)(2,1)}), bf16[4,272,256]{2,1,0:T(8,128)(2,1)S(1)}, u32[]{:S(2)}, u32[]{:S(2)}) async-start(bf16[4,272,256]{2,1,0:T(8,128)(2,1)} %attend.1), calls=%async_computation.2 | async-start | bytes 1114112 | tf_op jit(solution)/shard_map/all_to_all | solution.py:356
  112.0 1.9 %collective-permute-start = (bf16[15,256]{1,0:T(8,128)(2,1)S(1)}, bf16[15,256]{1,0:T(8,128)(2,1)S(1)}, u32[]{:S(2)}, u32[]{:S(2)}) collective-permute-start(bf16[15,256]{1,0:T(8,128)(2,1)S(1)} %slice.85), channel_id=1, source_target_pairs={{0,8},{8,16},{16,24},{24,32},{32,40},{40,48},{48,56},{56,64},{64,7... | collective-permute-start | bytes 23048 | tf_op jit(solution)/shard_map/ppermute | solution.py:372
  114.0 3.6 %collective-permute-done = bf16[15,256]{1,0:T(8,128)(2,1)S(1)} collective-permute-done((bf16[15,256]{1,0:T(8,128)(2,1)S(1)}, bf16[15,256]{1,0:T(8,128)(2,1)S(1)}, u32[]{:S(2)}, u32[]{:S(2)}) %collective-permute-start) | collective-permute-done | bytes 7712 | tf_op jit(solution)/shard_map/ppermute | solution.py:372
  117.6 0.7 fusion.1
  118.3 0.1 copy.58
  118.5 8.0 %all-to-all-done.2 = bf16[4,272,256]{2,1,0:T(8,128)(2,1)S(1)} async-done(((bf16[4,272,256]{2,1,0:T(8,128)(2,1)}), bf16[4,272,256]{2,1,0:T(8,128)(2,1)S(1)}, u32[]{:S(2)}, u32[]{:S(2)}) %all-to-all-start.2) | async-done | bytes 557088 | tf_op jit(solution)/shard_map/all_to_all | solution.py:356
  126.6 0.1 copy.62
  126.8 0.1 copy.63
  127.1 0.2 copy.57
  127.3 2.0 %mul.217 = f32[4,256,2,128]{3,2,1,0:T(2,128)} broadcast(f32[4,256,2]{2,1,0:T(8,128)S(1)} %copy.57), dimensions={0,1,2} | broadcast | bytes 1056768 | tf_op jit(solution)/shard_map/mul | solution.py:366
  129.4 3.1 %mul.218 = f32[4,256,256]{2,1,0:T(8,128)} reshape(f32[4,256,2,128]{3,2,1,0:T(2,128)} %mul.217) | data formatting | bytes 2097152 | tf_op jit(solution)/shard_map/mul | solution.py:366
  132.5 1.5 multiply_reduce_fusion
  134.0 0.4 fusion.39
  134.5 0.5 fusion
  135.0 1.9 %collective-permute-start.5 = (bf16[128,4096]{1,0:T(8,128)(2,1)S(1)}, bf16[128,4096]{1,0:T(8,128)(2,1)S(1)}, u32[]{:S(2)}, u32[]{:S(2)}) collective-permute-start(bf16[128,4096]{1,0:T(8,128)(2,1)S(1)} %fusion), channel_id=1, source_target_pairs={{0,1},{1,0},{2,3},{3,2},{4,5},{5,4},{6,7},{7,6},{8,9},{9,8},{10,11... | collective-permute-start | bytes 3145736 | tf_op jit(solution)/shard_map/ppermute | solution.py:398
  136.9 0.4 fusion.41
  137.4 2.2 %collective-permute-done.5 = bf16[128,4096]{1,0:T(8,128)(2,1)S(1)} collective-permute-done((bf16[128,4096]{1,0:T(8,128)(2,1)S(1)}, bf16[128,4096]{1,0:T(8,128)(2,1)S(1)}, u32[]{:S(2)}, u32[]{:S(2)}) %collective-permute-start.5) | collective-permute-done | bytes 1048608 | tf_op jit(solution)/shard_map/ppermute | solution.py:398
  139.6 1.6 %add_convert_fusion = bf16[128,4096]{1,0:T(8,128)(2,1)} fusion(bf16[128,4096]{1,0:T(8,128)(2,1)S(1)} %collective-permute-done.5, f32[128,4096]{1,0:T(8,128)S(1)} %fusion.41, bf16[256,4096]{1,0:T(8,128)(2,1)S(1)} %copy-done, bf16[128,384]{1,0:T(8,128)(2,1)S(1)} %bitcast.50), kind=kOutput, calls=%fused_computation.3 | convolution fusion | flops 270532608 | bytes 6356992 | tf_op jit(solution)/shard_map/dot_general | solution.py:393
  141.2 3.5 %all-to-all-start.3 = ((bf16[4,32,4096]{2,1,0:T(8,128)(2,1)}), bf16[4,32,4096]{2,1,0:T(8,128)(2,1)S(1)}, u32[]{:S(2)}, u32[]{:S(2)}) async-start(bf16[4,32,4096]{2,1,0:T(8,128)(2,1)} %bitcast.23), calls=%async_computation.3 | async-start | bytes 2097152 | tf_op jit(solution)/shard_map/all_to_all | solution.py:401
  144.7 0.7 add_multiply_fusion
  145.4 1.6 copy.59
  147.0 13.4 %all-to-all-done.3 = bf16[4,32,4096]{2,1,0:T(8,128)(2,1)S(1)} async-done(((bf16[4,32,4096]{2,1,0:T(8,128)(2,1)}), bf16[4,32,4096]{2,1,0:T(8,128)(2,1)S(1)}, u32[]{:S(2)}, u32[]{:S(2)}) %all-to-all-start.3) | async-done | bytes 1048608 | tf_op jit(solution)/shard_map/all_to_all | solution.py:401
  160.4 0.9 reduce_sum.75
  (68 shorter events, 1.4 us)
Async XLA Ops:
  0.6 133.8 %copy-start = (bf16[256,4096]{1,0:T(8,128)(2,1)S(1)}, bf16[256,4096]{1,0:T(8,128)(2,1)}, u32[]{:S(2)}) copy-start(bf16[256,4096]{1,0:T(8,128)(2,1)} %param.36) | copy-start | bytes 6291460
  4.6 28.4 %all-to-all-start = ((bf16[16,80,128]{2,1,0:T(8,128)(2,1)}), bf16[16,80,128]{2,1,0:T(8,128)(2,1)S(1)}, u32[]{:S(2)}, u32[]{:S(2)}) async-start(bf16[16,80,128]{2,1,0:T(8,128)(2,1)} %broadcast_in_dim.49), calls=%async_computation | async-start | bytes 655360 | tf_op jit(solution)/shard_map/all_to_all | solution.py:272
  21.7 17.0 %copy-start.3 = (bf16[256,512]{1,0:T(8,128)(2,1)S(1)}, bf16[256,512]{1,0:T(8,128)(2,1)}, u32[]{:S(2)}) copy-start(bf16[256,512]{1,0:T(8,128)(2,1)} %param.22) | copy-start | bytes 786436
  21.7 17.0 %copy-start.4 = (bf16[512,384]{1,0:T(8,128)(2,1)S(1)}, bf16[512,384]{1,0:T(8,128)(2,1)}, u32[]{:S(2)}) copy-start(bf16[512,384]{1,0:T(8,128)(2,1)} %param.31) | copy-start | bytes 1179652
  21.7 17.0 %copy-start.11 = (f32[512]{0:T(512)S(1)}, f32[512]{0:T(512)}, u32[]{:S(2)}) copy-start(f32[512]{0:T(512)} %param.26) | copy-start | bytes 6148
  34.2 5.0 %copy-start.17 = (f32[192]{0:T(256)S(1)}, f32[192]{0:T(256)}, u32[]{:S(2)}) copy-start(f32[192]{0:T(256)} %param.29) | copy-start | bytes 2308
  34.2 5.0 %copy-start.12 = (f32[192]{0:T(256)S(1)}, f32[192]{0:T(256)}, u32[]{:S(2)}) copy-start(f32[192]{0:T(256)} %param.28) | copy-start | bytes 2308
  34.2 20.7 %all-to-all-start.1 = ((bf16[4,16,80,128]{3,2,1,0:T(8,128)(2,1)}), bf16[4,16,80,128]{3,2,1,0:T(8,128)(2,1)}, u32[]{:S(2)}, u32[]{:S(2)}) async-start(bf16[4,16,80,128]{3,2,1,0:T(8,128)(2,1)} %broadcast_in_dim.50), calls=%async_computation.1 | async-start | bytes 2621440 | tf_op jit(solution)/shard_map/all_to_all | solution.py:272
  38.7 19.1 %copy-start.9 = (f32[256,32]{0,1:T(8,128)S(1)}, f32[256,32]{0,1:T(8,128)}, u32[]{:S(2)}) copy-start(f32[256,32]{0,1:T(8,128)} %constant.117.clone) | copy-start | bytes 98308
  38.7 19.1 %copy-start.10 = (f32[256,32]{0,1:T(8,128)S(1)}, f32[256,32]{0,1:T(8,128)}, u32[]{:S(2)}) copy-start(f32[256,32]{0,1:T(8,128)} %constant.116.clone) | copy-start | bytes 98308
  38.7 32.7 %copy-start.7 = (bf16[256,256]{1,0:T(8,128)(2,1)S(1)}, bf16[256,256]{1,0:T(8,128)(2,1)}, u32[]{:S(2)}) copy-start(bf16[256,256]{1,0:T(8,128)(2,1)} %param.32) | copy-start | bytes 393220
  38.7 34.0 %copy-start.8 = (f32[2,32,256]{2,1,0:T(8,128)S(1)}, f32[2,32,256]{2,1,0:T(8,128)}, u32[]{:S(2)}) copy-start(f32[2,32,256]{2,1,0:T(8,128)} %constant.118.clone) | copy-start | bytes 196612
  55.0 32.8 %collective-permute-start.1 = (bf16[4,16,80,128]{3,2,1,0:T(8,128)(2,1)}, bf16[4,16,80,128]{3,2,1,0:T(8,128)(2,1)}, u32[]{:S(2)}, u32[]{:S(2)}) collective-permute-start(bf16[4,16,80,128]{3,2,1,0:T(8,128)(2,1)} %all-to-all-done.1.mine_ref), channel_id=1, source_target_pairs={{0,1},{1,0},{2,3},{3,2},{4,5},{5,4},{6,7},{7,6},{8,9},{9,8},{10,11... | collective-permute-start | bytes 3932168 | tf_op jit(solution)/shard_map/ppermute | solution.py:316
  58.1 29.7 %copy-start.5 = (bf16[256,384]{1,0:T(8,128)(2,1)}, bf16[256,384]{1,0:T(8,128)(2,1)S(1)}, u32[]{:S(2)}) copy-start(bf16[256,384]{1,0:T(8,128)(2,1)S(1)} %pad_maximum_fusion.refs_0_) | copy-start | bytes 589828
  58.1 22.8 %collective-permute-start.4 = (bf16[256,384]{1,0:T(8,128)(2,1)S(1)}, bf16[256,384]{1,0:T(8,128)(2,1)S(1)}, u32[]{:S(2)}, u32[]{:S(2)}) collective-permute-start(bf16[256,384]{1,0:T(8,128)(2,1)S(1)} %pad_maximum_fusion.refs_0_), channel_id=1, source_target_pairs={{0,384},{128,0},{256,128},{384,256},{8,392},{136,8},{264,136},{392... | collective-permute-start | bytes 589832 | tf_op jit(solution)/shard_map/ppermute | solution.py:330
  64.3 21.1 %collective-permute-start.3 = (bf16[256,384]{1,0:T(8,128)(2,1)S(1)}, bf16[256,384]{1,0:T(8,128)(2,1)S(1)}, u32[]{:S(2)}, u32[]{:S(2)}) collective-permute-start(bf16[256,384]{1,0:T(8,128)(2,1)S(1)} %pad_maximum_fusion.refs_0_), channel_id=1, source_target_pairs={{0,256},{128,384},{256,0},{384,128},{8,264},{136,392},{264,8},{392... | collective-permute-start | bytes 589832 | tf_op jit(solution)/shard_map/ppermute | solution.py:330
  68.7 19.0 %collective-permute-start.2 = (bf16[256,384]{1,0:T(8,128)(2,1)S(1)}, bf16[256,384]{1,0:T(8,128)(2,1)S(1)}, u32[]{:S(2)}, u32[]{:S(2)}) collective-permute-start(bf16[256,384]{1,0:T(8,128)(2,1)S(1)} %pad_maximum_fusion.refs_0_), channel_id=1, source_target_pairs={{0,128},{128,256},{256,384},{384,0},{8,136},{136,264},{264,392},{3... | collective-permute-start | bytes 589832 | tf_op jit(solution)/shard_map/ppermute | solution.py:330
  80.9 6.9 %copy-start.13 = (bf16[256,384]{1,0:T(8,128)(2,1)}, bf16[256,384]{1,0:T(8,128)(2,1)S(1)}, u32[]{:S(2)}) copy-start(bf16[256,384]{1,0:T(8,128)(2,1)S(1)} %collective-permute-done.4.refs_3_) | copy-start | bytes 589828
  85.4 2.4 %copy-start.14 = (bf16[256,384]{1,0:T(8,128)(2,1)}, bf16[256,384]{1,0:T(8,128)(2,1)S(1)}, u32[]{:S(2)}) copy-start(bf16[256,384]{1,0:T(8,128)(2,1)S(1)} %collective-permute-done.3.refs_2_) | copy-start | bytes 589828
  87.8 0.7 copy-start.15
  88.5 23.6 %copy-start.6 = (bf16[256,256]{1,0:T(8,128)(2,1)S(1)}, bf16[256,256]{1,0:T(8,128)(2,1)}, u32[]{:S(2)}) copy-start(bf16[256,256]{1,0:T(8,128)(2,1)} %param.25) | copy-start | bytes 393220
  88.5 29.1 %copy-start.16 = (bf16[1,256,128]{2,1,0:T(8,128)(2,1)S(1)}, bf16[1,256,128]{2,1,0:T(8,128)(2,1)}, u32[]{:S(2)}) copy-start(bf16[1,256,128]{2,1,0:T(8,128)(2,1)} %param.34) | copy-start | bytes 196612
  88.5 29.2 %copy-start.18 = (f32[128]{0:T(128)S(1)}, f32[128]{0:T(128)}, u32[]{:S(2)}) copy-start(f32[128]{0:T(128)} %param.30) | copy-start | bytes 1540
  104.7 21.8 %all-to-all-start.2 = ((bf16[4,272,256]{2,1,0:T(8,128)(2,1)}), bf16[4,272,256]{2,1,0:T(8,128)(2,1)S(1)}, u32[]{:S(2)}, u32[]{:S(2)}) async-start(bf16[4,272,256]{2,1,0:T(8,128)(2,1)} %attend.1), calls=%async_computation.2 | async-start | bytes 1114112 | tf_op jit(solution)/shard_map/all_to_all | solution.py:356
  112.0 5.5 %collective-permute-start = (bf16[15,256]{1,0:T(8,128)(2,1)S(1)}, bf16[15,256]{1,0:T(8,128)(2,1)S(1)}, u32[]{:S(2)}, u32[]{:S(2)}) collective-permute-start(bf16[15,256]{1,0:T(8,128)(2,1)S(1)} %slice.85), channel_id=1, source_target_pairs={{0,8},{8,16},{16,24},{24,32},{32,40},{40,48},{48,56},{56,64},{64,7... | collective-permute-start | bytes 23048 | tf_op jit(solution)/shard_map/ppermute | solution.py:372
  126.5 0.8 copy-start.2
  129.3 4.7 %copy-start.1 = (bf16[128,4096]{1,0:T(8,128)(2,1)S(1)}, bf16[128,4096]{1,0:T(8,128)(2,1)}, u32[]{:S(2)}) copy-start(bf16[128,4096]{1,0:T(8,128)(2,1)} %param.35) | copy-start | bytes 3145732
  135.0 4.6 %collective-permute-start.5 = (bf16[128,4096]{1,0:T(8,128)(2,1)S(1)}, bf16[128,4096]{1,0:T(8,128)(2,1)S(1)}, u32[]{:S(2)}, u32[]{:S(2)}) collective-permute-start(bf16[128,4096]{1,0:T(8,128)(2,1)S(1)} %fusion), channel_id=1, source_target_pairs={{0,1},{1,0},{2,3},{3,2},{4,5},{5,4},{6,7},{7,6},{8,9},{9,8},{10,11... | collective-permute-start | bytes 3145736 | tf_op jit(solution)/shard_map/ppermute | solution.py:398
  141.2 19.2 %all-to-all-start.3 = ((bf16[4,32,4096]{2,1,0:T(8,128)(2,1)}), bf16[4,32,4096]{2,1,0:T(8,128)(2,1)S(1)}, u32[]{:S(2)}, u32[]{:S(2)}) async-start(bf16[4,32,4096]{2,1,0:T(8,128)(2,1)} %bitcast.23), calls=%async_computation.3 | async-start | bytes 2097152 | tf_op jit(solution)/shard_map/all_to_all | solution.py:401

commit v4 on v3

v4 whole, which is shorter than its diff:
```python
import math

import jax
import jax.numpy as jnp
import numpy as np
from jax import lax
from jax.experimental import pallas as pl
from jax.experimental.pallas import tpu as pltpu
from jax.sharding import PartitionSpec as P


NOPE = 128
ROPE = 64
VD = 128
EPS = 1e-06
THETA = 10000.0
HUGE = 1e30
LOG2E = math.log2(math.e)
LN2 = math.log(2.0)
HALF = 128
Y = 8
PLANES = 8
MEMBERS = 4
VMEM_LIMIT = 32 * 2**20
EXTRA = 16


def turn_tables(block_rows, blocks):
    frequency = 1.0 / THETA ** (np.arange(0, ROPE, 2, dtype=np.float64) / ROPE)
    at_block = (np.arange(blocks) * block_rows)[:, None] * frequency
    within = np.arange(block_rows)[:, None] * frequency
    return [t.astype(np.float32) for a in (at_block, within) for t in (np.cos(a), np.sin(a))]


def row_norm(values, row_gain):
    mean_sq = jnp.mean(values * values, axis=-1, keepdims=True)
    return values * lax.rsqrt(mean_sq + EPS) * row_gain


def make_queries(latent, lat_gain, q_up, norm_gain, key_gain, cosine, sine):
    row_count = latent.shape[0]
    normed = row_norm(latent.astype(jnp.float32), lat_gain).astype(jnp.bfloat16)
    query = jnp.dot(normed, q_up, preferred_element_type=jnp.float32).reshape(
        row_count, -1, NOPE + ROPE
    )
    query = row_norm(query, norm_gain)
    scale = LOG2E * (NOPE + ROPE) ** (-0.5)
    cosine, sine = cosine[:, None, :] * scale, sine[:, None, :] * scale
    a, b = query[..., NOPE : NOPE + ROPE // 2], query[..., NOPE + ROPE // 2 :]
    turned = jnp.concatenate([a * cosine - b * sine, a * sine + b * cosine], axis=-1)
    return jnp.concatenate(
        [
            (query[..., :NOPE] * (key_gain[:NOPE] * scale)).reshape(row_count, -1),
            turned.reshape(row_count, -1),
        ],
        axis=-1,
    ).astype(jnp.bfloat16)


def attend_kernel(place_ref, mine_ref, other_ref, *refs):
    query_refs, refs = refs[:MEMBERS], refs[MEMBERS:]
    key_up_ref, value_up_ref, gain_ref, block_ref, near_ref, far_ref, out_ref, *refs = refs
    q_ref, lat_ref, weight_ref, turn_ref, up_ref, *refs = refs
    heads = key_up_ref.shape[1] // NOPE
    max_refs, sum_refs, acc_refs, key_refs, score_refs, top_refs = (
        refs[n * heads : (n + 1) * heads] for n in range(6)
    )
    count = MEMBERS
    rows = query_refs[0].shape[0]
    parity, own_y, offset, member = place_ref[2], place_ref[3], place_ref[4], place_ref[5]
    width = Y * rows
    slices = [pl.ds(n * 128, 128) for n in range(width // 128)]
    chunk = min(4, Y) * HALF

    for d in range(count):
        q_ref[lax.rem(member + (count - d), count)] = query_refs[d][...]
    for h in range(heads):
        max_refs[h][...] = jnp.full(max_refs[h].shape, -HUGE, jnp.float32)
        sum_refs[h][...] = jnp.zeros_like(sum_refs[h])
        acc_refs[h][...] = jnp.zeros_like(acc_refs[h])
        key_refs[h][NOPE:, :] = jnp.zeros((256 - NOPE, width), jnp.bfloat16)
    up_ref[...] = key_up_ref[...].T
    gain = jnp.broadcast_to(gain_ref[:, NOPE:], (ROPE, ROPE)).T[:, :1]

    def build_keys(step, plane):
        for u, (keys_ref, in_ref) in enumerate(((mine_ref, near_ref), (other_ref, far_ref))):
            for n in range(Y):
                at = pl.ds((u * Y + n) * HALF, HALF)
                for x in range(4):
                    part = keys_ref[x, step * Y + n]
                    if x < 3:
                        lat_ref[x * 80 : (x + 1) * 80, at] = part
                    else:
                        lat_ref[240:256, at] = part[:16]
                        turn_ref[:, at] = part[16:].astype(jnp.float32)

        def turn(u, in_ref):
            for n in range(Y):
                at = pl.ds((u * Y + n) * HALF, HALF)
                in_cos, in_sin = in_ref[0], in_ref[1]
                block_cos = block_ref[plane, : ROPE // 2, n : n + 1]
                block_sin = block_ref[plane, ROPE // 2 :, n : n + 1]
                cosine = block_cos * in_cos - block_sin * in_sin
                sine = block_sin * in_cos + block_cos * in_sin
                raw = turn_ref[:, at]
                square = jnp.sum(raw * raw, axis=0, keepdims=True)
                raw = raw * gain
                a, b = raw[: ROPE // 2], raw[ROPE // 2 :]
                turn_ref[: ROPE // 2, at] = a * cosine - b * sine
                turn_ref[ROPE // 2 :, at] = a * sine + b * cosine
                top_refs[0][n : n + 1, u * 128 : (u + 1) * 128] = square

        for u, in_ref in enumerate((near_ref, far_ref)):
            turn(u, in_ref)
        for n in range(width // chunk):
            at = pl.ds(n * chunk, chunk)
            raw = jnp.dot(up_ref[...], lat_ref[:, at], preferred_element_type=jnp.float32)
            u, first = n * chunk // (Y * HALF), n * chunk % (Y * HALF) // HALF
            rope_sq = jnp.concatenate(
                [top_refs[0][k : k + 1, u * 128 : (u + 1) * 128] for k in range(first, first + chunk // HALF)],
                axis=1,
            )
            for h in range(heads):
                part = raw[h * NOPE : (h + 1) * NOPE]
                square = jnp.sum(part * part, axis=0, keepdims=True) + rope_sq
                inverse = lax.rsqrt(square * (1.0 / (NOPE + ROPE)) + EPS)
                key_refs[h][:NOPE, at] = (part * inverse).astype(jnp.bfloat16)
                key_refs[h][NOPE + h * ROPE : NOPE + (h + 1) * ROPE, at] = (
                    turn_ref[:, at] * inverse
                ).astype(jnp.bfloat16)

    def score(i, h):
        query = jnp.concatenate(
            [q_ref[i, :, h * NOPE : (h + 1) * NOPE], q_ref[i, :, heads * NOPE :]], axis=1
        )
        scores = jnp.dot(query, key_refs[h][...], preferred_element_type=jnp.float32)
        score_refs[h][...] = scores
        top = scores[:, :128]
        for n in range(1, width // 128):
            top = jnp.maximum(top, scores[:, n * 128 : (n + 1) * 128])
        top_refs[h][:, :128] = top

    def mask(h):
        column = lax.broadcasted_iota(jnp.int32, (rows, width), 1)
        row = lax.broadcasted_iota(jnp.int32, (rows, width), 0)
        half_at = jnp.where(column < Y * HALF, offset, HALF - offset)
        key_at = (column % (Y * HALF)) // HALF * rows + half_at + column % HALF
        seen = key_at <= own_y * rows + row
        scores = jnp.where(seen, score_refs[h][...], -HUGE)
        score_refs[h][...] = scores
        top = scores[:, :128]
        for n in range(1, width // 128):
            top = jnp.maximum(top, scores[:, n * 128 : (n + 1) * 128])
        top_refs[h][:, :128] = top

    def weigh(i, h):
        before = max_refs[h][i]
        after = jnp.maximum(before, jnp.max(top_refs[h][:, :128], axis=1, keepdims=True))
        factor = jnp.exp2(before - after)
        total = sum_refs[h][i] * factor
        for at in slices:
            weights = jnp.exp2(score_refs[h][:, at] - after)
            weight_ref[:, at] = weights.astype(jnp.bfloat16)
            total = total + weights
        max_refs[h][i] = after
        sum_refs[h][i] = total
        update = lax.dot_general(
            weight_ref[...],
            lat_ref[...],
            (((1,), (1,)), ((), ())),
            preferred_element_type=jnp.float32,
        )
        acc_refs[h][i] = acc_refs[h][i] * jnp.concatenate([factor, factor], axis=1) + update

    @pl.loop(0, 2)
    def _(step):
        plane = place_ref[step]
        first = lax.div(plane - parity + 1, 2)

        @pl.when(first < count)
        def _():
            build_keys(step, plane)
            score(first, 0)
            own = plane == parity + 2 * first

            @pl.when(own)
            def _():
                for h in range(1, heads):
                    score(first, h)
                for h in range(heads):
                    mask(h)
                for h in range(heads):
                    weigh(first, h)
                score(jnp.minimum(first + 1, count - 1), 0)

            @pl.loop(jnp.where(own, first + 1, first), count)
            def _(i):
                for h in range(heads):
                    if h + 1 < heads:
                        score(i, h + 1)
                    else:
                        score(jnp.minimum(i + 1, count - 1), 0)
                    weigh(i, h)

    @pl.loop(0, count)
    def _(i):
        out_ref[i, rows:, :] = jnp.zeros((EXTRA, heads * VD), out_ref.dtype)
        for h in range(heads):
            total = jnp.sum(sum_refs[h][i], axis=1, keepdims=True)
            seen = total > 0.0
            total = jnp.where(seen, total, 1.0)
            mean = (acc_refs[h][i] * (1.0 / total)).astype(jnp.bfloat16)
            out_ref[i, :rows, h * VD : (h + 1) * VD] = jnp.dot(
                mean, value_up_ref[:, h * VD : (h + 1) * VD], preferred_element_type=jnp.float32
            ).astype(out_ref.dtype)
            level = jnp.where(seen, max_refs[h][i] + jnp.log2(total), -HUGE).T[:1]
            for term in range(3):
                rounded = level.astype(jnp.bfloat16)
                out_ref[i, pl.ds(rows + h * 3 + term, 1), :] = rounded
                level = level - rounded.astype(jnp.float32)


def attend(place, mine, other, queries, key_up, value_up, gain, block_table, near, far):
    rows, channels = queries[0].shape
    heads = key_up.shape[1] // NOPE
    vmem = pl.BlockSpec(memory_space=pltpu.VMEM)
    wide = [
        pltpu.VMEM((MEMBERS, rows, 128), jnp.float32),
        pltpu.VMEM((MEMBERS, rows, 128), jnp.float32),
        pltpu.VMEM((MEMBERS, rows, 256), jnp.float32),
        pltpu.VMEM((256, Y * rows), jnp.bfloat16),
        pltpu.VMEM((rows, Y * rows), jnp.float32),
        pltpu.VMEM((rows, 256), jnp.float32),
    ]
    return pl.pallas_call(
        attend_kernel,
        out_shape=jax.ShapeDtypeStruct((MEMBERS, rows + EXTRA, heads * VD), jnp.bfloat16),
        in_specs=[pl.BlockSpec(memory_space=pltpu.SMEM)] + [vmem] * (8 + MEMBERS),
        out_specs=vmem,
        scratch_shapes=[
            pltpu.VMEM((MEMBERS, rows, channels), jnp.bfloat16),
            pltpu.VMEM((256, Y * rows), jnp.bfloat16),
            pltpu.VMEM((rows, Y * rows), jnp.bfloat16),
            pltpu.VMEM((ROPE, Y * rows), jnp.float32),
            pltpu.VMEM(key_up.shape[::-1], jnp.bfloat16),
            *[s for s in wide for _ in range(heads)],
        ],
        compiler_params=pltpu.CompilerParams(vmem_limit_bytes=VMEM_LIMIT),
        cost_estimate=pl.CostEstimate(
            flops=5 * 2 * rows * Y * rows * heads * 512,
            bytes_accessed=mine.size * 4,
            transcendentals=5 * rows * Y * rows * heads,
        ),
        name="attend",
    )(place, mine, other, *queries, key_up, value_up, gain, block_table, near, far)


def share_kernel(place_ref, latent_ref, rope_ref, gain_ref, out_ref, all_ref):
    latent = latent_ref[...].astype(jnp.float32)
    normed = row_norm(latent, gain_ref[...]).astype(jnp.bfloat16)
    all_ref[: latent.shape[1]] = normed.T
    all_ref[latent.shape[1] :] = rope_ref[...].T
    own = all_ref[pl.ds(pl.multiple_of(place_ref[1] * 80, 16), 80), :]
    for n in range(out_ref.shape[0]):
        out_ref[n] = own


def key_share(place, latent, rope, gain, count):
    channels = latent.shape[1] + rope.shape[1]
    return pl.pallas_call(
        share_kernel,
        out_shape=jax.ShapeDtypeStruct((count, 80, HALF), jnp.bfloat16),
        grid_spec=pltpu.PrefetchScalarGridSpec(
            num_scalar_prefetch=1,
            grid=(1,),
            in_specs=[
                pl.BlockSpec((HALF, latent.shape[1]), lambda i, w: (w[0], 0)),
                pl.BlockSpec((HALF, rope.shape[1]), lambda i, w: (w[0], 0)),
                pl.BlockSpec((1, latent.shape[1]), lambda i, w: (0, 0)),
            ],
            out_specs=pl.BlockSpec((count, 80, HALF), lambda i, w: (0, 0, 0)),
            scratch_shapes=[pltpu.VMEM((channels, HALF), jnp.bfloat16)],
        ),
        cost_estimate=pl.CostEstimate(flops=10**6, bytes_accessed=10**6, transcendentals=HALF),
        compiler_params=pltpu.CompilerParams(vmem_limit_bytes=4 * 2**20),
        name="key_share",
    )(place, latent, rope, gain[None])


def merge_kernel(parts_ref, out_ref, log_ref, turn_ref):
    count, rows = parts_ref.shape[0], out_ref.shape[0]
    heads = out_ref.shape[1] // VD
    turn_ref[...] = jnp.zeros_like(turn_ref)
    for h in range(heads):
        levels = []
        for i in range(count):
            terms = [
                parts_ref[i, rows : rows + EXTRA, :].astype(jnp.float32)[h * 3 + k : h * 3 + k + 1]
                for k in range(3)
            ]
            levels.append(terms[0] + terms[1] + terms[2])
        top = levels[0]
        for level in levels[1:]:
            top = jnp.maximum(top, level)
        shares = [jnp.exp2(level - top) for level in levels]
        total = shares[0]
        for share in shares[1:]:
            total = total + share
        log_ref[h : h + 1, :] = (top + jnp.log2(total)) * LN2
        inverse = 1.0 / total
        for i in range(count):
            turn_ref[h * count + i : h * count + i + 1, :] = shares[i] * inverse
    turned = turn_ref[...].T
    for h in range(heads):
        merged = jnp.zeros((rows, VD), jnp.float32)
        for i in range(count):
            k = h * count + i
            part = parts_ref[i, :rows, h * VD : (h + 1) * VD].astype(jnp.float32)
            merged = merged + part * turned[:, k : k + 1]
        out_ref[:, h * VD : (h + 1) * VD] = merged.astype(out_ref.dtype)


def merge(parts):
    _, rows, channels = parts.shape
    rows -= EXTRA
    vmem = pl.BlockSpec(memory_space=pltpu.VMEM)
    return pl.pallas_call(
        merge_kernel,
        out_shape=[
            jax.ShapeDtypeStruct((rows, channels), jnp.bfloat16),
            jax.ShapeDtypeStruct((channels // VD, rows), jnp.float32),
        ],
        in_specs=[vmem],
        out_specs=[vmem, vmem],
        scratch_shapes=[pltpu.VMEM((128, rows), jnp.float32)],
        cost_estimate=pl.CostEstimate(flops=10**6, bytes_accessed=10**6, transcendentals=10**4),
        compiler_params=pltpu.CompilerParams(vmem_limit_bytes=8 * 2**20),
        name="merge",
    )(parts)


def to_all(value, axis):
    count = lax.axis_size(axis)
    return lax.all_to_all(jnp.broadcast_to(value[None], (count, *value.shape)), axis, 0, 0)


def local(
    q_latent,
    kv_latent,
    key_rope,
    pool_input,
    q_lat_gain,
    kv_lat_gain,
    q_head_gain,
    k_head_gain,
    pool_gain,
    q_up,
    key_up,
    value_up,
    pool_mix,
    out_pool,
    out_attn,
):
    row_count = q_latent.shape[0]
    sp_index = lax.axis_index("sp")
    sp_size = lax.axis_size("sp")
    core = lax.axis_index("tp")
    line = lax.axis_index("fs")
    z, y = lax.div(sp_index, Y), lax.rem(sp_index, Y)
    own_pos = sp_index * row_count + jnp.arange(row_count, dtype=jnp.int32)
    key_groups = [
        [p * Y + n for p in (j, PLANES - 1 - j) for n in range(Y)] for j in range(PLANES // 2)
    ]
    query_groups = [
        [(c + 2 * i) * Y + n for i in range(MEMBERS)] for c in range(2) for n in range(Y)
    ]
    block_cos, block_sin, in_cos, in_sin = turn_tables(row_count, sp_size)
    plane_turns = np.transpose(
        np.concatenate([block_cos, block_sin], axis=1).reshape(-1, Y, ROPE), (0, 2, 1)
    )

    share = key_share(
        jnp.stack([core, line]).astype(jnp.int32), kv_latent, key_rope, kv_lat_gain, 2 * Y
    )
    mine = lax.all_to_all(share, "sp", 0, 0, axis_index_groups=key_groups)
    mine = to_all(mine, "fs")
    other = lax.ppermute(mine, "tp", [(0, 1), (1, 0)])

    own_cos = lax.dynamic_slice_in_dim(jnp.asarray(block_cos), sp_index, 1, 0)
    own_sin = lax.dynamic_slice_in_dim(jnp.asarray(block_sin), sp_index, 1, 0)
    queries = make_queries(
        q_latent,
        q_lat_gain,
        q_up,
        q_head_gain,
        k_head_gain,
        own_cos * in_cos - own_sin * in_sin,
        own_sin * in_cos + own_cos * in_sin,
    )

    def turned(d):
        pairs = [(g[i], g[(i + d) % MEMBERS]) for g in query_groups for i in range(MEMBERS)]
        return lax.ppermute(queries, "sp", pairs)

    queries = [queries] + [turned(d) for d in range(1, MEMBERS)]
    within = jnp.asarray(np.stack([in_cos.T, in_sin.T]))
    near = lax.dynamic_slice_in_dim(within, core * HALF, HALF, 2)
    far = lax.dynamic_slice_in_dim(within, HALF - core * HALF, HALF, 2)
    low_plane = jnp.minimum(z, PLANES - 1 - z)
    place = jnp.stack(
        [low_plane, PLANES - 1 - low_plane, lax.rem(z, 2), y, core * HALF, lax.div(z, 2)]
    ).astype(jnp.int32)
    partial_out = attend(
        place,
        mine,
        other,
        queries,
        key_up,
        value_up,
        k_head_gain[None],
        jnp.asarray(plane_turns),
        near,
        far,
    )
    parts = lax.all_to_all(partial_out, "sp", 0, 0, axis_index_groups=query_groups)
    attended, log_weight = merge(parts)

    earlier = lax.ppermute(
        pool_input[row_count - 15 :], "sp", [(i, i + 1) for i in range(sp_size - 1)]
    )
    extended = jnp.concatenate([earlier, pool_input], axis=0).astype(jnp.float32)
    window = jnp.left_shift(jnp.int32(2), line)
    window_sum = jnp.zeros((row_count, pool_input.shape[1]), jnp.float32)
    for lag_rows in range(16):
        window_sum = window_sum + jnp.where(
            lag_rows < window, extended[15 - lag_rows : 15 - lag_rows + row_count], 0.0
        )
    counts = jnp.minimum(own_pos + 1, window).astype(jnp.float32)[:, None]
    pool_diff = (window_sum / counts - extended[15:]).astype(jnp.bfloat16)
    pooled = (
        jnp.dot(pool_diff, pool_mix[0], preferred_element_type=jnp.float32) * pool_gain
    ).astype(jnp.bfloat16)

    lines = lax.axis_size("fs")
    channels = jnp.concatenate([pooled, attended], axis=1).reshape(
        lines, 2, -1, pooled.shape[1] + attended.shape[1]
    )

    def projected(rows):
        rows = rows.reshape(-1, rows.shape[-1])
        return jnp.dot(rows[:, :128], out_pool, preferred_element_type=jnp.float32) + jnp.dot(
            rows[:, 128:], out_attn, preferred_element_type=jnp.float32
        )

    sent = projected(lax.dynamic_index_in_dim(channels, 1 - core, 1, False)).astype(jnp.bfloat16)
    received = lax.ppermute(sent, "tp", [(0, 1), (1, 0)])
    kept = projected(lax.dynamic_index_in_dim(channels, core, 1, False))
    chip = (kept + received.astype(jnp.float32)).astype(jnp.bfloat16)
    chip = lax.all_to_all(chip.reshape(lines, -1, chip.shape[1]), "fs", 0, 0)
    mixed = jnp.sum(chip.astype(jnp.float32), axis=0).astype(jnp.bfloat16)
    return (mixed, log_weight)


def solution(mesh):
    in_specs = (
        P("sp", None),
        P("sp", None),
        P("sp", None),
        P("sp", "fs"),
        P(),
        P(),
        P(),
        P(),
        P(("fs", "tp")),
        P(None, ("fs", "tp")),
        P(None, ("fs", "tp")),
        P(None, ("fs", "tp")),
        P("fs", None, "tp"),
        P(("fs", "tp"), None),
        P(("fs", "tp"), None),
    )
    out_specs = (P(("sp", "fs", "tp"), None), P(("fs", "tp"), "sp"))

    return jax.shard_map(local, mesh=mesh, in_specs=in_specs, out_specs=out_specs, check_vma=False)
```

time: 162 us -> 161 us (level)
  blocking collectives: 0 us -> 18.1 us
  waiting for transfers between devices: 68.4 us -> 52.8 us
  starting transfers between devices: 49.6 us -> 44.6 us
  other arithmetic: 6.85 us -> 9.67 us
  local copies, waits for them, and re-layouts: 14.9 us -> 12.1 us
  matrix products: 4.1 us -> 6.34 us
    all_to_all x0 -> x1, blocking collectives: none -> 18.1 us  [local(): chip = lax.all_to_all(chip.reshape(lines, -1, chip.shape[1]), 'fs', 0, 0)]
    all_to_all x2 -> x1, starting transfers between devices: 20.5 us -> 4.42 us  [to_all(): lax.all_to_all(jnp.broadcast_to(value[None], (count, *value.shape)), axis...]
    all_to_all x2 -> x1, waiting for transfers between devices: 26.9 us -> 13.5 us  [to_all(): lax.all_to_all(jnp.broadcast_to(value[None], (count, *value.shape)), axis...]
    all_to_all x1, starting transfers between devices: 3.51 us -> 16 us  [local(): mine = lax.all_to_all(share, 'sp', 0, 0, axis_index_groups=key_groups)]
    mul x2 -> x0, local copies, waits for them, and re-layouts: 5.15 us -> none  [local(): parts[:, :row_count].reshape(MEMBERS, row_count, head_count, VD)]
    pallas_call x1, Pallas kernels: 16.2 us -> 12.6 us  [attend(): pl.pallas_call(attend_kernel, out_shape=jax.ShapeDtypeStruct((MEMBERS, ro...]
    another operation x2 -> x3, other arithmetic: 0.11 us -> 2.68 us
    pallas_call x0 -> x2, Pallas kernels: none -> 2.48 us  [the longest x1 1.49 us: key_share(): pl.pallas_call(share_kernel, out_shape=jax.ShapeDtypeStruct((count, 80, H...]
  transfers between devices with their start and end apart: 10 -> 9, of which waited for: 9 -> 8; matrix products, arithmetic and copies ran while one was open for 6% -> 11% of each run, Pallas kernels for 0% -> 0%
where the time goes in v4:
time: 161 us; the launch traced here: 160 us
  waiting for transfers between devices  52.8 us (33%)
  starting transfers between devices  44.6 us (28%)
  blocking collectives  18.1 us (11%)
  Pallas kernels  15 us (9%)
  local copies, waits for them, and re-layouts  12.1 us (8%)
  other arithmetic  9.67 us (6%)
  matrix products  6.34 us (4%)
    all_to_all x1, blocking collectives, local(): chip = lax.all_to_all(chip.reshape(lines, -1, chip.shape[1]), 'fs', 0, 0)  18.1 us
    ppermute x3, waiting for transfers between devices, turned(): return lax.ppermute(queries, 'sp', pairs)  16.5 us
    all_to_all x1, starting transfers between devices, local(): mine = lax.all_to_all(share, 'sp', 0, 0, axis_index_groups=key_groups)  16 us
    all_to_all x1, waiting for transfers between devices, to_all(): lax.all_to_all(jnp.broadcast_to(value[None], (count, *value.shape)), axis...  13.5 us
    pallas_call x1, Pallas kernels, attend(): pl.pallas_call(attend_kernel, out_shape=jax.ShapeDtypeStruct((MEMBERS, ro...  12.6 us
    ppermute x3, starting transfers between devices, turned(): return lax.ppermute(queries, 'sp', pairs)  12.5 us
    all_to_all x1, waiting for transfers between devices, local(): mine = lax.all_to_all(share, 'sp', 0, 0, axis_index_groups=key_groups)  11.3 us
    all_to_all x1, starting transfers between devices, local(): lax.all_to_all(partial_out, 'sp', 0, 0, axis_index_groups=query_groups)  5.83 us
  transfers between devices with their start and end apart: 9, of which 8 were waited for; matrix products, arithmetic and copies ran while one was open for 11% of the time, Pallas kernels for 0%

profile of v4, /device:TPU:8, one launch (start us, length us, event | category | flops | bytes accessed | tf_op | source)
XLA Modules:
  0.0 159.6 jit_solution(1814862154745536130)
XLA Ops:
  0.7 1.0 copy.26.rope_ref
  1.8 0.9 copy-done.2
  2.7 0.7 copy-done.3
  3.3 1.5 key_share.1
  4.8 16.0 %all-to-all-start = ((bf16[16,80,128]{2,1,0:T(8,128)(2,1)}), bf16[16,80,128]{2,1,0:T(8,128)(2,1)S(1)}, u32[]{:S(2)}, u32[]{:S(2)}) async-start(bf16[16,80,128]{2,1,0:T(8,128)(2,1)} %key_share.1), calls=%async_computation | async-start | bytes 655360 | tf_op jit(solution)/shard_map/all_to_all | solution.py:385
  20.9 1.1 fusion.2
  22.0 11.3 %all-to-all-done = bf16[16,80,128]{2,1,0:T(8,128)(2,1)S(1)} async-done(((bf16[16,80,128]{2,1,0:T(8,128)(2,1)}), bf16[16,80,128]{2,1,0:T(8,128)(2,1)S(1)}, u32[]{:S(2)}, u32[]{:S(2)}) %all-to-all-start) | async-done | bytes 327712 | tf_op jit(solution)/shard_map/all_to_all | solution.py:385
  33.2 1.2 broadcast_in_dim.42
  34.5 4.4 %all-to-all-start.1 = ((bf16[4,16,80,128]{3,2,1,0:T(8,128)(2,1)}), bf16[4,16,80,128]{3,2,1,0:T(8,128)(2,1)S(1)}, u32[]{:S(2)}, u32[]{:S(2)}) async-start(bf16[4,16,80,128]{3,2,1,0:T(8,128)(2,1)} %broadcast_in_dim.42), calls=%async_computation.1 | async-start | bytes 2621440 | tf_op jit(solution)/shard_map/all_to_all | solution.py:344
  38.9 1.5 fusion.5
  40.5 0.8 multiply_multiply_fusion
  41.4 13.5 %all-to-all-done.1.mine_ref = bf16[4,16,80,128]{3,2,1,0:T(8,128)(2,1)S(1)} async-done(((bf16[4,16,80,128]{3,2,1,0:T(8,128)(2,1)}), bf16[4,16,80,128]{3,2,1,0:T(8,128)(2,1)S(1)}, u32[]{:S(2)}, u32[]{:S(2)}) %all-to-all-start.1) | async-done | bytes 1310752 | tf_op jit(solution)/shard_map/all_to_all | solution.py:344
  54.9 1.9 %collective-permute-start.1 = (bf16[4,16,80,128]{3,2,1,0:T(8,128)(2,1)S(1)}, bf16[4,16,80,128]{3,2,1,0:T(8,128)(2,1)}, u32[]{:S(2)}, u32[]{:S(2)}) collective-permute-start(bf16[4,16,80,128]{3,2,1,0:T(8,128)(2,1)S(1)} %all-to-all-done.1.mine_ref), channel_id=1, source_target_pairs={{0,1},{1,0},{2,3},{3,2},{4,5},{5,4},{6,7},{7,6},{8,9},{9,8},{10,11... | collective-permute-start | bytes 3932168 | tf_op jit(solution)/shard_map/ppermute | solution.py:387
  56.8 1.7 %fusion.7 = bf16[256,2,128]{0,2,1:T(8,128)(2,1)} fusion(f32[256,2,192]{0,2,1:T(8,128)} %multiply_multiply_fusion, f32[128]{0:T(128)S(1)} %slice_multiply_fusion.1), kind=kLoop, calls=%fused_computation.15 | loop fusion | flops 131072 | bytes 393728 | tf_op jit(solution)/shard_map/convert.6
  58.5 1.7 %copy.32 = bf16[256,256]{1,0:T(8,128)(2,1)} copy(bf16[256,256]{0,1:T(8,128)(2,1)} %bitcast.35) | data formatting | bytes 262144 | tf_op jit(solution)/shard_map/reshape | solution.py:53
  60.2 0.7 fusion.38
  60.9 0.9 subtract_multiply_fusion
  61.8 0.9 subtract_convert_fusion
  62.7 0.6 pad_maximum_fusion.2
  63.3 1.6 copy.29
  64.9 1.6 %pad_maximum_fusion.refs_0_ = bf16[256,384]{1,0:T(8,128)(2,1)} fusion(bf16[256,128]{1,0:T(8,128)(2,1)} %copy.29, bf16[256,256]{1,0:T(8,128)(2,1)} %copy.32), kind=kLoop, calls=%fused_computation.51 | loop fusion | flops 393216 | bytes 393216 | tf_op jit(solution)/shard_map/concatenate | solution.py:51
  66.5 6.2 %collective-permute-start.4 = (bf16[256,384]{1,0:T(8,128)(2,1)}, bf16[256,384]{1,0:T(8,128)(2,1)}, u32[]{:S(2)}, u32[]{:S(2)}) collective-permute-start(bf16[256,384]{1,0:T(8,128)(2,1)} %pad_maximum_fusion.refs_0_), channel_id=1, source_target_pairs={{0,384},{128,0},{256,128},{384,256},{8,392},{136,8},{264,136},{392... | collective-permute-start | bytes 589832 | tf_op jit(solution)/shard_map/ppermute | solution.py:403
  72.7 4.4 %collective-permute-start.3 = (bf16[256,384]{1,0:T(8,128)(2,1)}, bf16[256,384]{1,0:T(8,128)(2,1)}, u32[]{:S(2)}, u32[]{:S(2)}) collective-permute-start(bf16[256,384]{1,0:T(8,128)(2,1)} %pad_maximum_fusion.refs_0_), channel_id=1, source_target_pairs={{0,256},{128,384},{256,0},{384,128},{8,264},{136,392},{264,8},{392... | collective-permute-start | bytes 589832 | tf_op jit(solution)/shard_map/ppermute | solution.py:403
  77.1 1.9 %collective-permute-start.2 = (bf16[256,384]{1,0:T(8,128)(2,1)}, bf16[256,384]{1,0:T(8,128)(2,1)}, u32[]{:S(2)}, u32[]{:S(2)}) collective-permute-start(bf16[256,384]{1,0:T(8,128)(2,1)} %pad_maximum_fusion.refs_0_), channel_id=1, source_target_pairs={{0,128},{128,256},{256,384},{384,0},{8,136},{136,264},{264,392},{3... | collective-permute-start | bytes 589832 | tf_op jit(solution)/shard_map/ppermute | solution.py:403
  79.2 0.8 constant_dynamic-slice_fusion.2
  80.0 9.7 %collective-permute-done.4.refs_3_ = bf16[256,384]{1,0:T(8,128)(2,1)} collective-permute-done((bf16[256,384]{1,0:T(8,128)(2,1)}, bf16[256,384]{1,0:T(8,128)(2,1)}, u32[]{:S(2)}, u32[]{:S(2)}) %collective-permute-start.4) | collective-permute-done | bytes 196640 | tf_op jit(solution)/shard_map/ppermute | solution.py:403
  89.6 4.5 %collective-permute-done.3.refs_2_ = bf16[256,384]{1,0:T(8,128)(2,1)} collective-permute-done((bf16[256,384]{1,0:T(8,128)(2,1)}, bf16[256,384]{1,0:T(8,128)(2,1)}, u32[]{:S(2)}, u32[]{:S(2)}) %collective-permute-start.3) | collective-permute-done | bytes 196640 | tf_op jit(solution)/shard_map/ppermute | solution.py:403
  94.1 2.4 %collective-permute-done.2.refs_1_ = bf16[256,384]{1,0:T(8,128)(2,1)} collective-permute-done((bf16[256,384]{1,0:T(8,128)(2,1)}, bf16[256,384]{1,0:T(8,128)(2,1)}, u32[]{:S(2)}, u32[]{:S(2)}) %collective-permute-start.2) | collective-permute-done | bytes 196640 | tf_op jit(solution)/shard_map/ppermute | solution.py:403
  96.5 0.9 copy-done.5
  97.4 0.9 copy-done.7
  98.4 12.6 %attend.1 = bf16[4,272,256]{2,1,0:T(8,128)(2,1)S(1)} custom-call(s32[6]{0:T(128)S(1)} %stack.36.place_ref, bf16[4,16,80,128]{3,2,1,0:T(8,128)(2,1)S(1)} %all-to-all-done.1.mine_ref, bf16[4,16,80,128]{3,2,1,0:T(8,128)(2,1)} %collective-permute-done.1.other_ref, bf16[256,384]{1,0:T(8,128)(2,1)} %pad_maximum_fusion.refs_0_, ...), custom_call_target="tpu_custom_call" | custom-call | flops 5368709120 | bytes 2621440 | tf_op jit(solution)/shard_map/attend/pallas_call | solution.py:235
  111.0 0.8 copy-done.1
  111.8 5.8 %all-to-all-start.2 = ((bf16[4,272,256]{2,1,0:T(8,128)(2,1)}), bf16[4,272,256]{2,1,0:T(8,128)(2,1)S(1)}, u32[]{:S(2)}, u32[]{:S(2)}) async-start(bf16[4,272,256]{2,1,0:T(8,128)(2,1)} %copy-done.1), calls=%async_computation.2 | async-start | bytes 1114112 | tf_op jit(solution)/shard_map/all_to_all | solution.py:425
  117.6 0.7 slice.76
  118.3 1.9 %collective-permute-start = (bf16[15,256]{1,0:T(8,128)(2,1)S(1)}, bf16[15,256]{1,0:T(8,128)(2,1)S(1)}, u32[]{:S(2)}, u32[]{:S(2)}) collective-permute-start(bf16[15,256]{1,0:T(8,128)(2,1)S(1)} %slice.76), channel_id=1, source_target_pairs={{0,8},{8,16},{16,24},{24,32},{32,40},{40,48},{48,56},{56,64},{64,7... | collective-permute-start | bytes 23048 | tf_op jit(solution)/shard_map/ppermute | solution.py:428
  120.3 3.6 %collective-permute-done = bf16[15,256]{1,0:T(8,128)(2,1)S(1)} collective-permute-done((bf16[15,256]{1,0:T(8,128)(2,1)S(1)}, bf16[15,256]{1,0:T(8,128)(2,1)S(1)}, u32[]{:S(2)}, u32[]{:S(2)}) %collective-permute-start) | collective-permute-done | bytes 7712 | tf_op jit(solution)/shard_map/ppermute | solution.py:428
  123.8 0.9 maximum_convert_fusion
  124.8 1.6 %fusion.1 = bf16[256,128]{1,0:T(8,128)(2,1)S(1)} fusion(f32[271,256]{1,0:T(8,128)S(1)} %maximum_convert_fusion, f32[256]{0:T(256)S(1)} %minimum_convert_fusion, pred[]{:T(512)S(6)} %gt.63, pred[]{:T(512)S(6)} %gt.62, pred[]{:T(512)S(6)} %gt.61, pred[]{:T(512)S(6)} %gt.60, pred[]{:T(512)S(6)} %gt.59, pred[]{:T(512)S(6)} %gt.58, pred[]{:T(512)S(6)} %gt.57, ...), kind=kOutput, calls=%fused_computation.5 | convolution fusion | flops 19070976 | bytes 4326928 | tf_op jit(solution)/shard_map/dot_general | solution.py:441
  126.4 5.7 %all-to-all-done.2.parts_ref = bf16[4,272,256]{2,1,0:T(8,128)(2,1)S(1)} async-done(((bf16[4,272,256]{2,1,0:T(8,128)(2,1)}), bf16[4,272,256]{2,1,0:T(8,128)(2,1)S(1)}, u32[]{:S(2)}, u32[]{:S(2)}) %all-to-all-start.2) | async-done | bytes 557088 | tf_op jit(solution)/shard_map/all_to_all | solution.py:425
  132.1 1.0 merge.1
  133.2 1.6 %fusion.34 = f32[128,4096]{1,0:T(8,128)S(1)} fusion(bf16[128,4096]{1,0:T(8,128)(2,1)} %param.34, bf16[128,384]{1,0:T(8,128)(2,1)S(1)} %bitcast.38), kind=kOutput, calls=%fused_computation.60 | convolution fusion | flops 134217728 | bytes 3178496 | tf_op jit(solution)/shard_map/dot_general | solution.py:451
  134.8 0.5 fusion
  135.4 1.9 %collective-permute-start.5 = (bf16[128,4096]{1,0:T(8,128)(2,1)S(1)}, bf16[128,4096]{1,0:T(8,128)(2,1)S(1)}, u32[]{:S(2)}, u32[]{:S(2)}) collective-permute-start(bf16[128,4096]{1,0:T(8,128)(2,1)S(1)} %fusion), channel_id=1, source_target_pairs={{0,1},{1,0},{2,3},{3,2},{4,5},{5,4},{6,7},{7,6},{8,9},{9,8},{10,11... | collective-permute-start | bytes 3145736 | tf_op jit(solution)/shard_map/ppermute | solution.py:456
  137.3 0.4 fusion.36
  137.7 2.2 %collective-permute-done.5 = bf16[128,4096]{1,0:T(8,128)(2,1)S(1)} collective-permute-done((bf16[128,4096]{1,0:T(8,128)(2,1)S(1)}, bf16[128,4096]{1,0:T(8,128)(2,1)S(1)}, u32[]{:S(2)}, u32[]{:S(2)}) %collective-permute-start.5) | collective-permute-done | bytes 1048608 | tf_op jit(solution)/shard_map/ppermute | solution.py:456
  139.9 0.6 add_convert_fusion
  140.6 18.1 %all_to_all.20 = bf16[4,32,4096]{2,1,0:T(8,128)(2,1)S(1)} all-to-all(bf16[4,32,4096]{2,1,0:T(8,128)(2,1)S(1)} %bitcast.31), channel_id=1, replica_groups=mesh['sp'=64,'fs'=4,'tp'=2] {'fs'}, dimensions={0} | all-to-all | bytes 2097152 | tf_op jit(solution)/shard_map/all_to_all | solution.py:459
  158.7 0.9 reduce_sum.32
  (29 shorter events, 0.3 us)
Async XLA Ops:
  0.6 134.2 %copy-start = (bf16[256,4096]{1,0:T(8,128)(2,1)S(1)}, bf16[256,4096]{1,0:T(8,128)(2,1)}, u32[]{:S(2)}) copy-start(bf16[256,4096]{1,0:T(8,128)(2,1)} %param.35) | copy-start | bytes 6291460
  1.8 0.9 copy-start.2
  2.7 0.7 copy-start.3
  4.8 28.4 %all-to-all-start = ((bf16[16,80,128]{2,1,0:T(8,128)(2,1)}), bf16[16,80,128]{2,1,0:T(8,128)(2,1)S(1)}, u32[]{:S(2)}, u32[]{:S(2)}) async-start(bf16[16,80,128]{2,1,0:T(8,128)(2,1)} %key_share.1), calls=%async_computation | async-start | bytes 655360 | tf_op jit(solution)/shard_map/all_to_all | solution.py:385
  21.9 17.0 %copy-start.9 = (f32[512]{0:T(512)S(1)}, f32[512]{0:T(512)}, u32[]{:S(2)}) copy-start(f32[512]{0:T(512)} %param.25) | copy-start | bytes 6148
  34.5 6.0 %copy-start.10 = (f32[192]{0:T(256)S(1)}, f32[192]{0:T(256)}, u32[]{:S(2)}) copy-start(f32[192]{0:T(256)} %param.27) | copy-start | bytes 2308
  34.5 22.3 %copy-start.6 = (f32[192]{0:T(256)S(1)}, f32[192]{0:T(256)}, u32[]{:S(2)}) copy-start(f32[192]{0:T(256)} %param.28) | copy-start | bytes 2308
  34.5 20.4 %all-to-all-start.1 = ((bf16[4,16,80,128]{3,2,1,0:T(8,128)(2,1)}), bf16[4,16,80,128]{3,2,1,0:T(8,128)(2,1)S(1)}, u32[]{:S(2)}, u32[]{:S(2)}) async-start(bf16[4,16,80,128]{3,2,1,0:T(8,128)(2,1)} %broadcast_in_dim.42), calls=%async_computation.1 | async-start | bytes 2621440 | tf_op jit(solution)/shard_map/all_to_all | solution.py:344
  38.9 57.6 %copy-start.4 = (bf16[256,256]{1,0:T(8,128)(2,1)S(1)}, bf16[256,256]{1,0:T(8,128)(2,1)}, u32[]{:S(2)}) copy-start(bf16[256,256]{1,0:T(8,128)(2,1)} %refs_4_.1) | copy-start | bytes 393220
  54.9 41.6 %collective-permute-start.1 = (bf16[4,16,80,128]{3,2,1,0:T(8,128)(2,1)S(1)}, bf16[4,16,80,128]{3,2,1,0:T(8,128)(2,1)}, u32[]{:S(2)}, u32[]{:S(2)}) collective-permute-start(bf16[4,16,80,128]{3,2,1,0:T(8,128)(2,1)S(1)} %all-to-all-done.1.mine_ref), channel_id=1, source_target_pairs={{0,1},{1,0},{2,3},{3,2},{4,5},{5,4},{6,7},{7,6},{8,9},{9,8},{10,11... | collective-permute-start | bytes 3932168 | tf_op jit(solution)/shard_map/ppermute | solution.py:387
  66.5 23.1 %collective-permute-start.4 = (bf16[256,384]{1,0:T(8,128)(2,1)}, bf16[256,384]{1,0:T(8,128)(2,1)}, u32[]{:S(2)}, u32[]{:S(2)}) collective-permute-start(bf16[256,384]{1,0:T(8,128)(2,1)} %pad_maximum_fusion.refs_0_), channel_id=1, source_target_pairs={{0,384},{128,0},{256,128},{384,256},{8,392},{136,8},{264,136},{392... | collective-permute-start | bytes 589832 | tf_op jit(solution)/shard_map/ppermute | solution.py:403
  72.7 21.4 %collective-permute-start.3 = (bf16[256,384]{1,0:T(8,128)(2,1)}, bf16[256,384]{1,0:T(8,128)(2,1)}, u32[]{:S(2)}, u32[]{:S(2)}) collective-permute-start(bf16[256,384]{1,0:T(8,128)(2,1)} %pad_maximum_fusion.refs_0_), channel_id=1, source_target_pairs={{0,256},{128,384},{256,0},{384,128},{8,264},{136,392},{264,8},{392... | collective-permute-start | bytes 589832 | tf_op jit(solution)/shard_map/ppermute | solution.py:403
  77.1 19.4 %collective-permute-start.2 = (bf16[256,384]{1,0:T(8,128)(2,1)}, bf16[256,384]{1,0:T(8,128)(2,1)}, u32[]{:S(2)}, u32[]{:S(2)}) collective-permute-start(bf16[256,384]{1,0:T(8,128)(2,1)} %pad_maximum_fusion.refs_0_), channel_id=1, source_target_pairs={{0,128},{128,256},{256,384},{384,0},{8,136},{136,264},{264,392},{3... | collective-permute-start | bytes 589832 | tf_op jit(solution)/shard_map/ppermute | solution.py:403
  96.5 0.9 copy-start.5
  97.4 0.9 copy-start.7
  98.4 26.4 %copy-start.11 = (f32[128]{0:T(128)S(1)}, f32[128]{0:T(128)}, u32[]{:S(2)}) copy-start(f32[128]{0:T(128)} %param.29) | copy-start | bytes 1540
  110.9 0.8 copy-start.1
  111.8 20.4 %all-to-all-start.2 = ((bf16[4,272,256]{2,1,0:T(8,128)(2,1)}), bf16[4,272,256]{2,1,0:T(8,128)(2,1)S(1)}, u32[]{:S(2)}, u32[]{:S(2)}) async-start(bf16[4,272,256]{2,1,0:T(8,128)(2,1)} %copy-done.1), calls=%async_computation.2 | async-start | bytes 1114112 | tf_op jit(solution)/shard_map/all_to_all | solution.py:425
  118.3 5.5 %collective-permute-start = (bf16[15,256]{1,0:T(8,128)(2,1)S(1)}, bf16[15,256]{1,0:T(8,128)(2,1)S(1)}, u32[]{:S(2)}, u32[]{:S(2)}) collective-permute-start(bf16[15,256]{1,0:T(8,128)(2,1)S(1)} %slice.76), channel_id=1, source_target_pairs={{0,8},{8,16},{16,24},{24,32},{32,40},{40,48},{48,56},{56,64},{64,7... | collective-permute-start | bytes 23048 | tf_op jit(solution)/shard_map/ppermute | solution.py:428
  134.8 2.5 %copy-start.8 = (bf16[128,4096]{1,0:T(8,128)(2,1)S(1)}, bf16[128,4096]{1,0:T(8,128)(2,1)}, u32[]{:S(2)}) copy-start(bf16[128,4096]{1,0:T(8,128)(2,1)} %param.34) | copy-start | bytes 3145732
  135.4 4.6 %collective-permute-start.5 = (bf16[128,4096]{1,0:T(8,128)(2,1)S(1)}, bf16[128,4096]{1,0:T(8,128)(2,1)S(1)}, u32[]{:S(2)}, u32[]{:S(2)}) collective-permute-start(bf16[128,4096]{1,0:T(8,128)(2,1)S(1)} %fusion), channel_id=1, source_target_pairs={{0,1},{1,0},{2,3},{3,2},{4,5},{5,4},{6,7},{7,6},{8,9},{9,8},{10,11... | collective-permute-start | bytes 3145736 | tf_op jit(solution)/shard_map/ppermute | solution.py:456

commit v5 on v4

--- a/solution.py
+++ b/solution.py
@@ -60,7 +60,7 @@
 def attend_kernel(place_ref, mine_ref, other_ref, *refs):
     query_refs, refs = refs[:MEMBERS], refs[MEMBERS:]
     key_up_ref, value_up_ref, gain_ref, block_ref, near_ref, far_ref, out_ref, *refs = refs
-    q_ref, lat_ref, weight_ref, turn_ref, up_ref, *refs = refs
+    q_ref, lat_ref, turn_ref, up_ref, far_keys_ref, sems, *refs = refs
     heads = key_up_ref.shape[1] // NOPE
     max_refs, sum_refs, acc_refs, key_refs, score_refs, top_refs = (
         refs[n * heads : (n + 1) * heads] for n in range(6)
@@ -72,8 +72,16 @@
     slices = [pl.ds(n * 128, 128) for n in range(width // 128)]
     chunk = min(4, Y) * HALF
 
-    for d in range(count):
-        q_ref[lax.rem(member + (count - d), count)] = query_refs[d][...]
+    arrivals = [
+        pltpu.make_async_copy(
+            query_refs[d], q_ref.at[lax.rem(member + (count - d), count)], sems.at[d]
+        )
+        for d in range(count)
+    ]
+    arrival = pltpu.make_async_copy(other_ref, far_keys_ref, sems.at[count])
+    arrival.start()
+    for copy in arrivals:
+        copy.start()
     for h in range(heads):
         max_refs[h][...] = jnp.full(max_refs[h].shape, -HUGE, jnp.float32)
         sum_refs[h][...] = jnp.zeros_like(sum_refs[h])
@@ -83,51 +91,40 @@
     gain = jnp.broadcast_to(gain_ref[:, NOPE:], (ROPE, ROPE)).T[:, :1]
 
     def build_keys(step, plane):
-        for u, (keys_ref, in_ref) in enumerate(((mine_ref, near_ref), (other_ref, far_ref))):
+        for u, (keys_ref, in_ref) in enumerate(((mine_ref, near_ref), (far_keys_ref, far_ref))):
+            in_cos, in_sin = in_ref[0], in_ref[1]
             for n in range(Y):
                 at = pl.ds((u * Y + n) * HALF, HALF)
-                for x in range(4):
-                    part = keys_ref[x, step * Y + n]
-                    if x < 3:
-                        lat_ref[x * 80 : (x + 1) * 80, at] = part
-                    else:
-                        lat_ref[240:256, at] = part[:16]
-                        turn_ref[:, at] = part[16:].astype(jnp.float32)
-
-        def turn(u, in_ref):
-            for n in range(Y):
-                at = pl.ds((u * Y + n) * HALF, HALF)
-                in_cos, in_sin = in_ref[0], in_ref[1]
+                for x in range(3):
+                    lat_ref[x * 80 : (x + 1) * 80, at] = keys_ref[x, step * Y + n]
+                last = keys_ref[3, step * Y + n]
+                lat_ref[240:256, at] = last[:16]
+                raw = last[16:].astype(jnp.float32)
+                square = jnp.sum(raw * raw, axis=0, keepdims=True)
+                top_refs[0][n : n + 1, u * 128 : (u + 1) * 128] = square
                 block_cos = block_ref[plane, : ROPE // 2, n : n + 1]
                 block_sin = block_ref[plane, ROPE // 2 :, n : n + 1]
                 cosine = block_cos * in_cos - block_sin * in_sin
                 sine = block_sin * in_cos + block_cos * in_sin
-                raw = turn_ref[:, at]
-                square = jnp.sum(raw * raw, axis=0, keepdims=True)
                 raw = raw * gain
                 a, b = raw[: ROPE // 2], raw[ROPE // 2 :]
                 turn_ref[: ROPE // 2, at] = a * cosine - b * sine
                 turn_ref[ROPE // 2 :, at] = a * sine + b * cosine
-                top_refs[0][n : n + 1, u * 128 : (u + 1) * 128] = square
-
-        for u, in_ref in enumerate((near_ref, far_ref)):
-            turn(u, in_ref)
-        for n in range(width // chunk):
-            at = pl.ds(n * chunk, chunk)
-            raw = jnp.dot(up_ref[...], lat_ref[:, at], preferred_element_type=jnp.float32)
-            u, first = n * chunk // (Y * HALF), n * chunk % (Y * HALF) // HALF
-            rope_sq = jnp.concatenate(
-                [top_refs[0][k : k + 1, u * 128 : (u + 1) * 128] for k in range(first, first + chunk // HALF)],
-                axis=1,
-            )
-            for h in range(heads):
-                part = raw[h * NOPE : (h + 1) * NOPE]
-                square = jnp.sum(part * part, axis=0, keepdims=True) + rope_sq
-                inverse = lax.rsqrt(square * (1.0 / (NOPE + ROPE)) + EPS)
-                key_refs[h][:NOPE, at] = (part * inverse).astype(jnp.bfloat16)
-                key_refs[h][NOPE + h * ROPE : NOPE + (h + 1) * ROPE, at] = (
-                    turn_ref[:, at] * inverse
-                ).astype(jnp.bfloat16)
+            for n in range(Y * HALF // chunk):
+                at = pl.ds(u * Y * HALF + n * chunk, chunk)
+                raw = jnp.dot(up_ref[...], lat_ref[:, at], preferred_element_type=jnp.float32)
+                blocks = range(n * chunk // HALF, (n + 1) * chunk // HALF)
+                rope_sq = jnp.concatenate(
+                    [top_refs[0][k : k + 1, u * 128 : (u + 1) * 128] for k in blocks], axis=1
+                )
+                for h in range(heads):
+                    part = raw[h * NOPE : (h + 1) * NOPE]
+                    square = jnp.sum(part * part, axis=0, keepdims=True) + rope_sq
+                    inverse = lax.rsqrt(square * (1.0 / (NOPE + ROPE)) + EPS)
+                    key_refs[h][:NOPE, at] = (part * inverse).astype(jnp.bfloat16)
+                    key_refs[h][NOPE + h * ROPE : NOPE + (h + 1) * ROPE, at] = (
+                        turn_ref[:, at] * inverse
+                    ).astype(jnp.bfloat16)
 
     def score(i, h):
         query = jnp.concatenate(
@@ -153,24 +150,47 @@
             top = jnp.maximum(top, scores[:, n * 128 : (n + 1) * 128])
         top_refs[h][:, :128] = top
 
-    def weigh(i, h):
+    def weigh(i, h, following=None):
         before = max_refs[h][i]
         after = jnp.maximum(before, jnp.max(top_refs[h][:, :128], axis=1, keepdims=True))
         factor = jnp.exp2(before - after)
         total = sum_refs[h][i] * factor
-        for at in slices:
-            weights = jnp.exp2(score_refs[h][:, at] - after)
-            weight_ref[:, at] = weights.astype(jnp.bfloat16)
-            total = total + weights
+        update = acc_refs[h][i] * jnp.concatenate([factor, factor], axis=1)
+        top = None
+        if following is not None:
+            j, other = following
+            query = jnp.concatenate(
+                [q_ref[j, :, other * NOPE : (other + 1) * NOPE], q_ref[j, :, heads * NOPE :]],
+                axis=1,
+            )
+        for n in range(0, len(slices), 4):
+            if following is not None:
+                at = slice(n * 128, (n + 4) * 128)
+                scores = jnp.dot(query, key_refs[other][:, at], preferred_element_type=jnp.float32)
+                score_refs[other][:, at] = scores
+                for k in range(4):
+                    piece = scores[:, k * 128 : (k + 1) * 128]
+                    top = piece if top is None else jnp.maximum(top, piece)
+            pieces = []
+            for at in slices[n : n + 4]:
+                weights = jnp.exp2(score_refs[h][:, at] - after)
+                pieces.append(weights.astype(jnp.bfloat16))
+                total = total + weights
+            update = update + lax.dot_general(
+                jnp.concatenate(pieces, axis=1),
+                lat_ref[:, n * 128 : (n + 4) * 128],
+                (((1,), (1,)), ((), ())),
+                preferred_element_type=jnp.float32,
+            )
         max_refs[h][i] = after
         sum_refs[h][i] = total
-        update = lax.dot_general(
-            weight_ref[...],
-            lat_ref[...],
-            (((1,), (1,)), ((), ())),
-            preferred_element_type=jnp.float32,
-        )
-        acc_refs[h][i] = acc_refs[h][i] * jnp.concatenate([factor, factor], axis=1) + update
+        acc_refs[h][i] = update
+        if following is not None:
+            top_refs[other][:, :128] = top
+
+    arrival.wait()
+    for copy in arrivals:
+        copy.wait()
 
     @pl.loop(0, 2)
     def _(step):
@@ -197,10 +217,9 @@
             def _(i):
                 for h in range(heads):
                     if h + 1 < heads:
-                        score(i, h + 1)
+                        weigh(i, h, (i, h + 1))
                     else:
-                        score(jnp.minimum(i + 1, count - 1), 0)
-                    weigh(i, h)
+                        weigh(i, h, (jnp.minimum(i + 1, count - 1), 0))
 
     @pl.loop(0, count)
     def _(i):
@@ -235,14 +254,20 @@
     return pl.pallas_call(
         attend_kernel,
         out_shape=jax.ShapeDtypeStruct((MEMBERS, rows + EXTRA, heads * VD), jnp.bfloat16),
-        in_specs=[pl.BlockSpec(memory_space=pltpu.SMEM)] + [vmem] * (8 + MEMBERS),
+        in_specs=[
+            pl.BlockSpec(memory_space=pltpu.SMEM),
+            vmem,
+            *[pl.BlockSpec(memory_space=pl.ANY)] * (1 + MEMBERS),
+            *[vmem] * 6,
+        ],
         out_specs=vmem,
         scratch_shapes=[
             pltpu.VMEM((MEMBERS, rows, channels), jnp.bfloat16),
             pltpu.VMEM((256, Y * rows), jnp.bfloat16),
-            pltpu.VMEM((rows, Y * rows), jnp.bfloat16),
             pltpu.VMEM((ROPE, Y * rows), jnp.float32),
             pltpu.VMEM(key_up.shape[::-1], jnp.bfloat16),
+            pltpu.VMEM(other.shape, jnp.bfloat16),
+            pltpu.SemaphoreType.DMA((MEMBERS + 1,)),
             *[s for s in wide for _ in range(heads)],
         ],
         compiler_params=pltpu.CompilerParams(vmem_limit_bytes=VMEM_LIMIT),
@@ -259,14 +284,14 @@
     latent = latent_ref[...].astype(jnp.float32)
     normed = row_norm(latent, gain_ref[...]).astype(jnp.bfloat16)
     all_ref[: latent.shape[1]] = normed.T
-    all_ref[latent.shape[1] :] = rope_ref[...].T
+    all_ref[latent.shape[1] :] = rope_ref[...]
     own = all_ref[pl.ds(pl.multiple_of(place_ref[1] * 80, 16), 80), :]
     for n in range(out_ref.shape[0]):
         out_ref[n] = own
 
 
 def key_share(place, latent, rope, gain, count):
-    channels = latent.shape[1] + rope.shape[1]
+    channels = latent.shape[1] + rope.shape[0]
     return pl.pallas_call(
         share_kernel,
         out_shape=jax.ShapeDtypeStruct((count, 80, HALF), jnp.bfloat16),
@@ -275,7 +300,7 @@
             grid=(1,),
             in_specs=[
                 pl.BlockSpec((HALF, latent.shape[1]), lambda i, w: (w[0], 0)),
-                pl.BlockSpec((HALF, rope.shape[1]), lambda i, w: (w[0], 0)),
+                pl.BlockSpec((rope.shape[0], HALF), lambda i, w: (0, w[0])),
                 pl.BlockSpec((1, latent.shape[1]), lambda i, w: (0, 0)),
             ],
             out_specs=pl.BlockSpec((count, 80, HALF), lambda i, w: (0, 0, 0)),
@@ -380,7 +405,7 @@
     )
 
     share = key_share(
-        jnp.stack([core, line]).astype(jnp.int32), kv_latent, key_rope, kv_lat_gain, 2 * Y
+        jnp.stack([core, line]).astype(jnp.int32), kv_latent, key_rope.T, kv_lat_gain, 2 * Y
     )
     mine = lax.all_to_all(share, "sp", 0, 0, axis_index_groups=key_groups)
     mine = to_all(mine, "fs")
@@ -442,19 +467,23 @@
     ).astype(jnp.bfloat16)
 
     lines = lax.axis_size("fs")
-    channels = jnp.concatenate([pooled, attended], axis=1).reshape(
-        lines, 2, -1, pooled.shape[1] + attended.shape[1]
-    )
-
-    def projected(rows):
-        rows = rows.reshape(-1, rows.shape[-1])
-        return jnp.dot(rows[:, :128], out_pool, preferred_element_type=jnp.float32) + jnp.dot(
-            rows[:, 128:], out_attn, preferred_element_type=jnp.float32
+
+    def rows_of(array, part):
+        array = array.reshape(lines, 2, -1, array.shape[1])
+        array = lax.dynamic_index_in_dim(array, part, 1, False)
+        return array.reshape(-1, array.shape[-1])
+
+    def projected(part):
+        from_pool = jnp.dot(
+            rows_of(pooled, part), out_pool, preferred_element_type=jnp.float32
         )
-
-    sent = projected(lax.dynamic_index_in_dim(channels, 1 - core, 1, False)).astype(jnp.bfloat16)
+        return from_pool + jnp.dot(
+            rows_of(attended, part), out_attn, preferred_element_type=jnp.float32
+        )
+
+    sent = projected(1 - core).astype(jnp.bfloat16)
     received = lax.ppermute(sent, "tp", [(0, 1), (1, 0)])
-    kept = projected(lax.dynamic_index_in_dim(channels, core, 1, False))
+    kept = projected(core)
     chip = (kept + received.astype(jnp.float32)).astype(jnp.bfloat16)
     chip = lax.all_to_all(chip.reshape(lines, -1, chip.shape[1]), "fs", 0, 0)
     mixed = jnp.sum(chip.astype(jnp.float32), axis=0).astype(jnp.bfloat16)

time: 161 us -> 162 us (level)
  the two profiles are of different devices: /device:TPU:8 before, /device:TPU:72 now
where the time goes in v5:
time: 162 us; the launch traced here: 161 us
  waiting for transfers between devices  48.9 us (30%)
  starting transfers between devices  41.5 us (26%)
  blocking collectives  18.8 us (12%)
  Pallas kernels  17.9 us (11%)
  local copies, waits for them, and re-layouts  13 us (8%)
  other arithmetic  12.1 us (7%)
  matrix products  8.05 us (5%)
    all_to_all x1, blocking collectives, local(): chip = lax.all_to_all(chip.reshape(lines, -1, chip.shape[1]), 'fs', 0, 0)  18.8 us
    pallas_call x1, Pallas kernels, attend(): pl.pallas_call(attend_kernel, out_shape=jax.ShapeDtypeStruct((MEMBERS, ro...  15.5 us
    all_to_all x1, starting transfers between devices, local(): mine = lax.all_to_all(share, 'sp', 0, 0, axis_index_groups=key_groups)  15.1 us
    all_to_all x1, waiting for transfers between devices, local(): mine = lax.all_to_all(share, 'sp', 0, 0, axis_index_groups=key_groups)  13.1 us
    ppermute x3, starting transfers between devices, turned(): return lax.ppermute(queries, 'sp', pairs)  12.3 us
    all_to_all x1, waiting for transfers between devices, to_all(): lax.all_to_all(jnp.broadcast_to(value[None], (count, *value.shape)), axis...  11.6 us
    all_to_all x1, waiting for transfers between devices, local(): lax.all_to_all(partial_out, 'sp', 0, 0, axis_index_groups=query_groups)  11 us
    ppermute x3, waiting for transfers between devices, turned(): return lax.ppermute(queries, 'sp', pairs)  11 us
  transfers between devices with their start and end apart: 9, of which 6 were waited for; matrix products, arithmetic and copies ran while one was open for 14% of the time, Pallas kernels for 10%

profile of v5, /device:TPU:72, one launch (start us, length us, event | category | flops | bytes accessed | tf_op | source)
XLA Modules:
  0.0 161.3 jit_solution(10151851327977527744)
XLA Ops:
  0.7 1.0 copy-done.2
  1.8 0.8 copy-done.3
  2.5 0.7 copy-done.4
  3.2 1.5 key_share.1
  4.7 15.1 %all-to-all-start = ((bf16[16,80,128]{2,1,0:T(8,128)(2,1)}), bf16[16,80,128]{2,1,0:T(8,128)(2,1)S(1)}, u32[]{:S(2)}, u32[]{:S(2)}) async-start(bf16[16,80,128]{2,1,0:T(8,128)(2,1)} %key_share.1), calls=%async_computation | async-start | bytes 655360 | tf_op jit(solution)/shard_map/all_to_all | solution.py:410
  19.8 1.1 fusion.2
  20.9 13.1 %all-to-all-done = bf16[16,80,128]{2,1,0:T(8,128)(2,1)S(1)} async-done(((bf16[16,80,128]{2,1,0:T(8,128)(2,1)}), bf16[16,80,128]{2,1,0:T(8,128)(2,1)S(1)}, u32[]{:S(2)}, u32[]{:S(2)}) %all-to-all-start) | async-done | bytes 327712 | tf_op jit(solution)/shard_map/all_to_all | solution.py:410
  34.0 1.2 broadcast_in_dim.42
  35.2 4.3 %all-to-all-start.1 = ((bf16[4,16,80,128]{3,2,1,0:T(8,128)(2,1)}), bf16[4,16,80,128]{3,2,1,0:T(8,128)(2,1)S(1)}, u32[]{:S(2)}, u32[]{:S(2)}) async-start(bf16[4,16,80,128]{3,2,1,0:T(8,128)(2,1)} %broadcast_in_dim.42), calls=%async_computation.1 | async-start | bytes 2621440 | tf_op jit(solution)/shard_map/all_to_all | solution.py:369
  39.5 1.2 fusion.30
  40.8 1.5 fusion.5
  42.3 1.5 multiply_multiply_fusion
  43.9 11.6 %all-to-all-done.1.mine_ref = bf16[4,16,80,128]{3,2,1,0:T(8,128)(2,1)S(1)} async-done(((bf16[4,16,80,128]{3,2,1,0:T(8,128)(2,1)}), bf16[4,16,80,128]{3,2,1,0:T(8,128)(2,1)S(1)}, u32[]{:S(2)}, u32[]{:S(2)}) %all-to-all-start.1) | async-done | bytes 1310752 | tf_op jit(solution)/shard_map/all_to_all | solution.py:369
  55.5 1.9 %collective-permute-start.1 = (bf16[4,16,80,128]{3,2,1,0:T(8,128)(2,1)S(1)}, bf16[4,16,80,128]{3,2,1,0:T(8,128)(2,1)}, u32[]{:S(2)}, u32[]{:S(2)}) collective-permute-start(bf16[4,16,80,128]{3,2,1,0:T(8,128)(2,1)S(1)} %all-to-all-done.1.mine_ref), channel_id=1, source_target_pairs={{0,1},{1,0},{2,3},{3,2},{4,5},{5,4},{6,7},{7,6},{8,9},{9,8},{10,11... | collective-permute-start | bytes 3932168 | tf_op jit(solution)/shard_map/ppermute | solution.py:412
  57.4 0.9 subtract_multiply_fusion
  58.3 0.9 subtract_convert_fusion
  59.2 0.6 pad_maximum_fusion.1
  59.8 1.6 copy.25
  61.4 1.7 %fusion.7 = bf16[256,2,128]{0,2,1:T(8,128)(2,1)} fusion(f32[256,2,192]{0,2,1:T(8,128)} %multiply_multiply_fusion, f32[128]{0:T(128)S(1)} %slice_multiply_fusion.1), kind=kLoop, calls=%fused_computation.15 | loop fusion | flops 131072 | bytes 393728 | tf_op jit(solution)/shard_map/convert.6
  63.1 1.7 %copy.27 = bf16[256,256]{1,0:T(8,128)(2,1)} copy(bf16[256,256]{0,1:T(8,128)(2,1)} %bitcast.44) | data formatting | bytes 262144 | tf_op jit(solution)/shard_map/reshape | solution.py:53
  64.7 1.6 %pad_maximum_fusion.refs_0_ = bf16[256,384]{1,0:T(8,128)(2,1)} fusion(bf16[256,128]{1,0:T(8,128)(2,1)} %copy.25, bf16[256,256]{1,0:T(8,128)(2,1)} %copy.27), kind=kLoop, calls=%fused_computation.51 | loop fusion | flops 393216 | bytes 393216 | tf_op jit(solution)/shard_map/concatenate | solution.py:51
  66.4 1.9 %collective-permute-start.2 = (bf16[256,384]{1,0:T(8,128)(2,1)}, bf16[256,384]{1,0:T(8,128)(2,1)}, u32[]{:S(2)}, u32[]{:S(2)}) collective-permute-start(bf16[256,384]{1,0:T(8,128)(2,1)} %pad_maximum_fusion.refs_0_), channel_id=1, source_target_pairs={{0,128},{128,256},{256,384},{384,0},{8,136},{136,264},{264,392},{3... | collective-permute-start | bytes 589832 | tf_op jit(solution)/shard_map/ppermute | solution.py:428
  68.3 5.0 %collective-permute-start.3 = (bf16[256,384]{1,0:T(8,128)(2,1)}, bf16[256,384]{1,0:T(8,128)(2,1)}, u32[]{:S(2)}, u32[]{:S(2)}) collective-permute-start(bf16[256,384]{1,0:T(8,128)(2,1)} %pad_maximum_fusion.refs_0_), channel_id=1, source_target_pairs={{0,256},{128,384},{256,0},{384,128},{8,264},{136,392},{264,8},{392... | collective-permute-start | bytes 589832 | tf_op jit(solution)/shard_map/ppermute | solution.py:428
  73.3 5.5 %collective-permute-start.4 = (bf16[256,384]{1,0:T(8,128)(2,1)}, bf16[256,384]{1,0:T(8,128)(2,1)}, u32[]{:S(2)}, u32[]{:S(2)}) collective-permute-start(bf16[256,384]{1,0:T(8,128)(2,1)} %pad_maximum_fusion.refs_0_), channel_id=1, source_target_pairs={{0,384},{128,0},{256,128},{384,256},{8,392},{136,8},{264,136},{392... | collective-permute-start | bytes 589832 | tf_op jit(solution)/shard_map/ppermute | solution.py:428
  78.7 1.3 slice.64
  80.0 1.9 %collective-permute-start = (bf16[15,256]{1,0:T(8,128)(2,1)}, bf16[15,256]{1,0:T(8,128)(2,1)S(1)}, u32[]{:S(2)}, u32[]{:S(2)}) collective-permute-start(bf16[15,256]{1,0:T(8,128)(2,1)} %slice.64), channel_id=1, source_target_pairs={{0,8},{8,16},{16,24},{24,32},{32,40},{40,48},{48,56},{56,64},{64,7... | collective-permute-start | bytes 23048 | tf_op jit(solution)/shard_map/ppermute | solution.py:453
  82.0 0.1 stack.36.place_ref
  82.1 0.6 minimum_convert_fusion
  82.7 0.8 constant_dynamic-slice_fusion.3
  83.4 5.8 %collective-permute-done.2.refs_1_ = bf16[256,384]{1,0:T(8,128)(2,1)} collective-permute-done((bf16[256,384]{1,0:T(8,128)(2,1)}, bf16[256,384]{1,0:T(8,128)(2,1)}, u32[]{:S(2)}, u32[]{:S(2)}) %collective-permute-start.2) | collective-permute-done | bytes 196640 | tf_op jit(solution)/shard_map/ppermute | solution.py:428
  89.2 5.2 %collective-permute-done.4.refs_3_ = bf16[256,384]{1,0:T(8,128)(2,1)} collective-permute-done((bf16[256,384]{1,0:T(8,128)(2,1)}, bf16[256,384]{1,0:T(8,128)(2,1)}, u32[]{:S(2)}, u32[]{:S(2)}) %collective-permute-start.4) | collective-permute-done | bytes 196640 | tf_op jit(solution)/shard_map/ppermute | solution.py:428
  94.4 0.9 copy-done.6
  95.3 0.9 copy-done.8
  96.3 15.5 %attend.1 = bf16[4,272,256]{2,1,0:T(8,128)(2,1)S(1)} custom-call(s32[6]{0:T(128)S(1)} %stack.36.place_ref, bf16[4,16,80,128]{3,2,1,0:T(8,128)(2,1)S(1)} %all-to-all-done.1.mine_ref, bf16[4,16,80,128]{3,2,1,0:T(8,128)(2,1)} %collective-permute-done.1.other_ref, bf16[256,384]{1,0:T(8,128)(2,1)} %pad_maximum_fusion.refs_0_, ...), custom_call_target="tpu_custom_call" | custom-call | flops 5368709120 | bytes 2621440 | tf_op jit(solution)/shard_map/attend/pallas_call | solution.py:254
  111.7 0.8 copy-done.1
  112.5 4.0 %all-to-all-start.2 = ((bf16[4,272,256]{2,1,0:T(8,128)(2,1)}), bf16[4,272,256]{2,1,0:T(8,128)(2,1)S(1)}, u32[]{:S(2)}, u32[]{:S(2)}) async-start(bf16[4,272,256]{2,1,0:T(8,128)(2,1)} %copy-done.1), calls=%async_computation.2 | async-start | bytes 1114112 | tf_op jit(solution)/shard_map/all_to_all | solution.py:450
  116.6 0.9 maximum_convert_fusion
  117.5 1.7 %fusion.1 = bf16[256,128]{1,0:T(8,128)(2,1)S(1)} fusion(f32[271,256]{1,0:T(8,128)S(1)} %maximum_convert_fusion, f32[256]{0:T(256)} %minimum_convert_fusion, pred[]{:T(512)S(6)} %gt.63, pred[]{:T(512)S(6)} %gt.62, pred[]{:T(512)S(6)} %gt.61, pred[]{:T(512)S(6)} %gt.60, pred[]{:T(512)S(6)} %gt.59, pred[]{:T(512)S(6)} %gt.58, pred[]{:T(512)S(6)} %gt.57, ...), kind=kOutput, calls=%fused_computation.5 | convolution fusion | flops 19070976 | bytes 4326928 | tf_op jit(solution)/shard_map/dot_general | solution.py:466
  119.2 1.8 %fusion.34 = f32[128,4096]{1,0:T(8,128)} fusion(bf16[128,128]{1,0:T(8,128)(2,1)S(1)} %bitcast.49, bf16[128,4096]{1,0:T(8,128)(2,1)S(1)} %copy-done.9), kind=kOutput, calls=%fused_computation.76 | convolution fusion | flops 134217728 | bytes 3178496 | tf_op jit(solution)/shard_map/dot_general | solution.py:477
  121.0 11.0 %all-to-all-done.2.parts_ref = bf16[4,272,256]{2,1,0:T(8,128)(2,1)S(1)} async-done(((bf16[4,272,256]{2,1,0:T(8,128)(2,1)}), bf16[4,272,256]{2,1,0:T(8,128)(2,1)S(1)}, u32[]{:S(2)}, u32[]{:S(2)}) %all-to-all-start.2) | async-done | bytes 557088 | tf_op jit(solution)/shard_map/all_to_all | solution.py:450
  132.0 1.0 merge.1
  133.0 2.1 %fusion = bf16[128,4096]{1,0:T(8,128)(2,1)S(1)} fusion(f32[128,4096]{1,0:T(8,128)} %fusion.34, bf16[128,256]{1,0:T(8,128)(2,1)S(1)} %bitcast.47, bf16[256,4096]{1,0:T(8,128)(2,1)S(1)} %copy-done), kind=kOutput, calls=%fused_computation.2 | convolution fusion | flops 269484032 | bytes 5308416 | tf_op jit(solution)/shard_map/dot_general | solution.py:480
  135.2 1.9 %collective-permute-start.5 = (bf16[128,4096]{1,0:T(8,128)(2,1)S(1)}, bf16[128,4096]{1,0:T(8,128)(2,1)S(1)}, u32[]{:S(2)}, u32[]{:S(2)}) collective-permute-start(bf16[128,4096]{1,0:T(8,128)(2,1)S(1)} %fusion), channel_id=1, source_target_pairs={{0,1},{1,0},{2,3},{3,2},{4,5},{5,4},{6,7},{7,6},{8,9},{9,8},{10,11... | collective-permute-start | bytes 3145736 | tf_op jit(solution)/shard_map/ppermute | solution.py:485
  137.1 0.4 fusion.33
  137.5 2.2 %collective-permute-done.5 = bf16[128,4096]{1,0:T(8,128)(2,1)S(1)} collective-permute-done((bf16[128,4096]{1,0:T(8,128)(2,1)S(1)}, bf16[128,4096]{1,0:T(8,128)(2,1)S(1)}, u32[]{:S(2)}, u32[]{:S(2)}) %collective-permute-start.5) | collective-permute-done | bytes 1048608 | tf_op jit(solution)/shard_map/ppermute | solution.py:485
  139.7 0.6 add_convert_fusion
  140.3 18.8 %all_to_all.20 = bf16[4,32,4096]{2,1,0:T(8,128)(2,1)} all-to-all(bf16[4,32,4096]{2,1,0:T(8,128)(2,1)S(1)} %bitcast.41), channel_id=1, replica_groups=mesh['sp'=64,'fs'=4,'tp'=2] {'fs'}, dimensions={0} | all-to-all | bytes 2097152 | tf_op jit(solution)/shard_map/all_to_all | solution.py:488
  159.1 2.2 %reduce_sum.32 = bf16[32,4096]{1,0:T(8,128)(2,1)} reduce(bf16[4,32,4096]{2,1,0:T(8,128)(2,1)} %all_to_all.20, bf16[]{:T(256)} %constant.102.clone.1), dimensions={0}, to_apply=%region_2.3 | reduce | flops 393216 | bytes 1310722 | tf_op jit(solution)/shard_map/reduce_sum | solution.py:489
  (28 shorter events, 0.2 us)
Async XLA Ops:
  0.6 132.4 %copy-start = (bf16[256,4096]{1,0:T(8,128)(2,1)S(1)}, bf16[256,4096]{1,0:T(8,128)(2,1)}, u32[]{:S(2)}) copy-start(bf16[256,4096]{1,0:T(8,128)(2,1)} %param.35) | copy-start | bytes 6291460
  0.7 1.0 copy-start.2
  1.8 0.8 copy-start.3
  2.5 0.7 copy-start.4
  4.7 29.3 %all-to-all-start = ((bf16[16,80,128]{2,1,0:T(8,128)(2,1)}), bf16[16,80,128]{2,1,0:T(8,128)(2,1)S(1)}, u32[]{:S(2)}, u32[]{:S(2)}) async-start(bf16[16,80,128]{2,1,0:T(8,128)(2,1)} %key_share.1), calls=%async_computation | async-start | bytes 655360 | tf_op jit(solution)/shard_map/all_to_all | solution.py:410
  20.9 19.9 %copy-start.11 = (f32[512]{0:T(512)S(1)}, f32[512]{0:T(512)}, u32[]{:S(2)}) copy-start(f32[512]{0:T(512)} %param.25) | copy-start | bytes 6148
  35.2 20.3 %all-to-all-start.1 = ((bf16[4,16,80,128]{3,2,1,0:T(8,128)(2,1)}), bf16[4,16,80,128]{3,2,1,0:T(8,128)(2,1)S(1)}, u32[]{:S(2)}, u32[]{:S(2)}) async-start(bf16[4,16,80,128]{3,2,1,0:T(8,128)(2,1)} %broadcast_in_dim.42), calls=%async_computation.1 | async-start | bytes 2621440 | tf_op jit(solution)/shard_map/all_to_all | solution.py:369
  39.5 21.9 %copy-start.7 = (f32[192]{0:T(256)S(1)}, f32[192]{0:T(256)}, u32[]{:S(2)}) copy-start(f32[192]{0:T(256)} %param.28) | copy-start | bytes 2308
  40.8 53.6 %copy-start.5 = (bf16[256,256]{1,0:T(8,128)(2,1)S(1)}, bf16[256,256]{1,0:T(8,128)(2,1)}, u32[]{:S(2)}) copy-start(bf16[256,256]{1,0:T(8,128)(2,1)} %refs_4_.1) | copy-start | bytes 393220
  55.5 38.9 %collective-permute-start.1 = (bf16[4,16,80,128]{3,2,1,0:T(8,128)(2,1)S(1)}, bf16[4,16,80,128]{3,2,1,0:T(8,128)(2,1)}, u32[]{:S(2)}, u32[]{:S(2)}) collective-permute-start(bf16[4,16,80,128]{3,2,1,0:T(8,128)(2,1)S(1)} %all-to-all-done.1.mine_ref), channel_id=1, source_target_pairs={{0,1},{1,0},{2,3},{3,2},{4,5},{5,4},{6,7},{7,6},{8,9},{9,8},{10,11... | collective-permute-start | bytes 3932168 | tf_op jit(solution)/shard_map/ppermute | solution.py:412
  66.4 22.8 %collective-permute-start.2 = (bf16[256,384]{1,0:T(8,128)(2,1)}, bf16[256,384]{1,0:T(8,128)(2,1)}, u32[]{:S(2)}, u32[]{:S(2)}) collective-permute-start(bf16[256,384]{1,0:T(8,128)(2,1)} %pad_maximum_fusion.refs_0_), channel_id=1, source_target_pairs={{0,128},{128,256},{256,384},{384,0},{8,136},{136,264},{264,392},{3... | collective-permute-start | bytes 589832 | tf_op jit(solution)/shard_map/ppermute | solution.py:428
  68.3 20.9 %collective-permute-start.3 = (bf16[256,384]{1,0:T(8,128)(2,1)}, bf16[256,384]{1,0:T(8,128)(2,1)}, u32[]{:S(2)}, u32[]{:S(2)}) collective-permute-start(bf16[256,384]{1,0:T(8,128)(2,1)} %pad_maximum_fusion.refs_0_), channel_id=1, source_target_pairs={{0,256},{128,384},{256,0},{384,128},{8,264},{136,392},{264,8},{392... | collective-permute-start | bytes 589832 | tf_op jit(solution)/shard_map/ppermute | solution.py:428
  73.3 21.1 %collective-permute-start.4 = (bf16[256,384]{1,0:T(8,128)(2,1)}, bf16[256,384]{1,0:T(8,128)(2,1)}, u32[]{:S(2)}, u32[]{:S(2)}) collective-permute-start(bf16[256,384]{1,0:T(8,128)(2,1)} %pad_maximum_fusion.refs_0_), channel_id=1, source_target_pairs={{0,384},{128,0},{256,128},{384,256},{8,392},{136,8},{264,136},{392... | collective-permute-start | bytes 589832 | tf_op jit(solution)/shard_map/ppermute | solution.py:428
  80.0 36.5 %collective-permute-start = (bf16[15,256]{1,0:T(8,128)(2,1)}, bf16[15,256]{1,0:T(8,128)(2,1)S(1)}, u32[]{:S(2)}, u32[]{:S(2)}) collective-permute-start(bf16[15,256]{1,0:T(8,128)(2,1)} %slice.64), channel_id=1, source_target_pairs={{0,8},{8,16},{16,24},{24,32},{32,40},{40,48},{48,56},{56,64},{64,7... | collective-permute-start | bytes 23048 | tf_op jit(solution)/shard_map/ppermute | solution.py:453
  94.4 0.9 copy-start.6
  95.3 0.9 copy-start.8
  111.7 0.8 copy-start.1
  112.5 19.5 %all-to-all-start.2 = ((bf16[4,272,256]{2,1,0:T(8,128)(2,1)}), bf16[4,272,256]{2,1,0:T(8,128)(2,1)S(1)}, u32[]{:S(2)}, u32[]{:S(2)}) async-start(bf16[4,272,256]{2,1,0:T(8,128)(2,1)} %copy-done.1), calls=%async_computation.2 | async-start | bytes 1114112 | tf_op jit(solution)/shard_map/all_to_all | solution.py:450
  117.5 1.7 %copy-start.9 = (bf16[128,4096]{1,0:T(8,128)(2,1)S(1)}, bf16[128,4096]{1,0:T(8,128)(2,1)}, u32[]{:S(2)}) copy-start(bf16[128,4096]{1,0:T(8,128)(2,1)} %param.34) | copy-start | bytes 3145732
  133.0 4.1 %copy-start.10 = (bf16[128,4096]{1,0:T(8,128)(2,1)S(1)}, bf16[128,4096]{1,0:T(8,128)(2,1)}, u32[]{:S(2)}) copy-start(bf16[128,4096]{1,0:T(8,128)(2,1)} %param.34) | copy-start | bytes 3145732
  135.2 4.6 %collective-permute-start.5 = (bf16[128,4096]{1,0:T(8,128)(2,1)S(1)}, bf16[128,4096]{1,0:T(8,128)(2,1)S(1)}, u32[]{:S(2)}, u32[]{:S(2)}) collective-permute-start(bf16[128,4096]{1,0:T(8,128)(2,1)S(1)} %fusion), channel_id=1, source_target_pairs={{0,1},{1,0},{2,3},{3,2},{4,5},{5,4},{6,7},{7,6},{8,9},{9,8},{10,11... | collective-permute-start | bytes 3145736 | tf_op jit(solution)/shard_map/ppermute | solution.py:485

commit v6 on v5

--- a/solution.py
+++ b/solution.py
@@ -22,6 +22,7 @@
 PLANES = 8
 MEMBERS = 4
 VMEM_LIMIT = 32 * 2**20
+SHARE_LIMIT = 58 * 2**20
 EXTRA = 16
 
 
@@ -59,9 +60,10 @@
 
 def attend_kernel(place_ref, mine_ref, other_ref, *refs):
     query_refs, refs = refs[:MEMBERS], refs[MEMBERS:]
-    key_up_ref, value_up_ref, gain_ref, block_ref, near_ref, far_ref, out_ref, *refs = refs
+    up_hbm, gain_ref, table_ref, out_ref, *refs = refs
     q_ref, lat_ref, turn_ref, up_ref, far_keys_ref, sems, *refs = refs
-    heads = key_up_ref.shape[1] // NOPE
+    both_ref, *refs = refs
+    heads = up_hbm.shape[2] // NOPE
     max_refs, sum_refs, acc_refs, key_refs, score_refs, top_refs = (
         refs[n * heads : (n + 1) * heads] for n in range(6)
     )
@@ -78,8 +80,9 @@
         )
         for d in range(count)
     ]
-    arrival = pltpu.make_async_copy(other_ref, far_keys_ref, sems.at[count])
-    arrival.start()
+    arrivals.append(pltpu.make_async_copy(other_ref, far_keys_ref, sems.at[count]))
+    weights = pltpu.make_async_copy(up_hbm, both_ref, sems.at[count + 1])
+    weights.start()
     for copy in arrivals:
         copy.start()
     for h in range(heads):
@@ -87,12 +90,15 @@
         sum_refs[h][...] = jnp.zeros_like(sum_refs[h])
         acc_refs[h][...] = jnp.zeros_like(acc_refs[h])
         key_refs[h][NOPE:, :] = jnp.zeros((256 - NOPE, width), jnp.bfloat16)
-    up_ref[...] = key_up_ref[...].T
+    weights.wait()
+    up_ref[...] = both_ref[0].T
     gain = jnp.broadcast_to(gain_ref[:, NOPE:], (ROPE, ROPE)).T[:, :1]
 
     def build_keys(step, plane):
-        for u, (keys_ref, in_ref) in enumerate(((mine_ref, near_ref), (far_keys_ref, far_ref))):
-            in_cos, in_sin = in_ref[0], in_ref[1]
+        for u, keys_ref in enumerate((mine_ref, far_keys_ref)):
+            in_cos = table_ref[u * ROPE : u * ROPE + ROPE // 2, :]
+            in_sin = table_ref[u * ROPE + ROPE // 2 : (u + 1) * ROPE, :]
+            block_at = pl.multiple_of((2 + plane) * ROPE, ROPE)
             for n in range(Y):
                 at = pl.ds((u * Y + n) * HALF, HALF)
                 for x in range(3):
@@ -102,8 +108,8 @@
                 raw = last[16:].astype(jnp.float32)
                 square = jnp.sum(raw * raw, axis=0, keepdims=True)
                 top_refs[0][n : n + 1, u * 128 : (u + 1) * 128] = square
-                block_cos = block_ref[plane, : ROPE // 2, n : n + 1]
-                block_sin = block_ref[plane, ROPE // 2 :, n : n + 1]
+                block_cos = table_ref[pl.ds(block_at, ROPE // 2), n : n + 1]
+                block_sin = table_ref[pl.ds(block_at + ROPE // 2, ROPE // 2), n : n + 1]
                 cosine = block_cos * in_cos - block_sin * in_sin
                 sine = block_sin * in_cos + block_cos * in_sin
                 raw = raw * gain
@@ -188,7 +194,6 @@
         if following is not None:
             top_refs[other][:, :128] = top
 
-    arrival.wait()
     for copy in arrivals:
         copy.wait()
 
@@ -230,7 +235,7 @@
             total = jnp.where(seen, total, 1.0)
             mean = (acc_refs[h][i] * (1.0 / total)).astype(jnp.bfloat16)
             out_ref[i, :rows, h * VD : (h + 1) * VD] = jnp.dot(
-                mean, value_up_ref[:, h * VD : (h + 1) * VD], preferred_element_type=jnp.float32
+                mean, both_ref[1, :, h * VD : (h + 1) * VD], preferred_element_type=jnp.float32
             ).astype(out_ref.dtype)
             level = jnp.where(seen, max_refs[h][i] + jnp.log2(total), -HUGE).T[:1]
             for term in range(3):
@@ -239,9 +244,9 @@
                 level = level - rounded.astype(jnp.float32)
 
 
-def attend(place, mine, other, queries, key_up, value_up, gain, block_table, near, far):
+def attend(place, mine, other, queries, up, gain, table):
     rows, channels = queries[0].shape
-    heads = key_up.shape[1] // NOPE
+    heads = up.shape[2] // NOPE
     vmem = pl.BlockSpec(memory_space=pltpu.VMEM)
     wide = [
         pltpu.VMEM((MEMBERS, rows, 128), jnp.float32),
@@ -257,17 +262,18 @@
         in_specs=[
             pl.BlockSpec(memory_space=pltpu.SMEM),
             vmem,
-            *[pl.BlockSpec(memory_space=pl.ANY)] * (1 + MEMBERS),
-            *[vmem] * 6,
+            *[pl.BlockSpec(memory_space=pl.ANY)] * (1 + MEMBERS + 1),
+            *[vmem] * 2,
         ],
         out_specs=vmem,
         scratch_shapes=[
             pltpu.VMEM((MEMBERS, rows, channels), jnp.bfloat16),
             pltpu.VMEM((256, Y * rows), jnp.bfloat16),
             pltpu.VMEM((ROPE, Y * rows), jnp.float32),
-            pltpu.VMEM(key_up.shape[::-1], jnp.bfloat16),
+            pltpu.VMEM(up.shape[:0:-1], jnp.bfloat16),
             pltpu.VMEM(other.shape, jnp.bfloat16),
-            pltpu.SemaphoreType.DMA((MEMBERS + 1,)),
+            pltpu.SemaphoreType.DMA((MEMBERS + 2,)),
+            pltpu.VMEM(up.shape, jnp.bfloat16),
             *[s for s in wide for _ in range(heads)],
         ],
         compiler_params=pltpu.CompilerParams(vmem_limit_bytes=VMEM_LIMIT),
@@ -277,37 +283,46 @@
             transcendentals=5 * rows * Y * rows * heads,
         ),
         name="attend",
-    )(place, mine, other, *queries, key_up, value_up, gain, block_table, near, far)
-
-
-def share_kernel(place_ref, latent_ref, rope_ref, gain_ref, out_ref, all_ref):
-    latent = latent_ref[...].astype(jnp.float32)
-    normed = row_norm(latent, gain_ref[...]).astype(jnp.bfloat16)
-    all_ref[: latent.shape[1]] = normed.T
-    all_ref[latent.shape[1] :] = rope_ref[...]
+    )(place, mine, other, *queries, up, gain, table)
+
+
+def share_kernel(
+    place_ref, latent_ref, rope_ref, gain_ref, out_ref, half_ref, all_ref, scale_ref, sems
+):
+    channels = latent_ref.shape[1]
+    at = pl.ds(pl.multiple_of(place_ref[0] * HALF, HALF), HALF)
+    copies = [
+        pltpu.make_async_copy(latent_ref.at[at], half_ref, sems.at[0]),
+        pltpu.make_async_copy(rope_ref.at[:, at], all_ref.at[pl.ds(channels, ROPE)], sems.at[1]),
+        pltpu.make_async_copy(gain_ref, scale_ref, sems.at[2]),
+    ]
+    for copy in copies:
+        copy.start()
+    for copy in copies:
+        copy.wait()
+    normed = row_norm(half_ref[...].astype(jnp.float32), scale_ref[...]).astype(jnp.bfloat16)
+    all_ref[:channels] = normed.T
     own = all_ref[pl.ds(pl.multiple_of(place_ref[1] * 80, 16), 80), :]
     for n in range(out_ref.shape[0]):
         out_ref[n] = own
 
 
 def key_share(place, latent, rope, gain, count):
-    channels = latent.shape[1] + rope.shape[0]
+    channels = latent.shape[1]
+    hbm = pl.BlockSpec(memory_space=pl.ANY)
     return pl.pallas_call(
         share_kernel,
         out_shape=jax.ShapeDtypeStruct((count, 80, HALF), jnp.bfloat16),
-        grid_spec=pltpu.PrefetchScalarGridSpec(
-            num_scalar_prefetch=1,
-            grid=(1,),
-            in_specs=[
-                pl.BlockSpec((HALF, latent.shape[1]), lambda i, w: (w[0], 0)),
-                pl.BlockSpec((rope.shape[0], HALF), lambda i, w: (0, w[0])),
-                pl.BlockSpec((1, latent.shape[1]), lambda i, w: (0, 0)),
-            ],
-            out_specs=pl.BlockSpec((count, 80, HALF), lambda i, w: (0, 0, 0)),
-            scratch_shapes=[pltpu.VMEM((channels, HALF), jnp.bfloat16)],
-        ),
+        in_specs=[pl.BlockSpec(memory_space=pltpu.SMEM), hbm, hbm, hbm],
+        out_specs=pl.BlockSpec(memory_space=pltpu.VMEM),
+        scratch_shapes=[
+            pltpu.VMEM((HALF, channels), jnp.bfloat16),
+            pltpu.VMEM((channels + ROPE, HALF), jnp.bfloat16),
+            pltpu.VMEM((1, channels), jnp.float32),
+            pltpu.SemaphoreType.DMA((3,)),
+        ],
         cost_estimate=pl.CostEstimate(flops=10**6, bytes_accessed=10**6, transcendentals=HALF),
-        compiler_params=pltpu.CompilerParams(vmem_limit_bytes=4 * 2**20),
+        compiler_params=pltpu.CompilerParams(vmem_limit_bytes=SHARE_LIMIT),
         name="key_share",
     )(place, latent, rope, gain[None])
 
@@ -402,11 +417,13 @@
     block_cos, block_sin, in_cos, in_sin = turn_tables(row_count, sp_size)
     plane_turns = np.transpose(
         np.concatenate([block_cos, block_sin], axis=1).reshape(-1, Y, ROPE), (0, 2, 1)
-    )
-
-    share = key_share(
-        jnp.stack([core, line]).astype(jnp.int32), kv_latent, key_rope.T, kv_lat_gain, 2 * Y
-    )
+    ).reshape(-1, Y)
+    plane_turns = np.pad(plane_turns, ((0, 0), (0, HALF - Y)))
+    halves = [np.concatenate([in_cos.T, in_sin.T])[:, c * HALF : (c + 1) * HALF] for c in range(2)]
+    tables = np.stack([np.concatenate([halves[c], halves[1 - c], plane_turns]) for c in range(2)])
+
+    seat = jnp.stack([core, line]).astype(jnp.int32)
+    share = key_share(seat, kv_latent, key_rope.T, kv_lat_gain, 2 * Y)
     mine = lax.all_to_all(share, "sp", 0, 0, axis_index_groups=key_groups)
     mine = to_all(mine, "fs")
     other = lax.ppermute(mine, "tp", [(0, 1), (1, 0)])
@@ -428,9 +445,6 @@
         return lax.ppermute(queries, "sp", pairs)
 
     queries = [queries] + [turned(d) for d in range(1, MEMBERS)]
-    within = jnp.asarray(np.stack([in_cos.T, in_sin.T]))
-    near = lax.dynamic_slice_in_dim(within, core * HALF, HALF, 2)
-    far = lax.dynamic_slice_in_dim(within, HALF - core * HALF, HALF, 2)
     low_plane = jnp.minimum(z, PLANES - 1 - z)
     place = jnp.stack(
         [low_plane, PLANES - 1 - low_plane, lax.rem(z, 2), y, core * HALF, lax.div(z, 2)]
@@ -440,12 +454,9 @@
         mine,
         other,
         queries,
-        key_up,
-        value_up,
+        jnp.stack([key_up, value_up]),
         k_head_gain[None],
-        jnp.asarray(plane_turns),
-        near,
-        far,
+        lax.dynamic_index_in_dim(jnp.asarray(tables), core, 0, False),
     )
     parts = lax.all_to_all(partial_out, "sp", 0, 0, axis_index_groups=query_groups)
     attended, log_weight = merge(parts)

time: 162 us -> 157 us (0.969)
  local copies, waits for them, and re-layouts: 13 us -> 6.93 us
    unnamed x24 -> x20, local copies, waits for them, and re-layouts: 5.16 us -> 0.84 us
    another operation x3 -> x4, other arithmetic: 2.66 us -> 4.17 us
  transfers between devices with their start and end apart: 9 -> 9, of which waited for: 6 -> 6; matrix products, arithmetic and copies ran while one was open for 14% -> 12% of each run, Pallas kernels for 10% -> 10%
where the time goes in v6:
time: 157 us; the launch traced here: 156 us
  waiting for transfers between devices  49.8 us (32%)
  starting transfers between devices  41.6 us (26%)
  Pallas kernels  19.3 us (12%)
  blocking collectives  18.8 us (12%)
  other arithmetic  10.5 us (7%)
  matrix products  8.03 us (5%)
  local copies, waits for them, and re-layouts  6.93 us (4%)
    all_to_all x1, blocking collectives, local(): chip = lax.all_to_all(chip.reshape(lines, -1, chip.shape[1]), 'fs', 0, 0)  18.8 us
    pallas_call x1, Pallas kernels, attend(): pl.pallas_call(attend_kernel, out_shape=jax.ShapeDtypeStruct((MEMBERS, ro...  15.7 us
    all_to_all x1, starting transfers between devices, local(): mine = lax.all_to_all(share, 'sp', 0, 0, axis_index_groups=key_groups)  15.1 us
    all_to_all x1, waiting for transfers between devices, local(): mine = lax.all_to_all(share, 'sp', 0, 0, axis_index_groups=key_groups)  13.1 us
    all_to_all x1, waiting for transfers between devices, to_all(): lax.all_to_all(jnp.broadcast_to(value[None], (count, *value.shape)), axis...  12.8 us
    ppermute x3, starting transfers between devices, turned(): return lax.ppermute(queries, 'sp', pairs)  12.3 us
    all_to_all x1, waiting for transfers between devices, local(): lax.all_to_all(partial_out, 'sp', 0, 0, axis_index_groups=query_groups)  11.9 us
    ppermute x3, waiting for transfers between devices, turned(): return lax.ppermute(queries, 'sp', pairs)  9.74 us
  transfers between devices with their start and end apart: 9, of which 6 were waited for; matrix products, arithmetic and copies ran while one was open for 12% of the time, Pallas kernels for 10%

profile of v6, /device:TPU:72, one launch (start us, length us, event | category | flops | bytes accessed | tf_op | source)
XLA Modules:
  0.0 156.0 jit_solution(7109898755813692840)
XLA Ops:
  0.6 0.0 copy-start
  0.7 0.6 pad_add_fusion.place_ref
  1.2 2.6 %key_share.1 = bf16[16,80,128]{2,1,0:T(8,128)(2,1)} custom-call(s32[2]{0:T(128)} %pad_add_fusion.place_ref, bf16[256,256]{1,0:T(8,128)(2,1)} %latent_ref.1, bf16[64,256]{1,0:T(8,128)(2,1)} %bitcast.55, f32[1,256]{1,0:T(1,128)} %bitcast.56), custom_call_target="tpu_custom_call" | custom-call | flops 1000000 | bytes 1000000 | tf_op jit(solution)/shard_map/key_share/pallas_call | solution.py:313
  3.8 15.1 %all-to-all-start = ((bf16[16,80,128]{2,1,0:T(8,128)(2,1)}), bf16[16,80,128]{2,1,0:T(8,128)(2,1)S(1)}, u32[]{:S(2)}, u32[]{:S(2)}) async-start(bf16[16,80,128]{2,1,0:T(8,128)(2,1)} %key_share.1), calls=%async_computation | async-start | bytes 655360 | tf_op jit(solution)/shard_map/all_to_all | solution.py:427
  19.0 1.1 fusion.2
  20.1 0.0 copy-start.8
  20.1 13.1 %all-to-all-done = bf16[16,80,128]{2,1,0:T(8,128)(2,1)S(1)} async-done(((bf16[16,80,128]{2,1,0:T(8,128)(2,1)}), bf16[16,80,128]{2,1,0:T(8,128)(2,1)S(1)}, u32[]{:S(2)}, u32[]{:S(2)}) %all-to-all-start) | async-done | bytes 327712 | tf_op jit(solution)/shard_map/all_to_all | solution.py:427
  33.2 1.3 broadcast_in_dim.42
  34.4 4.4 %all-to-all-start.1 = ((bf16[4,16,80,128]{3,2,1,0:T(8,128)(2,1)}), bf16[4,16,80,128]{3,2,1,0:T(8,128)(2,1)S(1)}, u32[]{:S(2)}, u32[]{:S(2)}) async-start(bf16[4,16,80,128]{3,2,1,0:T(8,128)(2,1)} %broadcast_in_dim.42), calls=%async_computation.1 | async-start | bytes 2621440 | tf_op jit(solution)/shard_map/all_to_all | solution.py:384
  38.9 0.7 fusion.30
  39.6 1.5 fusion.5
  41.0 0.1 multiply_reduce_fusion
  41.1 0.8 multiply_multiply_fusion
  42.0 12.8 %all-to-all-done.1.mine_ref = bf16[4,16,80,128]{3,2,1,0:T(8,128)(2,1)S(1)} async-done(((bf16[4,16,80,128]{3,2,1,0:T(8,128)(2,1)}), bf16[4,16,80,128]{3,2,1,0:T(8,128)(2,1)S(1)}, u32[]{:S(2)}, u32[]{:S(2)}) %all-to-all-start.1) | async-done | bytes 1310752 | tf_op jit(solution)/shard_map/all_to_all | solution.py:384
  54.8 1.9 %collective-permute-start.1 = (bf16[4,16,80,128]{3,2,1,0:T(8,128)(2,1)S(1)}, bf16[4,16,80,128]{3,2,1,0:T(8,128)(2,1)}, u32[]{:S(2)}, u32[]{:S(2)}) collective-permute-start(bf16[4,16,80,128]{3,2,1,0:T(8,128)(2,1)S(1)} %all-to-all-done.1.mine_ref), channel_id=1, source_target_pairs={{0,1},{1,0},{2,3},{3,2},{4,5},{5,4},{6,7},{7,6},{8,9},{9,8},{10,11... | collective-permute-start | bytes 3932168 | tf_op jit(solution)/shard_map/ppermute | solution.py:429
  56.7 0.1 subtract_multiply_fusion
  56.8 0.9 subtract_convert_fusion
  57.8 0.7 copy.24
  58.5 1.7 %fusion.7 = bf16[256,2,128]{0,2,1:T(8,128)(2,1)} fusion(f32[256,2,192]{0,2,1:T(8,128)} %multiply_multiply_fusion, f32[128]{0:T(128)S(1)} %slice_multiply_fusion.1), kind=kLoop, calls=%fused_computation.16 | loop fusion | flops 131072 | bytes 393728 | tf_op jit(solution)/shard_map/convert.6
  60.2 1.0 copy.26
  61.2 1.5 pad_maximum_fusion.1.refs_0_
  62.7 1.9 %collective-permute-start.2 = (bf16[256,384]{1,0:T(8,128)(2,1)}, bf16[256,384]{1,0:T(8,128)(2,1)}, u32[]{:S(2)}, u32[]{:S(2)}) collective-permute-start(bf16[256,384]{1,0:T(8,128)(2,1)} %pad_maximum_fusion.1.refs_0_), channel_id=1, source_target_pairs={{0,128},{128,256},{256,384},{384,0},{8,136},{136,264},{264,392},{3... | collective-permute-start | bytes 589832 | tf_op jit(solution)/shard_map/ppermute | solution.py:445
  64.6 5.0 %collective-permute-start.3 = (bf16[256,384]{1,0:T(8,128)(2,1)}, bf16[256,384]{1,0:T(8,128)(2,1)}, u32[]{:S(2)}, u32[]{:S(2)}) collective-permute-start(bf16[256,384]{1,0:T(8,128)(2,1)} %pad_maximum_fusion.1.refs_0_), channel_id=1, source_target_pairs={{0,256},{128,384},{256,0},{384,128},{8,264},{136,392},{264,8},{392... | collective-permute-start | bytes 589832 | tf_op jit(solution)/shard_map/ppermute | solution.py:445
  69.6 5.5 %collective-permute-start.4 = (bf16[256,384]{1,0:T(8,128)(2,1)}, bf16[256,384]{1,0:T(8,128)(2,1)}, u32[]{:S(2)}, u32[]{:S(2)}) collective-permute-start(bf16[256,384]{1,0:T(8,128)(2,1)} %pad_maximum_fusion.1.refs_0_), channel_id=1, source_target_pairs={{0,384},{128,0},{256,128},{384,256},{8,392},{136,8},{264,136},{392... | collective-permute-start | bytes 589832 | tf_op jit(solution)/shard_map/ppermute | solution.py:445
  75.1 1.3 slice.64
  76.4 1.9 %collective-permute-start = (bf16[15,256]{1,0:T(8,128)(2,1)}, bf16[15,256]{1,0:T(8,128)(2,1)S(1)}, u32[]{:S(2)}, u32[]{:S(2)}) collective-permute-start(bf16[15,256]{1,0:T(8,128)(2,1)} %slice.64), channel_id=1, source_target_pairs={{0,8},{8,16},{16,24},{24,32},{32,40},{40,48},{48,56},{56,64},{64,7... | collective-permute-start | bytes 23048 | tf_op jit(solution)/shard_map/ppermute | solution.py:464
  78.3 0.1 stack.45.place_ref
  78.4 1.0 pad_maximum_fusion.refs_4_
  79.4 0.6 minimum_convert_fusion
  80.0 1.0 dynamic-slice_bitcast_fusion.refs_6_
  81.0 4.6 %collective-permute-done.2.refs_1_ = bf16[256,384]{1,0:T(8,128)(2,1)} collective-permute-done((bf16[256,384]{1,0:T(8,128)(2,1)}, bf16[256,384]{1,0:T(8,128)(2,1)}, u32[]{:S(2)}, u32[]{:S(2)}) %collective-permute-start.2) | collective-permute-done | bytes 196640 | tf_op jit(solution)/shard_map/ppermute | solution.py:445
  85.6 5.2 %collective-permute-done.4.refs_3_ = bf16[256,384]{1,0:T(8,128)(2,1)} collective-permute-done((bf16[256,384]{1,0:T(8,128)(2,1)}, bf16[256,384]{1,0:T(8,128)(2,1)}, u32[]{:S(2)}, u32[]{:S(2)}) %collective-permute-start.4) | collective-permute-done | bytes 196640 | tf_op jit(solution)/shard_map/ppermute | solution.py:445
  90.7 15.7 %attend.1 = bf16[4,272,256]{2,1,0:T(8,128)(2,1)S(1)} custom-call(s32[6]{0:T(128)S(1)} %stack.45.place_ref, bf16[4,16,80,128]{3,2,1,0:T(8,128)(2,1)S(1)} %all-to-all-done.1.mine_ref, bf16[4,16,80,128]{3,2,1,0:T(8,128)(2,1)} %collective-permute-done.1.other_ref, bf16[256,384]{1,0:T(8,128)(2,1)} %pad_maximum_fusion.1.refs_0_, ...), custom_call_target="tpu_custom_call" | custom-call | flops 5368709120 | bytes 2621440 | tf_op jit(solution)/shard_map/attend/pallas_call | solution.py:259
  106.5 0.8 copy-done.1
  107.3 4.0 %all-to-all-start.2 = ((bf16[4,272,256]{2,1,0:T(8,128)(2,1)}), bf16[4,272,256]{2,1,0:T(8,128)(2,1)S(1)}, u32[]{:S(2)}, u32[]{:S(2)}) async-start(bf16[4,272,256]{2,1,0:T(8,128)(2,1)} %copy-done.1), calls=%async_computation.2 | async-start | bytes 1114112 | tf_op jit(solution)/shard_map/all_to_all | solution.py:461
  111.3 0.0 copy-start.3
  111.3 1.7 %fusion.1 = bf16[256,128]{1,0:T(8,128)(2,1)S(1)} fusion(f32[271,256]{1,0:T(8,128)S(1)} %maximum_convert_fusion, f32[256]{0:T(256)} %minimum_convert_fusion, pred[]{:T(512)S(6)} %gt.63, pred[]{:T(512)S(6)} %gt.62, pred[]{:T(512)S(6)} %gt.61, pred[]{:T(512)S(6)} %gt.60, pred[]{:T(512)S(6)} %gt.59, pred[]{:T(512)S(6)} %gt.58, pred[]{:T(512)S(6)} %gt.57, ...), kind=kOutput, calls=%fused_computation.5 | convolution fusion | flops 19070976 | bytes 4326928 | tf_op jit(solution)/shard_map/dot_general | solution.py:477
  113.1 1.8 %fusion.34 = f32[128,4096]{1,0:T(8,128)} fusion(bf16[128,128]{1,0:T(8,128)(2,1)S(1)} %bitcast.51, bf16[128,4096]{1,0:T(8,128)(2,1)S(1)} %copy-done.3), kind=kOutput, calls=%fused_computation.76 | convolution fusion | flops 134217728 | bytes 3178496 | tf_op jit(solution)/shard_map/dot_general | solution.py:488
  114.8 11.9 %all-to-all-done.2.parts_ref = bf16[4,272,256]{2,1,0:T(8,128)(2,1)S(1)} async-done(((bf16[4,272,256]{2,1,0:T(8,128)(2,1)}), bf16[4,272,256]{2,1,0:T(8,128)(2,1)S(1)}, u32[]{:S(2)}, u32[]{:S(2)}) %all-to-all-start.2) | async-done | bytes 557088 | tf_op jit(solution)/shard_map/all_to_all | solution.py:461
  126.7 1.0 merge.1
  127.7 0.0 copy-start.4
  127.8 2.1 %fusion = bf16[128,4096]{1,0:T(8,128)(2,1)S(1)} fusion(f32[128,4096]{1,0:T(8,128)} %fusion.34, bf16[128,256]{1,0:T(8,128)(2,1)S(1)} %bitcast.49, bf16[256,4096]{1,0:T(8,128)(2,1)S(1)} %copy-done), kind=kOutput, calls=%fused_computation.2 | convolution fusion | flops 269484032 | bytes 5308416 | tf_op jit(solution)/shard_map/dot_general | solution.py:491
  129.9 1.9 %collective-permute-start.5 = (bf16[128,4096]{1,0:T(8,128)(2,1)S(1)}, bf16[128,4096]{1,0:T(8,128)(2,1)S(1)}, u32[]{:S(2)}, u32[]{:S(2)}) collective-permute-start(bf16[128,4096]{1,0:T(8,128)(2,1)S(1)} %fusion), channel_id=1, source_target_pairs={{0,1},{1,0},{2,3},{3,2},{4,5},{5,4},{6,7},{7,6},{8,9},{9,8},{10,11... | collective-permute-start | bytes 3145736 | tf_op jit(solution)/shard_map/ppermute | solution.py:496
  131.8 0.4 fusion.33
  132.3 2.2 %collective-permute-done.5 = bf16[128,4096]{1,0:T(8,128)(2,1)S(1)} collective-permute-done((bf16[128,4096]{1,0:T(8,128)(2,1)S(1)}, bf16[128,4096]{1,0:T(8,128)(2,1)S(1)}, u32[]{:S(2)}, u32[]{:S(2)}) %collective-permute-start.5) | collective-permute-done | bytes 1048608 | tf_op jit(solution)/shard_map/ppermute | solution.py:496
  134.5 0.6 add_convert_fusion
  135.0 18.8 %all_to_all.20 = bf16[4,32,4096]{2,1,0:T(8,128)(2,1)} all-to-all(bf16[4,32,4096]{2,1,0:T(8,128)(2,1)S(1)} %bitcast.43), channel_id=1, replica_groups=mesh['sp'=64,'fs'=4,'tp'=2] {'fs'}, dimensions={0} | all-to-all | bytes 2097152 | tf_op jit(solution)/shard_map/all_to_all | solution.py:499
  153.8 2.2 %reduce_sum.32 = bf16[32,4096]{1,0:T(8,128)(2,1)} reduce(bf16[4,32,4096]{2,1,0:T(8,128)(2,1)} %all_to_all.20, bf16[]{:T(256)} %constant.102.clone.1), dimensions={0}, to_apply=%region_2.3 | reduce | flops 393216 | bytes 1310722 | tf_op jit(solution)/shard_map/reduce_sum | solution.py:500
  (25 shorter events, 0.1 us)
Async XLA Ops:
  0.6 127.1 %copy-start = (bf16[256,4096]{1,0:T(8,128)(2,1)S(1)}, bf16[256,4096]{1,0:T(8,128)(2,1)}, u32[]{:S(2)}) copy-start(bf16[256,4096]{1,0:T(8,128)(2,1)} %param.34) | copy-start | bytes 6291460
  3.8 29.3 %all-to-all-start = ((bf16[16,80,128]{2,1,0:T(8,128)(2,1)}), bf16[16,80,128]{2,1,0:T(8,128)(2,1)S(1)}, u32[]{:S(2)}, u32[]{:S(2)}) async-start(bf16[16,80,128]{2,1,0:T(8,128)(2,1)} %key_share.1), calls=%async_computation | async-start | bytes 655360 | tf_op jit(solution)/shard_map/all_to_all | solution.py:427
  20.1 19.5 %copy-start.8 = (f32[512]{0:T(512)S(1)}, f32[512]{0:T(512)}, u32[]{:S(2)}) copy-start(f32[512]{0:T(512)} %param.24) | copy-start | bytes 6148
  34.4 6.7 %copy-start.9 = (f32[192]{0:T(256)S(1)}, f32[192]{0:T(256)}, u32[]{:S(2)}) copy-start(f32[192]{0:T(256)} %param.26) | copy-start | bytes 2308
  34.4 22.3 %copy-start.6 = (f32[256,32]{0,1:T(8,128)S(1)}, f32[256,32]{0,1:T(8,128)}, u32[]{:S(2)}) copy-start(f32[256,32]{0,1:T(8,128)} %constant.105.clone) | copy-start | bytes 98308
  34.4 22.3 %copy-start.7 = (f32[256,32]{0,1:T(8,128)S(1)}, f32[256,32]{0,1:T(8,128)}, u32[]{:S(2)}) copy-start(f32[256,32]{0,1:T(8,128)} %constant.106.clone) | copy-start | bytes 98308
  34.4 20.4 %all-to-all-start.1 = ((bf16[4,16,80,128]{3,2,1,0:T(8,128)(2,1)}), bf16[4,16,80,128]{3,2,1,0:T(8,128)(2,1)S(1)}, u32[]{:S(2)}, u32[]{:S(2)}) async-start(bf16[4,16,80,128]{3,2,1,0:T(8,128)(2,1)} %broadcast_in_dim.42), calls=%async_computation.1 | async-start | bytes 2621440 | tf_op jit(solution)/shard_map/all_to_all | solution.py:384
  38.8 19.6 %copy-start.2 = (f32[192]{0:T(256)S(1)}, f32[192]{0:T(256)}, u32[]{:S(2)}) copy-start(f32[192]{0:T(256)} %param.27) | copy-start | bytes 2308
  54.8 35.9 %collective-permute-start.1 = (bf16[4,16,80,128]{3,2,1,0:T(8,128)(2,1)S(1)}, bf16[4,16,80,128]{3,2,1,0:T(8,128)(2,1)}, u32[]{:S(2)}, u32[]{:S(2)}) collective-permute-start(bf16[4,16,80,128]{3,2,1,0:T(8,128)(2,1)S(1)} %all-to-all-done.1.mine_ref), channel_id=1, source_target_pairs={{0,1},{1,0},{2,3},{3,2},{4,5},{5,4},{6,7},{7,6},{8,9},{9,8},{10,11... | collective-permute-start | bytes 3932168 | tf_op jit(solution)/shard_map/ppermute | solution.py:429
  62.7 22.8 %collective-permute-start.2 = (bf16[256,384]{1,0:T(8,128)(2,1)}, bf16[256,384]{1,0:T(8,128)(2,1)}, u32[]{:S(2)}, u32[]{:S(2)}) collective-permute-start(bf16[256,384]{1,0:T(8,128)(2,1)} %pad_maximum_fusion.1.refs_0_), channel_id=1, source_target_pairs={{0,128},{128,256},{256,384},{384,0},{8,136},{136,264},{264,392},{3... | collective-permute-start | bytes 589832 | tf_op jit(solution)/shard_map/ppermute | solution.py:445
  64.6 20.9 %collective-permute-start.3 = (bf16[256,384]{1,0:T(8,128)(2,1)}, bf16[256,384]{1,0:T(8,128)(2,1)}, u32[]{:S(2)}, u32[]{:S(2)}) collective-permute-start(bf16[256,384]{1,0:T(8,128)(2,1)} %pad_maximum_fusion.1.refs_0_), channel_id=1, source_target_pairs={{0,256},{128,384},{256,0},{384,128},{8,264},{136,392},{264,8},{392... | collective-permute-start | bytes 589832 | tf_op jit(solution)/shard_map/ppermute | solution.py:445
  69.6 21.1 %collective-permute-start.4 = (bf16[256,384]{1,0:T(8,128)(2,1)}, bf16[256,384]{1,0:T(8,128)(2,1)}, u32[]{:S(2)}, u32[]{:S(2)}) collective-permute-start(bf16[256,384]{1,0:T(8,128)(2,1)} %pad_maximum_fusion.1.refs_0_), channel_id=1, source_target_pairs={{0,384},{128,0},{256,128},{384,256},{8,392},{136,8},{264,136},{392... | collective-permute-start | bytes 589832 | tf_op jit(solution)/shard_map/ppermute | solution.py:445
  76.4 34.9 %collective-permute-start = (bf16[15,256]{1,0:T(8,128)(2,1)}, bf16[15,256]{1,0:T(8,128)(2,1)S(1)}, u32[]{:S(2)}, u32[]{:S(2)}) collective-permute-start(bf16[15,256]{1,0:T(8,128)(2,1)} %slice.64), channel_id=1, source_target_pairs={{0,8},{8,16},{16,24},{24,32},{32,40},{40,48},{48,56},{56,64},{64,7... | collective-permute-start | bytes 23048 | tf_op jit(solution)/shard_map/ppermute | solution.py:464
  90.7 20.5 %copy-start.5 = (bf16[256,256]{1,0:T(8,128)(2,1)S(1)}, bf16[256,256]{1,0:T(8,128)(2,1)}, u32[]{:S(2)}) copy-start(bf16[256,256]{1,0:T(8,128)(2,1)} %param.23) | copy-start | bytes 393220
  106.5 0.8 copy-start.1
  107.3 19.5 %all-to-all-start.2 = ((bf16[4,272,256]{2,1,0:T(8,128)(2,1)}), bf16[4,272,256]{2,1,0:T(8,128)(2,1)S(1)}, u32[]{:S(2)}, u32[]{:S(2)}) async-start(bf16[4,272,256]{2,1,0:T(8,128)(2,1)} %copy-done.1), calls=%async_computation.2 | async-start | bytes 1114112 | tf_op jit(solution)/shard_map/all_to_all | solution.py:461
  111.3 1.7 %copy-start.3 = (bf16[128,4096]{1,0:T(8,128)(2,1)S(1)}, bf16[128,4096]{1,0:T(8,128)(2,1)}, u32[]{:S(2)}) copy-start(bf16[128,4096]{1,0:T(8,128)(2,1)} %param.33) | copy-start | bytes 3145732
  127.7 4.1 %copy-start.4 = (bf16[128,4096]{1,0:T(8,128)(2,1)S(1)}, bf16[128,4096]{1,0:T(8,128)(2,1)}, u32[]{:S(2)}) copy-start(bf16[128,4096]{1,0:T(8,128)(2,1)} %param.33) | copy-start | bytes 3145732
  129.9 4.6 %collective-permute-start.5 = (bf16[128,4096]{1,0:T(8,128)(2,1)S(1)}, bf16[128,4096]{1,0:T(8,128)(2,1)S(1)}, u32[]{:S(2)}, u32[]{:S(2)}) collective-permute-start(bf16[128,4096]{1,0:T(8,128)(2,1)S(1)} %fusion), channel_id=1, source_target_pairs={{0,1},{1,0},{2,3},{3,2},{4,5},{5,4},{6,7},{7,6},{8,9},{9,8},{10,11... | collective-permute-start | bytes 3145736 | tf_op jit(solution)/shard_map/ppermute | solution.py:496

commit v7 on v6

--- a/solution.py
+++ b/solution.py
@@ -287,10 +287,10 @@
 
 
 def share_kernel(
-    place_ref, latent_ref, rope_ref, gain_ref, out_ref, half_ref, all_ref, scale_ref, sems
+    latent_ref, rope_ref, gain_ref, out_ref, half_ref, all_ref, scale_ref, own_ref, sems
 ):
     channels = latent_ref.shape[1]
-    at = pl.ds(pl.multiple_of(place_ref[0] * HALF, HALF), HALF)
+    at = pl.ds(pl.multiple_of(lax.axis_index("tp") * HALF, HALF), HALF)
     copies = [
         pltpu.make_async_copy(latent_ref.at[at], half_ref, sems.at[0]),
         pltpu.make_async_copy(rope_ref.at[:, at], all_ref.at[pl.ds(channels, ROPE)], sems.at[1]),
@@ -302,29 +302,36 @@
         copy.wait()
     normed = row_norm(half_ref[...].astype(jnp.float32), scale_ref[...]).astype(jnp.bfloat16)
     all_ref[:channels] = normed.T
-    own = all_ref[pl.ds(pl.multiple_of(place_ref[1] * 80, 16), 80), :]
-    for n in range(out_ref.shape[0]):
-        out_ref[n] = own
-
-
-def key_share(place, latent, rope, gain, count):
+    own_ref[...] = all_ref[pl.ds(pl.multiple_of(lax.axis_index("fs") * 80, 16), 80), :]
+    copies = [
+        pltpu.make_async_copy(own_ref, out_ref.at[n], sems.at[3 + n])
+        for n in range(out_ref.shape[0])
+    ]
+    for copy in copies:
+        copy.start()
+    for copy in copies:
+        copy.wait()
+
+
+def key_share(latent, rope, gain, count):
     channels = latent.shape[1]
     hbm = pl.BlockSpec(memory_space=pl.ANY)
     return pl.pallas_call(
         share_kernel,
         out_shape=jax.ShapeDtypeStruct((count, 80, HALF), jnp.bfloat16),
-        in_specs=[pl.BlockSpec(memory_space=pltpu.SMEM), hbm, hbm, hbm],
-        out_specs=pl.BlockSpec(memory_space=pltpu.VMEM),
+        in_specs=[hbm, hbm, hbm],
+        out_specs=hbm,
         scratch_shapes=[
             pltpu.VMEM((HALF, channels), jnp.bfloat16),
             pltpu.VMEM((channels + ROPE, HALF), jnp.bfloat16),
             pltpu.VMEM((1, channels), jnp.float32),
-            pltpu.SemaphoreType.DMA((3,)),
+            pltpu.VMEM((80, HALF), jnp.bfloat16),
+            pltpu.SemaphoreType.DMA((3 + count,)),
         ],
         cost_estimate=pl.CostEstimate(flops=10**6, bytes_accessed=10**6, transcendentals=HALF),
         compiler_params=pltpu.CompilerParams(vmem_limit_bytes=SHARE_LIMIT),
         name="key_share",
-    )(place, latent, rope, gain[None])
+    )(latent, rope, gain[None])
 
 
 def merge_kernel(parts_ref, out_ref, log_ref, turn_ref):
@@ -422,8 +429,7 @@
     halves = [np.concatenate([in_cos.T, in_sin.T])[:, c * HALF : (c + 1) * HALF] for c in range(2)]
     tables = np.stack([np.concatenate([halves[c], halves[1 - c], plane_turns]) for c in range(2)])
 
-    seat = jnp.stack([core, line]).astype(jnp.int32)
-    share = key_share(seat, kv_latent, key_rope.T, kv_lat_gain, 2 * Y)
+    share = key_share(kv_latent, key_rope.T, kv_lat_gain, 2 * Y)
     mine = lax.all_to_all(share, "sp", 0, 0, axis_index_groups=key_groups)
     mine = to_all(mine, "fs")
     other = lax.ppermute(mine, "tp", [(0, 1), (1, 0)])

time: 157 us -> 156 us (level)
    another operation x3 -> x2, other arithmetic: 3.18 us -> 2.59 us
where the time goes in v7:
time: 156 us; the launch traced here: 155 us
  waiting for transfers between devices  49.9 us (32%)
  starting transfers between devices  41.6 us (27%)
  blocking collectives  18.8 us (12%)
  Pallas kernels  18.7 us (12%)
  other arithmetic  9.96 us (6%)
  matrix products  8.04 us (5%)
  local copies, waits for them, and re-layouts  6.93 us (4%)
    all_to_all x1, blocking collectives, local(): chip = lax.all_to_all(chip.reshape(lines, -1, chip.shape[1]), 'fs', 0, 0)  18.8 us
    pallas_call x1, Pallas kernels, attend(): pl.pallas_call(attend_kernel, out_shape=jax.ShapeDtypeStruct((MEMBERS, ro...  15.7 us
    all_to_all x1, starting transfers between devices, local(): mine = lax.all_to_all(share, 'sp', 0, 0, axis_index_groups=key_groups)  15.1 us
    all_to_all x1, waiting for transfers between devices, local(): mine = lax.all_to_all(share, 'sp', 0, 0, axis_index_groups=key_groups)  13.1 us
    all_to_all x1, waiting for transfers between devices, to_all(): lax.all_to_all(jnp.broadcast_to(value[None], (count, *value.shape)), axis...  12.8 us
    ppermute x3, starting transfers between devices, turned(): return lax.ppermute(queries, 'sp', pairs)  12.3 us
    all_to_all x1, waiting for transfers between devices, local(): lax.all_to_all(partial_out, 'sp', 0, 0, axis_index_groups=query_groups)  12.1 us
    ppermute x3, waiting for transfers between devices, turned(): return lax.ppermute(queries, 'sp', pairs)  9.74 us
  transfers between devices with their start and end apart: 9, of which 6 were waited for; matrix products, arithmetic and copies ran while one was open for 12% of the time, Pallas kernels for 10%

profile of v7, /device:TPU:72, one launch (start us, length us, event | category | flops | bytes accessed | tf_op | source)
XLA Modules:
  0.0 155.0 jit_solution(18436332314365859928)
XLA Ops:
  0.6 0.0 copy-start
  0.6 2.1 %key_share.1 = bf16[16,80,128]{2,1,0:T(8,128)(2,1)} custom-call(bf16[256,256]{1,0:T(8,128)(2,1)} %latent_ref.1, bf16[64,256]{1,0:T(8,128)(2,1)} %bitcast.53, f32[1,256]{1,0:T(1,128)} %bitcast.54), custom_call_target="tpu_custom_call" | custom-call | flops 1000000 | bytes 1000000 | tf_op jit(solution)/shard_map/key_share/pallas_call | solution.py:319
  2.7 15.1 %all-to-all-start = ((bf16[16,80,128]{2,1,0:T(8,128)(2,1)}), bf16[16,80,128]{2,1,0:T(8,128)(2,1)S(1)}, u32[]{:S(2)}, u32[]{:S(2)}) async-start(bf16[16,80,128]{2,1,0:T(8,128)(2,1)} %key_share.1), calls=%async_computation | async-start | bytes 655360 | tf_op jit(solution)/shard_map/all_to_all | solution.py:433
  17.8 1.1 fusion.2
  18.9 0.0 copy-start.8
  18.9 13.1 %all-to-all-done = bf16[16,80,128]{2,1,0:T(8,128)(2,1)S(1)} async-done(((bf16[16,80,128]{2,1,0:T(8,128)(2,1)}), bf16[16,80,128]{2,1,0:T(8,128)(2,1)S(1)}, u32[]{:S(2)}, u32[]{:S(2)}) %all-to-all-start) | async-done | bytes 327712 | tf_op jit(solution)/shard_map/all_to_all | solution.py:433
  32.0 1.3 broadcast_in_dim.42
  33.3 4.4 %all-to-all-start.1 = ((bf16[4,16,80,128]{3,2,1,0:T(8,128)(2,1)}), bf16[4,16,80,128]{3,2,1,0:T(8,128)(2,1)S(1)}, u32[]{:S(2)}, u32[]{:S(2)}) async-start(bf16[4,16,80,128]{3,2,1,0:T(8,128)(2,1)} %broadcast_in_dim.42), calls=%async_computation.1 | async-start | bytes 2621440 | tf_op jit(solution)/shard_map/all_to_all | solution.py:391
  37.7 0.7 fusion.30
  38.4 1.5 fusion.5
  39.9 0.1 multiply_reduce_fusion
  40.0 0.8 multiply_multiply_fusion
  40.8 12.8 %all-to-all-done.1.mine_ref = bf16[4,16,80,128]{3,2,1,0:T(8,128)(2,1)S(1)} async-done(((bf16[4,16,80,128]{3,2,1,0:T(8,128)(2,1)}), bf16[4,16,80,128]{3,2,1,0:T(8,128)(2,1)S(1)}, u32[]{:S(2)}, u32[]{:S(2)}) %all-to-all-start.1) | async-done | bytes 1310752 | tf_op jit(solution)/shard_map/all_to_all | solution.py:391
  53.7 1.9 %collective-permute-start.1 = (bf16[4,16,80,128]{3,2,1,0:T(8,128)(2,1)S(1)}, bf16[4,16,80,128]{3,2,1,0:T(8,128)(2,1)}, u32[]{:S(2)}, u32[]{:S(2)}) collective-permute-start(bf16[4,16,80,128]{3,2,1,0:T(8,128)(2,1)S(1)} %all-to-all-done.1.mine_ref), channel_id=1, source_target_pairs={{0,1},{1,0},{2,3},{3,2},{4,5},{5,4},{6,7},{7,6},{8,9},{9,8},{10,11... | collective-permute-start | bytes 3932168 | tf_op jit(solution)/shard_map/ppermute | solution.py:435
  55.6 0.1 subtract_multiply_fusion
  55.7 0.9 subtract_convert_fusion
  56.6 0.7 copy.24
  57.4 1.7 %fusion.7 = bf16[256,2,128]{0,2,1:T(8,128)(2,1)} fusion(f32[256,2,192]{0,2,1:T(8,128)} %multiply_multiply_fusion, f32[128]{0:T(128)S(1)} %slice_multiply_fusion.1), kind=kLoop, calls=%fused_computation.16 | loop fusion | flops 131072 | bytes 393728 | tf_op jit(solution)/shard_map/convert.6
  59.0 1.0 copy.26
  60.1 1.5 pad_maximum_fusion.1.refs_0_
  61.6 1.9 %collective-permute-start.2 = (bf16[256,384]{1,0:T(8,128)(2,1)}, bf16[256,384]{1,0:T(8,128)(2,1)}, u32[]{:S(2)}, u32[]{:S(2)}) collective-permute-start(bf16[256,384]{1,0:T(8,128)(2,1)} %pad_maximum_fusion.1.refs_0_), channel_id=1, source_target_pairs={{0,128},{128,256},{256,384},{384,0},{8,136},{136,264},{264,392},{3... | collective-permute-start | bytes 589832 | tf_op jit(solution)/shard_map/ppermute | solution.py:451
  63.5 5.0 %collective-permute-start.3 = (bf16[256,384]{1,0:T(8,128)(2,1)}, bf16[256,384]{1,0:T(8,128)(2,1)}, u32[]{:S(2)}, u32[]{:S(2)}) collective-permute-start(bf16[256,384]{1,0:T(8,128)(2,1)} %pad_maximum_fusion.1.refs_0_), channel_id=1, source_target_pairs={{0,256},{128,384},{256,0},{384,128},{8,264},{136,392},{264,8},{392... | collective-permute-start | bytes 589832 | tf_op jit(solution)/shard_map/ppermute | solution.py:451
  68.5 5.5 %collective-permute-start.4 = (bf16[256,384]{1,0:T(8,128)(2,1)}, bf16[256,384]{1,0:T(8,128)(2,1)}, u32[]{:S(2)}, u32[]{:S(2)}) collective-permute-start(bf16[256,384]{1,0:T(8,128)(2,1)} %pad_maximum_fusion.1.refs_0_), channel_id=1, source_target_pairs={{0,384},{128,0},{256,128},{384,256},{8,392},{136,8},{264,136},{392... | collective-permute-start | bytes 589832 | tf_op jit(solution)/shard_map/ppermute | solution.py:451
  73.9 1.3 slice.64
  75.2 1.9 %collective-permute-start = (bf16[15,256]{1,0:T(8,128)(2,1)}, bf16[15,256]{1,0:T(8,128)(2,1)S(1)}, u32[]{:S(2)}, u32[]{:S(2)}) collective-permute-start(bf16[15,256]{1,0:T(8,128)(2,1)} %slice.64), channel_id=1, source_target_pairs={{0,8},{8,16},{16,24},{24,32},{32,40},{40,48},{48,56},{56,64},{64,7... | collective-permute-start | bytes 23048 | tf_op jit(solution)/shard_map/ppermute | solution.py:470
  77.2 0.1 stack.36.place_ref
  77.3 1.0 pad_maximum_fusion.refs_4_
  78.3 0.6 minimum_convert_fusion
  78.9 1.0 dynamic-slice_bitcast_fusion.refs_6_
  79.9 4.5 %collective-permute-done.2.refs_1_ = bf16[256,384]{1,0:T(8,128)(2,1)} collective-permute-done((bf16[256,384]{1,0:T(8,128)(2,1)}, bf16[256,384]{1,0:T(8,128)(2,1)}, u32[]{:S(2)}, u32[]{:S(2)}) %collective-permute-start.2) | collective-permute-done | bytes 196640 | tf_op jit(solution)/shard_map/ppermute | solution.py:451
  84.4 5.2 %collective-permute-done.4.refs_3_ = bf16[256,384]{1,0:T(8,128)(2,1)} collective-permute-done((bf16[256,384]{1,0:T(8,128)(2,1)}, bf16[256,384]{1,0:T(8,128)(2,1)}, u32[]{:S(2)}, u32[]{:S(2)}) %collective-permute-start.4) | collective-permute-done | bytes 196640 | tf_op jit(solution)/shard_map/ppermute | solution.py:451
  89.6 0.0 collective-permute-done.1.other_ref
  89.6 15.7 %attend.1 = bf16[4,272,256]{2,1,0:T(8,128)(2,1)S(1)} custom-call(s32[6]{0:T(128)S(1)} %stack.36.place_ref, bf16[4,16,80,128]{3,2,1,0:T(8,128)(2,1)S(1)} %all-to-all-done.1.mine_ref, bf16[4,16,80,128]{3,2,1,0:T(8,128)(2,1)} %collective-permute-done.1.other_ref, bf16[256,384]{1,0:T(8,128)(2,1)} %pad_maximum_fusion.1.refs_0_, ...), custom_call_target="tpu_custom_call" | custom-call | flops 5368709120 | bytes 2621440 | tf_op jit(solution)/shard_map/attend/pallas_call | solution.py:259
  105.3 0.8 copy-done.1
  106.1 4.0 %all-to-all-start.2 = ((bf16[4,272,256]{2,1,0:T(8,128)(2,1)}), bf16[4,272,256]{2,1,0:T(8,128)(2,1)S(1)}, u32[]{:S(2)}, u32[]{:S(2)}) async-start(bf16[4,272,256]{2,1,0:T(8,128)(2,1)} %copy-done.1), calls=%async_computation.2 | async-start | bytes 1114112 | tf_op jit(solution)/shard_map/all_to_all | solution.py:467
  110.2 0.0 copy-start.3
  110.2 1.7 %fusion.1 = bf16[256,128]{1,0:T(8,128)(2,1)S(1)} fusion(f32[271,256]{1,0:T(8,128)S(1)} %maximum_convert_fusion, f32[256]{0:T(256)} %minimum_convert_fusion, pred[]{:T(512)S(6)} %gt.63, pred[]{:T(512)S(6)} %gt.62, pred[]{:T(512)S(6)} %gt.61, pred[]{:T(512)S(6)} %gt.60, pred[]{:T(512)S(6)} %gt.59, pred[]{:T(512)S(6)} %gt.58, pred[]{:T(512)S(6)} %gt.57, ...), kind=kOutput, calls=%fused_computation.5 | convolution fusion | flops 19070976 | bytes 4326928 | tf_op jit(solution)/shard_map/dot_general | solution.py:483
  111.9 1.8 %fusion.34 = f32[128,4096]{1,0:T(8,128)} fusion(bf16[128,128]{1,0:T(8,128)(2,1)S(1)} %bitcast.49, bf16[128,4096]{1,0:T(8,128)(2,1)S(1)} %copy-done.3), kind=kOutput, calls=%fused_computation.75 | convolution fusion | flops 134217728 | bytes 3178496 | tf_op jit(solution)/shard_map/dot_general | solution.py:494
  113.7 12.1 %all-to-all-done.2.parts_ref = bf16[4,272,256]{2,1,0:T(8,128)(2,1)S(1)} async-done(((bf16[4,272,256]{2,1,0:T(8,128)(2,1)}), bf16[4,272,256]{2,1,0:T(8,128)(2,1)S(1)}, u32[]{:S(2)}, u32[]{:S(2)}) %all-to-all-start.2) | async-done | bytes 557088 | tf_op jit(solution)/shard_map/all_to_all | solution.py:467
  125.7 1.0 merge.1
  126.8 0.0 copy-start.4
  126.8 2.1 %fusion = bf16[128,4096]{1,0:T(8,128)(2,1)S(1)} fusion(f32[128,4096]{1,0:T(8,128)} %fusion.34, bf16[128,256]{1,0:T(8,128)(2,1)S(1)} %bitcast.47, bf16[256,4096]{1,0:T(8,128)(2,1)S(1)} %copy-done), kind=kOutput, calls=%fused_computation.2 | convolution fusion | flops 269484032 | bytes 5308416 | tf_op jit(solution)/shard_map/dot_general | solution.py:497
  128.9 1.9 %collective-permute-start.5 = (bf16[128,4096]{1,0:T(8,128)(2,1)S(1)}, bf16[128,4096]{1,0:T(8,128)(2,1)S(1)}, u32[]{:S(2)}, u32[]{:S(2)}) collective-permute-start(bf16[128,4096]{1,0:T(8,128)(2,1)S(1)} %fusion), channel_id=1, source_target_pairs={{0,1},{1,0},{2,3},{3,2},{4,5},{5,4},{6,7},{7,6},{8,9},{9,8},{10,11... | collective-permute-start | bytes 3145736 | tf_op jit(solution)/shard_map/ppermute | solution.py:502
  130.8 0.4 fusion.33
  131.3 2.2 %collective-permute-done.5 = bf16[128,4096]{1,0:T(8,128)(2,1)S(1)} collective-permute-done((bf16[128,4096]{1,0:T(8,128)(2,1)S(1)}, bf16[128,4096]{1,0:T(8,128)(2,1)S(1)}, u32[]{:S(2)}, u32[]{:S(2)}) %collective-permute-start.5) | collective-permute-done | bytes 1048608 | tf_op jit(solution)/shard_map/ppermute | solution.py:502
  133.5 0.6 add_convert_fusion
  134.0 18.8 %all_to_all.20 = bf16[4,32,4096]{2,1,0:T(8,128)(2,1)} all-to-all(bf16[4,32,4096]{2,1,0:T(8,128)(2,1)S(1)} %bitcast.41), channel_id=1, replica_groups=mesh['sp'=64,'fs'=4,'tp'=2] {'fs'}, dimensions={0} | all-to-all | bytes 2097152 | tf_op jit(solution)/shard_map/all_to_all | solution.py:505
  152.8 2.2 %reduce_sum.32 = bf16[32,4096]{1,0:T(8,128)(2,1)} reduce(bf16[4,32,4096]{2,1,0:T(8,128)(2,1)} %all_to_all.20, bf16[]{:T(256)} %constant.102.clone.1), dimensions={0}, to_apply=%region_2.3 | reduce | flops 393216 | bytes 1310722 | tf_op jit(solution)/shard_map/reduce_sum | solution.py:506
  (24 shorter events, 0.1 us)
Async XLA Ops:
  0.6 126.1 %copy-start = (bf16[256,4096]{1,0:T(8,128)(2,1)S(1)}, bf16[256,4096]{1,0:T(8,128)(2,1)}, u32[]{:S(2)}) copy-start(bf16[256,4096]{1,0:T(8,128)(2,1)} %param.34) | copy-start | bytes 6291460
  2.7 29.3 %all-to-all-start = ((bf16[16,80,128]{2,1,0:T(8,128)(2,1)}), bf16[16,80,128]{2,1,0:T(8,128)(2,1)S(1)}, u32[]{:S(2)}, u32[]{:S(2)}) async-start(bf16[16,80,128]{2,1,0:T(8,128)(2,1)} %key_share.1), calls=%async_computation | async-start | bytes 655360 | tf_op jit(solution)/shard_map/all_to_all | solution.py:433
  18.9 19.5 %copy-start.8 = (f32[512]{0:T(512)S(1)}, f32[512]{0:T(512)}, u32[]{:S(2)}) copy-start(f32[512]{0:T(512)} %param.24) | copy-start | bytes 6148
  33.3 6.7 %copy-start.9 = (f32[192]{0:T(256)S(1)}, f32[192]{0:T(256)}, u32[]{:S(2)}) copy-start(f32[192]{0:T(256)} %param.26) | copy-start | bytes 2308
  33.3 22.3 %copy-start.6 = (f32[256,32]{0,1:T(8,128)S(1)}, f32[256,32]{0,1:T(8,128)}, u32[]{:S(2)}) copy-start(f32[256,32]{0,1:T(8,128)} %constant.105.clone) | copy-start | bytes 98308
  33.3 22.3 %copy-start.7 = (f32[256,32]{0,1:T(8,128)S(1)}, f32[256,32]{0,1:T(8,128)}, u32[]{:S(2)}) copy-start(f32[256,32]{0,1:T(8,128)} %constant.106.clone) | copy-start | bytes 98308
  33.3 20.4 %all-to-all-start.1 = ((bf16[4,16,80,128]{3,2,1,0:T(8,128)(2,1)}), bf16[4,16,80,128]{3,2,1,0:T(8,128)(2,1)S(1)}, u32[]{:S(2)}, u32[]{:S(2)}) async-start(bf16[4,16,80,128]{3,2,1,0:T(8,128)(2,1)} %broadcast_in_dim.42), calls=%async_computation.1 | async-start | bytes 2621440 | tf_op jit(solution)/shard_map/all_to_all | solution.py:391
  37.7 19.6 %copy-start.2 = (f32[192]{0:T(256)S(1)}, f32[192]{0:T(256)}, u32[]{:S(2)}) copy-start(f32[192]{0:T(256)} %param.27) | copy-start | bytes 2308
  53.7 35.9 %collective-permute-start.1 = (bf16[4,16,80,128]{3,2,1,0:T(8,128)(2,1)S(1)}, bf16[4,16,80,128]{3,2,1,0:T(8,128)(2,1)}, u32[]{:S(2)}, u32[]{:S(2)}) collective-permute-start(bf16[4,16,80,128]{3,2,1,0:T(8,128)(2,1)S(1)} %all-to-all-done.1.mine_ref), channel_id=1, source_target_pairs={{0,1},{1,0},{2,3},{3,2},{4,5},{5,4},{6,7},{7,6},{8,9},{9,8},{10,11... | collective-permute-start | bytes 3932168 | tf_op jit(solution)/shard_map/ppermute | solution.py:435
  61.6 22.8 %collective-permute-start.2 = (bf16[256,384]{1,0:T(8,128)(2,1)}, bf16[256,384]{1,0:T(8,128)(2,1)}, u32[]{:S(2)}, u32[]{:S(2)}) collective-permute-start(bf16[256,384]{1,0:T(8,128)(2,1)} %pad_maximum_fusion.1.refs_0_), channel_id=1, source_target_pairs={{0,128},{128,256},{256,384},{384,0},{8,136},{136,264},{264,392},{3... | collective-permute-start | bytes 589832 | tf_op jit(solution)/shard_map/ppermute | solution.py:451
  63.5 20.9 %collective-permute-start.3 = (bf16[256,384]{1,0:T(8,128)(2,1)}, bf16[256,384]{1,0:T(8,128)(2,1)}, u32[]{:S(2)}, u32[]{:S(2)}) collective-permute-start(bf16[256,384]{1,0:T(8,128)(2,1)} %pad_maximum_fusion.1.refs_0_), channel_id=1, source_target_pairs={{0,256},{128,384},{256,0},{384,128},{8,264},{136,392},{264,8},{392... | collective-permute-start | bytes 589832 | tf_op jit(solution)/shard_map/ppermute | solution.py:451
  68.5 21.1 %collective-permute-start.4 = (bf16[256,384]{1,0:T(8,128)(2,1)}, bf16[256,384]{1,0:T(8,128)(2,1)}, u32[]{:S(2)}, u32[]{:S(2)}) collective-permute-start(bf16[256,384]{1,0:T(8,128)(2,1)} %pad_maximum_fusion.1.refs_0_), channel_id=1, source_target_pairs={{0,384},{128,0},{256,128},{384,256},{8,392},{136,8},{264,136},{392... | collective-permute-start | bytes 589832 | tf_op jit(solution)/shard_map/ppermute | solution.py:451
  75.2 34.9 %collective-permute-start = (bf16[15,256]{1,0:T(8,128)(2,1)}, bf16[15,256]{1,0:T(8,128)(2,1)S(1)}, u32[]{:S(2)}, u32[]{:S(2)}) collective-permute-start(bf16[15,256]{1,0:T(8,128)(2,1)} %slice.64), channel_id=1, source_target_pairs={{0,8},{8,16},{16,24},{24,32},{32,40},{40,48},{48,56},{56,64},{64,7... | collective-permute-start | bytes 23048 | tf_op jit(solution)/shard_map/ppermute | solution.py:470
  89.6 20.5 %copy-start.5 = (bf16[256,256]{1,0:T(8,128)(2,1)S(1)}, bf16[256,256]{1,0:T(8,128)(2,1)}, u32[]{:S(2)}) copy-start(bf16[256,256]{1,0:T(8,128)(2,1)} %param.23) | copy-start | bytes 393220
  105.3 0.8 copy-start.1
  106.1 19.6 %all-to-all-start.2 = ((bf16[4,272,256]{2,1,0:T(8,128)(2,1)}), bf16[4,272,256]{2,1,0:T(8,128)(2,1)S(1)}, u32[]{:S(2)}, u32[]{:S(2)}) async-start(bf16[4,272,256]{2,1,0:T(8,128)(2,1)} %copy-done.1), calls=%async_computation.2 | async-start | bytes 1114112 | tf_op jit(solution)/shard_map/all_to_all | solution.py:467
  110.2 1.7 %copy-start.3 = (bf16[128,4096]{1,0:T(8,128)(2,1)S(1)}, bf16[128,4096]{1,0:T(8,128)(2,1)}, u32[]{:S(2)}) copy-start(bf16[128,4096]{1,0:T(8,128)(2,1)} %param.33) | copy-start | bytes 3145732
  126.8 4.1 %copy-start.4 = (bf16[128,4096]{1,0:T(8,128)(2,1)S(1)}, bf16[128,4096]{1,0:T(8,128)(2,1)}, u32[]{:S(2)}) copy-start(bf16[128,4096]{1,0:T(8,128)(2,1)} %param.33) | copy-start | bytes 3145732
  128.9 4.6 %collective-permute-start.5 = (bf16[128,4096]{1,0:T(8,128)(2,1)S(1)}, bf16[128,4096]{1,0:T(8,128)(2,1)S(1)}, u32[]{:S(2)}, u32[]{:S(2)}) collective-permute-start(bf16[128,4096]{1,0:T(8,128)(2,1)S(1)} %fusion), channel_id=1, source_target_pairs={{0,1},{1,0},{2,3},{3,2},{4,5},{5,4},{6,7},{7,6},{8,9},{9,8},{10,11... | collective-permute-start | bytes 3145736 | tf_op jit(solution)/shard_map/ppermute | solution.py:502
